TPU v7x, 128 devices: a whole 4x4x4 slice. The times are simulated.
128 devices in a mesh: kv: 16 (over z, x), tp: 8 (over y, core).
Axes of the slice: x: 4, y: 4, z: 4, core: 2. Of those that a mesh axis runs over, the one named last changes fastest.
Arguments:
- tokens: bfloat16 [96, 4096], P(None, 'kv'), may hold values from -210 to 210
- norm_gain: float32 [4096], P('kv'), may hold values from 0.1 to 1.9
- w_query: bfloat16 [4096, 4096], P('kv', 'tp'), may hold values from -1 to 1
- w_key: bfloat16 [4096, 4096], P('kv', 'tp'), may hold values from -2 to 2
- w_value: bfloat16 [4096, 4096], P('kv', 'tp'), may hold values from -0.09375 to 0.09375
- w_output: bfloat16 [4096, 4096], P('tp', 'kv'), may hold values from -0.09375 to 0.09375
- cache_keys: bfloat16 [4, 8192, 4096], P(None, 'kv', 'tp'), may hold values from -820 to 820
- cache_values: bfloat16 [4, 8192, 4096], P(None, 'kv', 'tp'), may hold values from -6 to 6
- map_lambda: float32 [64], P('tp'), may hold values from 0.3 to 0.8
- out_gain: float32 [4096], P('tp'), may hold values from 0.1 to 1.9
- parents: int32 [4, 24], replicated, may hold values from -1 to 22, as said below
- lengths: int32 [4], replicated, may hold values from 4096 to 8144, as said below
- accepted: int32 [4], replicated, may hold values from 0 to 24
Outputs:
- mixed: bfloat16 [96, 4096], P(None, 'kv')
- new_keys: bfloat16 [4, 8192, 4096], P(None, 'kv', 'tp')
- new_values: bfloat16 [4, 8192, 4096], P(None, 'kv', 'tp')
Inputs may be any that keep to these rules, and one draw needn't show every extreme that they name: parents[b, j] lies between -1 and j - 1. `lengths`: some sequence has exactly the largest value.
All inputs are finite; a program needn't handle non-finite values.
Results may differ from a plain program's by a relative error of at most 0.029.
Values may be sent and summed in bfloat16 or wider, within the bound.
A program may use at most 128 MiB of HBM per device.

v0:
```python
import functools

import jax
import jax.numpy as jnp
from jax import lax
from jax.sharding import Mesh
from jax.sharding import PartitionSpec as P

D = 4096
HEAD = 64
QK = 32
SEQS = 4
PROP = 24
KV = ("kv_0", "kv_1")


epsilon = 1e-05
masked_low = -1e30


def over_axes(array, axes):
    return functools.reduce(lax.psum, axes, array)


def cut_along(array, dim, length):
    lengths = array.shape
    blocks = array.reshape(*lengths[:dim], length, lengths[dim] // length, *lengths[dim + 1 :])
    return jnp.moveaxis(blocks, dim, 0)


def sum_at_owner(array, axis, dim):
    blocks = cut_along(array, dim, lax.axis_size(axis))
    arrived = lax.all_to_all(blocks, axis, split_axis=0, concat_axis=0, tiled=True)
    return arrived.sum(axis=0)


def in_order(blocks, dim):
    blocks = jnp.moveaxis(blocks, 0, dim)
    lengths = blocks.shape
    return blocks.reshape(*lengths[:dim], lengths[dim] * lengths[dim + 1], *lengths[dim + 2 :])


def copy_for_each(array, axis):
    copies = jnp.broadcast_to(array, (lax.axis_size(axis), *array.shape))
    return lax.all_to_all(copies, axis, split_axis=0, concat_axis=0, tiled=True)


def gathered_copies(array, axis, dim):
    return in_order(copy_for_each(array, axis), dim)


def folded_in_pairs(pieces, combine):
    while len(jax.tree.leaves(pieces)[0]) > 1:
        pieces = jax.vmap(combine)(
            *(jax.tree.map(lambda part: part[side::2], pieces) for side in (0, 1))
        )
    return jax.tree.map(lambda part: part[0], pieces)


def combined_all(array, axis, combine):
    pieces = jax.tree.map(
        lambda part: copy_for_each(part, axis),
        jax.tree.map(
            lambda part, kind: part.astype(kind), array, (jnp.bfloat16, jnp.bfloat16, jnp.bfloat16)
        ),
    )
    return folded_in_pairs(
        jax.tree.map(lambda part, own: part.astype(own.dtype), pieces, array), combine
    )


def over_copies(array, axis):
    return copy_for_each(array, axis).astype(jnp.float32).sum(axis=0)


def ancestry(parents):
    count = parents.shape[1]
    places = jnp.arange(count, dtype=jnp.int32)
    parent_links = (parents[:, :, None] == places[None, None, :]).astype(jnp.float32)
    identity = jnp.eye(count, dtype=jnp.float32)[None]

    def extend(turn_index, reached):
        return jnp.minimum(1.0, identity + jnp.einsum("bji,bik->bjk", parent_links, reached))

    reached = lax.fori_loop(0, count, extend, jnp.broadcast_to(identity, parent_links.shape))
    return reached > 0.5


def scaled_values(values, factor, local_heads):
    shaped = values.astype(jnp.float32).reshape(values.shape[0], 2, PROP, local_heads, HEAD)
    return shaped * jnp.transpose(factor, (0, 1, 3, 2))[..., None]


def combine_blocks(earlier, later):
    max_first, total_first, values_first = earlier
    max_second, total_second, values_second = later
    largest = jnp.maximum(max_first, max_second)
    factor_first = jnp.exp(max_first - largest)
    factor_second = jnp.exp(max_second - largest)
    summed_total = total_first * factor_first + total_second * factor_second
    local_heads = max_first.shape[2]
    merged = scaled_values(values_first, factor_first, local_heads) + scaled_values(
        values_second, factor_second, local_heads
    )
    merged = merged.reshape(values_first.shape).astype(jnp.bfloat16)
    return (largest, summed_total, merged)


def local(
    tokens,
    norm_gain,
    w_query,
    w_key,
    w_value,
    w_output,
    cache_keys,
    cache_values,
    map_lambda,
    out_gain,
    parents,
    lengths,
    accepted,
):
    f32 = jnp.float32
    bf16 = jnp.bfloat16
    tokens_wide = tokens.astype(f32)
    gained = (tokens_wide * norm_gain).astype(bf16)
    partial_value = jnp.concatenate(
        [
            jnp.dot(gained, weight_part, preferred_element_type=f32)
            for weight_part in (w_query, w_key, w_value)
        ],
        axis=1,
    )
    squares = jnp.sum(tokens_wide * tokens_wide, axis=1)
    total_squares = over_axes(squares, KV)
    norm_factor = lax.rsqrt(total_squares / D + epsilon)
    share = sum_at_owner(partial_value, KV, 1)
    projected = gathered_copies((share * norm_factor[:, None]).astype(bf16), KV, 1)
    width = w_query.shape[1]
    local_heads = width // HEAD
    queries = projected[:, :width].reshape(SEQS, PROP, local_heads, 2, QK)
    keys_flat = projected[:, width : 2 * width].reshape(SEQS, PROP, width)
    values_flat = projected[:, 2 * width :].reshape(SEQS, PROP, width)
    keys_new = keys_flat.reshape(SEQS, PROP, local_heads, 2, QK)
    values_new = values_flat.reshape(SEQS, PROP, local_heads, HEAD)
    start = lengths + accepted
    score_scale = QK ** (-0.5)
    block_len = cache_keys.shape[1]
    offset = lax.axis_index(KV) * block_len
    positions = offset + jnp.arange(block_len, dtype=jnp.int32)
    visible = (positions[None, :] < start[:, None])[:, None, None, None, :]
    block_keys = cache_keys.reshape(SEQS, block_len, local_heads, 2, QK)
    block_vals = cache_values.reshape(SEQS, block_len, local_heads, HEAD)
    scores = (
        jnp.einsum("bqhmd,bkhmd->bmhqk", queries, block_keys, preferred_element_type=f32)
        * score_scale
    )
    block_max = jnp.max(jnp.where(visible, scores, masked_low), axis=-1)
    block_weight = jnp.where(visible, jnp.exp(scores - block_max[..., None]), 0.0)
    block_total = jnp.sum(block_weight, axis=-1)
    block_values = jnp.einsum(
        "bmhqk,bkhd->bmqhd", block_weight.astype(bf16), block_vals, preferred_element_type=f32
    )
    block_values = block_values.reshape(SEQS, 2, PROP, width).astype(bf16)
    cache_max, cache_total, cache_sum = combined_all(
        (block_max, block_total, block_values), KV, combine_blocks
    )
    lineage = ancestry(parents)[:, None, None, :, :]
    self_scores = (
        jnp.einsum("bqhmd,bjhmd->bmhqj", queries, keys_new, preferred_element_type=f32)
        * score_scale
    )
    self_max = jnp.max(jnp.where(lineage, self_scores, masked_low), axis=-1)
    top = jnp.maximum(cache_max, self_max)
    self_weight = jnp.where(lineage, jnp.exp(self_scores - top[..., None]), 0.0)
    carried = jnp.exp(cache_max - top)
    denominator = cache_total * carried + jnp.sum(self_weight, axis=-1)
    self_values = jnp.einsum(
        "bmhqj,bjhd->bmqhd", self_weight.astype(bf16), values_new, preferred_element_type=f32
    )
    attended = (scaled_values(cache_sum, carried, local_heads) + self_values) / jnp.transpose(
        denominator, (0, 1, 3, 2)
    )[..., None]
    difference = attended[:, 0] - map_lambda[None, None, :, None] * attended[:, 1]
    gains = out_gain.reshape(local_heads, HEAD)[None, None]
    normed = (
        difference
        * lax.rsqrt(jnp.mean(difference * difference, axis=-1, keepdims=True) + epsilon)
        * gains
    )
    normed = normed.astype(bf16).reshape(SEQS * PROP, width)
    partial_out = jnp.dot(normed, w_output, preferred_element_type=f32).astype(bf16)
    partial_out = lax.optimization_barrier(partial_out).astype(f32)
    mixed = over_copies(partial_out.astype(jnp.bfloat16), "tp").astype(jnp.float32).astype(bf16)
    relative = positions[None, :] - start[:, None]
    slots = jnp.arange(PROP, dtype=jnp.int32)
    placing = (relative[:, :, None] == slots[None, None, :]).astype(bf16)
    written = ((relative >= 0) & (relative < PROP))[:, :, None]
    moved_keys = jnp.einsum("bkj,bjf->bkf", placing, keys_flat, preferred_element_type=f32).astype(
        bf16
    )
    moved_values = jnp.einsum(
        "bkj,bjf->bkf", placing, values_flat, preferred_element_type=f32
    ).astype(bf16)
    new_keys = jnp.where(written, moved_keys, cache_keys)
    new_values = jnp.where(written, moved_values, cache_values)
    return (mixed, new_keys, new_values)


def solution(mesh):
    torus = Mesh(mesh.devices.reshape(4, 4, mesh.shape["tp"]), ("kv_0", "kv_1", "tp"))
    return jax.shard_map(
        local,
        mesh=torus,
        in_specs=(
            P(None, KV),
            P(KV),
            P(KV, "tp"),
            P(KV, "tp"),
            P(KV, "tp"),
            P("tp", KV),
            P(None, KV, "tp"),
            P(None, KV, "tp"),
            P("tp"),
            P("tp"),
            P(),
            P(),
            P(),
        ),
        out_specs=(P(None, KV), P(None, KV, "tp"), P(None, KV, "tp")),
        check_vma=False,
    )
```

profile of v0, /device:TPU:1, one launch (start us, length us, event | category | flops | bytes accessed | tf_op | source)
XLA Modules:
  0.0 160.8 jit_solution(7291358375823799381)
XLA Ops:
  6.4 8.4 %all-to-all-start = ((f32[16,96,96]{2,1,0:T(8,128)}), f32[16,96,96]{2,1,0:T(8,128)S(1)}, u32[]{:S(2)}, u32[]{:S(2)}) async-start(f32[16,96,96]{2,1,0:T(8,128)} %bitcast.118), calls=%async_computation | async-start | bytes 1572864 | tf_op jit(solution)/shard_map/all_to_all | solution.py:33
  14.8 5.8 %while.11 = (s32[]{:T(128)}, f32[4,24,24]{2,1,0:T(8,128)S(1)}, s32[4,24]{1,0:T(4,128)S(1)}, s32[]{:T(128)}) while((s32[]{:T(128)}, f32[4,24,24]{2,1,0:T(8,128)S(1)}, s32[4,24]{1,0:T(4,128)S(1)}, s32[]{:T(128)}) %tuple.46), condition=%wide.region_6.7_spmd.clone, body=%wide.region_5.6_spmd.clone.sunk | while | flops 120962 | bytes 41909 | solution.py:85
  20.7 9.4 %psum.14 = f32[96]{0:T(128)S(1)} all-reduce(f32[96]{0:T(128)S(1)} %fusion.38), channel_id=1, replica_groups=mesh['kv_0'=4,'kv_1'=4,'tp'=8] {'kv_0'}, use_global_device_ids=true, to_apply=%region_2.0 | all-reduce | flops 96 | bytes 768 | tf_op jit(solution)/shard_map/psum | solution.py:22
  30.1 7.7 %psum.15 = f32[96]{0:T(128)S(1)} all-reduce(f32[96]{0:T(128)S(1)} %psum.14), channel_id=1, replica_groups=mesh['kv_0'=4,'kv_1'=4,'tp'=8] {'kv_1'}, use_global_device_ids=true, to_apply=%region_3.0 | all-reduce | flops 96 | bytes 768 | tf_op jit(solution)/shard_map/psum | solution.py:22
  38.8 3.6 %all-to-all-start.1 = ((bf16[16,96,96]{2,1,0:T(8,128)(2,1)}), bf16[16,96,96]{2,1,0:T(8,128)(2,1)S(1)}, u32[]{:S(2)}, u32[]{:S(2)}) async-start(bf16[16,96,96]{2,1,0:T(8,128)(2,1)} %broadcast_in_dim.96), calls=%async_computation.1 | async-start | bytes 786432 | tf_op jit(solution)/shard_map/all_to_all | solution.py:45
  42.4 2.8 %copy.114 = bf16[4,512,512]{1,2,0:T(8,128)(2,1)S(1)} copy(bf16[4,512,512]{2,1,0:T(8,128)(2,1)} %param.21) | data formatting | bytes 4194304 | tf_op args[6]
  45.3 5.3 %all-to-all-done.1 = bf16[16,96,96]{2,1,0:T(8,128)(2,1)S(1)} async-done(((bf16[16,96,96]{2,1,0:T(8,128)(2,1)}), bf16[16,96,96]{2,1,0:T(8,128)(2,1)S(1)}, u32[]{:S(2)}, u32[]{:S(2)}) %all-to-all-start.1) | async-done | bytes 294944 | tf_op jit(solution)/shard_map/all_to_all | solution.py:45
  52.3 2.2 %fusion.67 = (bf16[4,2,8,24,512]{4,3,2,1,0:T(8,128)(2,1)}, bf16[4,2,8,24]{3,2,1,0:T(8,128)(2,1)S(1)}) fusion(f32[4,2,8,24,512]{4,3,2,1,0:T(8,128)S(1)} %get-tuple-element.73, pred[4,512]{1,0:T(4,128)(4,1)S(1)} %get-tuple-element.68), kind=kOutput, calls=%fused_computation.111 | output fusion | flops 5505535 | bytes 4723712 | tf_op jit(solution)/shard_map/sub | solution.py:160
  55.6 3.5 %all-to-all-start.4 = ((bf16[16,2,768]{2,1,0:T(2,128)(2,1)}), bf16[16,2,768]{2,1,0:T(2,128)(2,1)S(1)}, u32[]{:S(2)}, u32[]{:S(2)}) async-start(bf16[16,2,768]{2,1,0:T(2,128)(2,1)} %reshape.218), calls=%async_computation.4 | async-start | bytes 98304 | tf_op jit(solution)/shard_map/all_to_all | solution.py:45
  59.1 2.4 %copy.117 = bf16[4,512,512]{1,2,0:T(8,128)(2,1)} copy(bf16[4,512,512]{2,1,0:T(8,128)(2,1)S(1)} %copy-done.3) | data formatting | bytes 4194304 | tf_op args[7]
  62.5 3.0 %all-to-all-done.4 = bf16[16,2,768]{2,1,0:T(2,128)(2,1)S(1)} async-done(((bf16[16,2,768]{2,1,0:T(2,128)(2,1)}), bf16[16,2,768]{2,1,0:T(2,128)(2,1)S(1)}, u32[]{:S(2)}, u32[]{:S(2)}) %all-to-all-start.4) | async-done | bytes 49184 | tf_op jit(solution)/shard_map/all_to_all | solution.py:45
  65.5 3.6 %all-to-all-start.3 = ((bf16[16,2,768]{2,1,0:T(2,128)(2,1)}), bf16[16,2,768]{2,1,0:T(2,128)(2,1)S(1)}, u32[]{:S(2)}, u32[]{:S(2)}) async-start(bf16[16,2,768]{2,1,0:T(2,128)(2,1)} %reshape.216), calls=%async_computation.3 | async-start | bytes 98304 | tf_op jit(solution)/shard_map/all_to_all | solution.py:45
  69.1 2.8 %fusion.24 = bf16[4,2,24,8,64]{4,2,1,3,0:T(8,128)(2,1)S(1)} fusion(bf16[4,512,8,64,1]{1,3,4,2,0:T(8,128)(2,1)} %bitcast.124, bf16[4,2,8,24,512]{4,3,2,1,0:T(8,128)(2,1)} %get-tuple-element.50), kind=kOutput, calls=%fused_computation.30 | convolution fusion | flops 100761600 | bytes 3866624 | tf_op jit(solution)/shard_map/bmhqk,bkhd->bmqhd/dot_general | solution.py:162
  72.3 3.3 %all-to-all-done.3 = bf16[16,2,768]{2,1,0:T(2,128)(2,1)S(1)} async-done(((bf16[16,2,768]{2,1,0:T(2,128)(2,1)}), bf16[16,2,768]{2,1,0:T(2,128)(2,1)S(1)}, u32[]{:S(2)}, u32[]{:S(2)}) %all-to-all-start.3) | async-done | bytes 49184 | tf_op jit(solution)/shard_map/all_to_all | solution.py:45
  77.6 4.8 %all-to-all-start.2 = ((bf16[16,4,2,24,512]{4,3,2,1,0:T(8,128)(2,1)}), bf16[16,4,2,24,512]{4,3,2,1,0:T(8,128)(2,1)}, u32[]{:S(2)}, u32[]{:S(2)}) async-start(bf16[16,4,2,24,512]{4,3,2,1,0:T(8,128)(2,1)} %broadcast_in_dim.99), calls=%async_computation.2 | async-start | bytes 6291456 | tf_op jit(solution)/shard_map/all_to_all | solution.py:45
  87.9 3.8 %mul.219 = f32[8,4,2,24,8,64]{5,4,3,2,1,0:T(8,128)} broadcast(f32[8,4,2,24,8]{4,3,2,1,0:T(8,128)S(1)} %copy.120), dimensions={0,1,2,3,4} | broadcast | bytes 3194880 | tf_op jit(solution)/shard_map/vmap()/mul | solution.py:91
  91.8 6.3 %mul.220 = f32[8,4,2,24,512]{4,3,2,1,0:T(8,128)} reshape(f32[8,4,2,24,8,64]{5,4,3,2,1,0:T(8,128)} %mul.219) | data formatting | bytes 6291456 | tf_op jit(solution)/shard_map/vmap()/mul | solution.py:91
  98.3 3.8 %mul.222 = f32[8,4,2,24,8,64]{5,4,3,2,1,0:T(8,128)} broadcast(f32[8,4,2,24,8]{4,3,2,1,0:T(8,128)S(1)} %copy.121), dimensions={0,1,2,3,4} | broadcast | bytes 3194880 | tf_op jit(solution)/shard_map/vmap()/mul | solution.py:91
  102.1 6.2 %mul.223 = f32[8,4,2,24,512]{4,3,2,1,0:T(8,128)} reshape(f32[8,4,2,24,8,64]{5,4,3,2,1,0:T(8,128)} %mul.222) | data formatting | bytes 6291456 | tf_op jit(solution)/shard_map/vmap()/mul | solution.py:91
  123.1 2.2 %mul.239 = f32[1,4,2,24,512]{4,3,2,1,0:T(8,128)} reshape(f32[4,2,24,8,64]{4,3,2,1,0:T(8,128)} %mul.238) | data formatting | bytes 786432 | tf_op jit(solution)/shard_map/vmap()/mul | solution.py:91
  126.6 2.1 %mul.243 = f32[1,4,2,24,512]{4,3,2,1,0:T(8,128)} reshape(f32[4,2,24,8,64]{4,3,2,1,0:T(8,128)} %mul.242) | data formatting | bytes 786432 | tf_op jit(solution)/shard_map/vmap()/mul | solution.py:91
  128.7 4.1 %add_convert_fusion = bf16[8,4,2,24,512]{4,3,2,1,0:T(8,128)(2,1)S(1)} fusion(f32[8,4,2,24,512]{4,3,2,1,0:T(8,128)} %mul.223, f32[8,4,2,24,512]{4,3,2,1,0:T(8,128)S(1)} %copy-done.2, bf16[16,4,2,24,512]{4,3,2,1,0:T(8,128)(2,1)} %all-to-all-done.2), kind=kLoop, calls=%fused_computation.10 | loop fusion | flops 4718592 | bytes 11010048 | tf_op jit(solution)/shard_map/vmap()/convert_element_type | solution.py:105
  139.6 12.8 %all-to-all-start.5 = ((bf16[8,96,256]{2,1,0:T(8,128)(2,1)}), bf16[8,96,256]{2,1,0:T(8,128)(2,1)S(1)}, u32[]{:S(2)}, u32[]{:S(2)}) async-start(bf16[8,96,256]{2,1,0:T(8,128)(2,1)} %broadcast_in_dim.106), calls=%async_computation.5 | async-start | bytes 786432 | tf_op jit(solution)/shard_map/all_to_all | solution.py:45
  156.4 3.7 %all-to-all-done.5 = bf16[8,96,256]{2,1,0:T(8,128)(2,1)S(1)} async-done(((bf16[8,96,256]{2,1,0:T(8,128)(2,1)}), bf16[8,96,256]{2,1,0:T(8,128)(2,1)S(1)}, u32[]{:S(2)}, u32[]{:S(2)}) %all-to-all-start.5) | async-done | bytes 393248 | tf_op jit(solution)/shard_map/all_to_all | solution.py:45
  (229 shorter events, 51.2 us)
Async XLA Ops:
  5.0 9.9 %copy-start.25 = (s32[4,24]{1,0:T(4,128)S(1)}, s32[4,24]{1,0:T(4,128)}, u32[]{:S(2)}) copy-start(s32[4,24]{1,0:T(4,128)} %param.25) | copy-start | bytes 1156
  5.2 15.4 %copy-start.18 = (bf16[96,256]{1,0:T(8,128)(2,1)S(1)}, bf16[96,256]{1,0:T(8,128)(2,1)}, u32[]{:S(2)}) copy-start(bf16[96,256]{1,0:T(8,128)(2,1)} %param.15) | copy-start | bytes 147460
  6.4 31.5 %all-to-all-start = ((f32[16,96,96]{2,1,0:T(8,128)}), f32[16,96,96]{2,1,0:T(8,128)S(1)}, u32[]{:S(2)}, u32[]{:S(2)}) async-start(f32[16,96,96]{2,1,0:T(8,128)} %bitcast.118), calls=%async_computation | async-start | bytes 1572864 | tf_op jit(solution)/shard_map/all_to_all | solution.py:33
  38.8 11.8 %all-to-all-start.1 = ((bf16[16,96,96]{2,1,0:T(8,128)(2,1)}), bf16[16,96,96]{2,1,0:T(8,128)(2,1)S(1)}, u32[]{:S(2)}, u32[]{:S(2)}) async-start(bf16[16,96,96]{2,1,0:T(8,128)(2,1)} %broadcast_in_dim.96), calls=%async_computation.1 | async-start | bytes 786432 | tf_op jit(solution)/shard_map/all_to_all | solution.py:45
  42.4 2.8 %copy-start.30 = (s32[4]{0:T(128)S(1)}, s32[4]{0:T(128)}, u32[]{:S(2)}) copy-start(s32[4]{0:T(128)} %param.26) | copy-start | bytes 52
  42.4 2.8 %copy-start.31 = (s32[4]{0:T(128)S(1)}, s32[4]{0:T(128)}, u32[]{:S(2)}) copy-start(s32[4]{0:T(128)} %param.27) | copy-start | bytes 52
  51.2 31.6 %copy-start.16 = (bf16[96,512]{1,0:T(8,128)(2,1)}, bf16[96,512]{1,0:T(8,128)(2,1)S(1)}, u32[]{:S(2)}) copy-start(bf16[96,512]{1,0:T(8,128)(2,1)S(1)} %get-tuple-element.61) | copy-start | bytes 294916
  51.2 31.8 %copy-start.14 = (bf16[96,512]{1,0:T(8,128)(2,1)}, bf16[96,512]{1,0:T(8,128)(2,1)S(1)}, u32[]{:S(2)}) copy-start(bf16[96,512]{1,0:T(8,128)(2,1)S(1)} %get-tuple-element.60) | copy-start | bytes 294916
  52.3 6.8 %copy-start.3 = (bf16[4,512,512]{2,1,0:T(8,128)(2,1)S(1)}, bf16[4,512,512]{2,1,0:T(8,128)(2,1)}, u32[]{:S(2)}) copy-start(bf16[4,512,512]{2,1,0:T(8,128)(2,1)} %param.22) | copy-start | bytes 6291460
  55.6 9.9 %all-to-all-start.4 = ((bf16[16,2,768]{2,1,0:T(2,128)(2,1)}), bf16[16,2,768]{2,1,0:T(2,128)(2,1)S(1)}, u32[]{:S(2)}, u32[]{:S(2)}) async-start(bf16[16,2,768]{2,1,0:T(2,128)(2,1)} %reshape.218), calls=%async_computation.4 | async-start | bytes 98304 | tf_op jit(solution)/shard_map/all_to_all | solution.py:45
  65.5 10.1 %all-to-all-start.3 = ((bf16[16,2,768]{2,1,0:T(2,128)(2,1)}), bf16[16,2,768]{2,1,0:T(2,128)(2,1)S(1)}, u32[]{:S(2)}, u32[]{:S(2)}) async-start(bf16[16,2,768]{2,1,0:T(2,128)(2,1)} %reshape.216), calls=%async_computation.3 | async-start | bytes 98304 | tf_op jit(solution)/shard_map/all_to_all | solution.py:45
  77.6 5.0 %copy-start.28 = (f32[8]{0:T(128)S(1)}, f32[8]{0:T(128)}, u32[]{:S(2)}) copy-start(f32[8]{0:T(128)} %param.23) | copy-start | bytes 100
  77.6 51.1 %all-to-all-start.2 = ((bf16[16,4,2,24,512]{4,3,2,1,0:T(8,128)(2,1)}), bf16[16,4,2,24,512]{4,3,2,1,0:T(8,128)(2,1)}, u32[]{:S(2)}, u32[]{:S(2)}) async-start(bf16[16,4,2,24,512]{4,3,2,1,0:T(8,128)(2,1)} %broadcast_in_dim.99), calls=%async_computation.2 | async-start | bytes 6291456 | tf_op jit(solution)/shard_map/all_to_all | solution.py:45
  85.3 2.4 %copy-start.10 = (f32[2,4,2,8,24]{4,3,2,1,0:T(8,128)}, f32[2,4,2,8,24]{4,3,2,1,0:T(8,128)S(1)}, u32[]{:S(2)}) copy-start(f32[2,4,2,8,24]{4,3,2,1,0:T(8,128)S(1)} %get-tuple-element.45) | copy-start | bytes 36868
  85.9 5.8 %copy-start.20 = (f32[1,4,2,8,24]{4,3,2,1,0:T(8,128)}, f32[1,4,2,8,24]{4,3,2,1,0:T(8,128)S(1)}, u32[]{:S(2)}) copy-start(f32[1,4,2,8,24]{4,3,2,1,0:T(8,128)S(1)} %get-tuple-element.43) | copy-start | bytes 18436
  121.9 6.7 %copy-start.24 = (f32[4,2,24,8]{2,3,1,0:T(8,128)S(1)}, f32[4,2,24,8]{2,3,1,0:T(8,128)}, u32[]{:S(2)}) copy-start(f32[4,2,24,8]{2,3,1,0:T(8,128)} %get-tuple-element.42) | copy-start | bytes 18436
  122.0 6.7 %copy-start.2 = (f32[8,4,2,24,512]{4,3,2,1,0:T(8,128)S(1)}, f32[8,4,2,24,512]{4,3,2,1,0:T(8,128)}, u32[]{:S(2)}) copy-start(f32[8,4,2,24,512]{4,3,2,1,0:T(8,128)} %mul.220) | copy-start | bytes 9437188
  128.7 4.1 %copy-start.6 = (f32[4,4,2,24,512]{4,3,2,1,0:T(8,128)S(1)}, f32[4,4,2,24,512]{4,3,2,1,0:T(8,128)}, u32[]{:S(2)}) copy-start(f32[4,4,2,24,512]{4,3,2,1,0:T(8,128)} %mul.226) | copy-start | bytes 4718596
  128.7 4.1 %copy-start.7 = (f32[4,4,2,24,512]{4,3,2,1,0:T(8,128)S(1)}, f32[4,4,2,24,512]{4,3,2,1,0:T(8,128)}, u32[]{:S(2)}) copy-start(f32[4,4,2,24,512]{4,3,2,1,0:T(8,128)} %mul.229) | copy-start | bytes 4718596
  137.1 15.3 %copy-start.4 = (bf16[4,512,512]{2,1,0:T(8,128)(2,1)S(1)}, bf16[4,512,512]{2,1,0:T(8,128)(2,1)}, u32[]{:S(2)}) copy-start(bf16[4,512,512]{2,1,0:T(8,128)(2,1)} %param.22) | copy-start | bytes 6291460
  137.1 15.3 %copy-start.15 = (bf16[96,512]{1,0:T(8,128)(2,1)S(1)}, bf16[96,512]{1,0:T(8,128)(2,1)}, u32[]{:S(2)}) copy-start(bf16[96,512]{1,0:T(8,128)(2,1)} %copy-done.14) | copy-start | bytes 294916
  139.6 20.5 %all-to-all-start.5 = ((bf16[8,96,256]{2,1,0:T(8,128)(2,1)}), bf16[8,96,256]{2,1,0:T(8,128)(2,1)S(1)}, u32[]{:S(2)}, u32[]{:S(2)}) async-start(bf16[8,96,256]{2,1,0:T(8,128)(2,1)} %broadcast_in_dim.106), calls=%async_computation.5 | async-start | bytes 786432 | tf_op jit(solution)/shard_map/all_to_all | solution.py:45
  152.4 2.0 %copy-start.5 = (bf16[4,512,512]{2,1,0:T(8,128)(2,1)S(1)}, bf16[4,512,512]{2,1,0:T(8,128)(2,1)}, u32[]{:S(2)}) copy-start(bf16[4,512,512]{2,1,0:T(8,128)(2,1)} %param.21) | copy-start | bytes 6291460
  154.4 6.4 %copy-start.1 = (bf16[256,512]{1,0:T(8,128)(2,1)S(1)}, bf16[256,512]{1,0:T(8,128)(2,1)}, u32[]{:S(2)}) copy-start(bf16[256,512]{1,0:T(8,128)(2,1)} %param.19) | copy-start | bytes 786436
  (14 other events, 18.6 us)
where the time goes:
time: 162 us; the launch traced here: 161 us
  local copies, waits for them, and re-layouts  60 us (37%)
  starting transfers between devices  36.6 us (23%)
  matrix products  18.4 us (11%)
  blocking collectives  17.2 us (11%)
  waiting for transfers between devices  15.2 us (9%)
  other arithmetic  11.5 us (7%)
    mul x18, local copies, waits for them, and re-layouts, scaled_values(): return shaped * jnp.transpose(factor, (0, 1, 3, 2))[..., None]  37.5 us
    all_to_all x5, starting transfers between devices, copy_for_each(): return lax.all_to_all(copies, axis, split_axis=0, concat_axis=0, tiled=True)  28.2 us
    psum x2, blocking collectives, over_axes(): return functools.reduce(lax.psum, axes, array)  17.2 us
    all_to_all x5, waiting for transfers between devices, copy_for_each(): return lax.all_to_all(copies, axis, split_axis=0, concat_axis=0, tiled=True)  15.2 us
    unnamed x70, local copies, waits for them, and re-layouts  10.6 us
    all_to_all x1, starting transfers between devices, sum_at_owner(): lax.all_to_all(blocks, axis, split_axis=0, concat_axis=0, tiled=True)  8.42 us
    dot_general x24, matrix products, extend(): jnp.einsum('bji,bik->bjk', parent_links, reached)  4.94 us
    convert_element_type x3, other arithmetic, combine_blocks(): merged = merged.reshape(values_first.shape).astype(jnp.bfloat16)  4.84 us
  transfers between devices with their start and end apart: 6, of which 4 were waited for; matrix products, arithmetic and copies ran while one was open for 40% of the time, Pallas kernels for 0%

commit v1 on v0

v1 whole, which is shorter than its diff:
```python
import functools

import jax
import jax.numpy as jnp
from jax import lax
from jax.experimental import pallas as pl
from jax.experimental.pallas import tpu as pltpu
from jax.sharding import PartitionSpec as P

D = 4096
HEAD = 64
QK = 32
SEQS = 4
PROP = 24
KV = 16
TP = 8
BLOCK = 128
PAD = 32
POS = 512
ROWS = 96
EPS = 1e-05
LOW = -1e30
LOG2E = 1.4426950408889634
SCALE2 = QK ** (-0.5) * LOG2E
F32 = jnp.float32
BF16 = jnp.bfloat16
NT = (((1,), (1,)), ((), ()))


def _distance(step):
    ring = (0, 1, 2, 1)
    return ring[step >> 2] + ring[step & 3]


PARTNERS = sorted(range(1, KV), key=lambda step: -_distance(step))


def _dot(a, b):
    return jnp.dot(a, b, preferred_element_type=F32)


def _dot_nt(a, b):
    return lax.dot_general(a, b, NT, preferred_element_type=F32)


def _lane_head_map(rows):
    lane = lax.broadcasted_iota(jnp.int32, (rows, BLOCK), 1)
    return lane


def _expanded(chunk):
    lane = lax.broadcasted_iota(jnp.int32, (PROP, BLOCK), 1)
    parts = []
    for which in range(2):
        for head in range(2):
            low = head * HEAD + which * QK
            inside = (lane >= low) & (lane < low + QK)
            parts.append(jnp.where(inside, chunk, 0.0))
    parts.append(jnp.zeros((BLOCK - 4 * PROP, BLOCK), F32))
    return jnp.concatenate(parts, axis=0).astype(BF16)


def _main_kernel(
    tok_hbm,
    gain_ref,
    wq_hbm,
    wk_hbm,
    wv_hbm,
    wo_hbm,
    ck_hbm,
    cv_hbm,
    lam_ref,
    og_ref,
    par_ref,
    len_ref,
    acc_ref,
    mixed_ref,
    kvn_ref,
    tok,
    wqkv,
    wo,
    kbuf,
    vbuf,
    vt,
    pq,
    rq,
    pkv,
    rkv,
    qg,
    kvg,
    dv,
    rdv,
    ds,
    rds,
    ng,
    part,
    rpart,
    par_pad,
    qe,
    load_sem,
    q_send,
    q_recv,
    kv_send,
    kv_recv,
    qg_send,
    qg_recv,
    kvg_send,
    kvg_recv,
    dv_send,
    dv_recv,
    ds_send,
    ds_recv,
    ng_send,
    ng_recv,
    mx_send,
    mx_recv,
):
    me = lax.axis_index("kv")
    tp = lax.axis_index("tp")
    z = me // 4
    x = lax.rem(me, 4)

    loads = {}

    def load(name, src, dst, index):
        copy = pltpu.make_async_copy(src, dst, load_sem.at[index])
        copy.start()
        loads[name] = copy

    load("tok", tok_hbm, tok, 0)
    load("wq", wq_hbm, wqkv.at[0], 1)
    load("wk", wk_hbm, wqkv.at[1], 2)
    load("wv", wv_hbm, wqkv.at[2], 3)
    for b in range(SEQS):
        load(("v", b), cv_hbm.at[b], vbuf.at[b], 4 + b)
    for b in range(SEQS):
        load(("k", b), ck_hbm.at[b], kbuf.at[b], 8 + b)
    load("wo", wo_hbm, wo, 12)

    barrier = pltpu.get_barrier_semaphore()
    for step in PARTNERS:
        pl.semaphore_signal(barrier, inc=1, device_id={"kv": me ^ step}, device_id_type=pl.DeviceIdType.MESH)
    for step in range(1, TP):
        pl.semaphore_signal(barrier, inc=1, device_id={"tp": tp ^ step}, device_id_type=pl.DeviceIdType.MESH)

    def to_kv(step, src, dst, send, recv):
        return pltpu.make_async_remote_copy(
            src_ref=src,
            dst_ref=dst,
            send_sem=send.at[step],
            recv_sem=recv.at[step],
            device_id={"kv": me ^ step},
            device_id_type=pl.DeviceIdType.MESH,
        )

    def q_copy(step):
        return to_kv(step, pq.at[me ^ step], rq.at[step], q_send, q_recv)

    def kv_copy(step):
        return to_kv(step, pkv.at[me ^ step], rkv.at[step], kv_send, kv_recv)

    def qg_copy(step):
        return to_kv(step, qg.at[me], qg.at[me], qg_send, qg_recv)

    def kvg_copy(step):
        return to_kv(step, kvg.at[me], kvg.at[me], kvg_send, kvg_recv)

    def dv_copy(step):
        return to_kv(step, dv.at[me ^ step], rdv.at[step], dv_send, dv_recv)

    def ds_copy(step):
        return to_kv(step, ds.at[me ^ step], rds.at[step], ds_send, ds_recv)

    def ng_slot():
        return ng.at[x, pl.ds(pl.multiple_of(z * PAD, PAD), PAD), :]

    def ng_copy(step):
        return to_kv(step, ng_slot(), ng_slot(), ng_send, ng_recv)

    def mx_copy(step):
        return pltpu.make_async_remote_copy(
            src_ref=part,
            dst_ref=rpart.at[step],
            send_sem=mx_send.at[step],
            recv_sem=mx_recv.at[step],
            device_id={"tp": tp ^ step},
            device_id_type=pl.DeviceIdType.MESH,
        )

    loads["tok"].wait()
    wide = tok[...].astype(F32)
    gained = (wide * gain_ref[...]).astype(BF16)
    square = jnp.sum(wide * wide, axis=1, keepdims=True)
    eye = lax.broadcasted_iota(jnp.int32, (PROP, BLOCK), 0) == lax.broadcasted_iota(jnp.int32, (PROP, BLOCK), 1)
    loads["wq"].wait()
    partial_q = _dot(gained, wqkv[0])
    for b in range(SEQS):
        column = square[b * PROP : (b + 1) * PROP]
        row = jnp.sum(jnp.where(eye, column, 0.0), axis=0, keepdims=True)
        tail = jnp.broadcast_to(row, (PAD - PROP, BLOCK))
        for block in range(4):
            pq[b * 4 + block, 0:PROP] = partial_q[b * PROP : (b + 1) * PROP, block * BLOCK : (block + 1) * BLOCK]
            pq[b * 4 + block, PROP:PAD] = tail
    pl.semaphore_wait(barrier, KV - 1 + TP - 1)
    for step in PARTNERS:
        q_copy(step).start()
    for which in range(2):
        loads["wk" if which == 0 else "wv"].wait()
        partial_kv = _dot(gained, wqkv[1 + which])
        for b in range(SEQS):
            for block in range(4):
                pkv[b * 4 + block, which] = partial_kv[
                    b * PROP : (b + 1) * PROP, block * BLOCK : (block + 1) * BLOCK
                ]
    for step in PARTNERS:
        kv_copy(step).start()

    def transpose_values(b):
        loads[("v", b)].wait()
        for block in range(4):
            vt[b, block * BLOCK : (block + 1) * BLOCK, :] = jnp.transpose(
                vbuf[b, :, block * BLOCK : (block + 1) * BLOCK]
            )

    transpose_values(0)
    transpose_values(1)

    for step in PARTNERS:
        q_copy(step).wait_recv()
    total = pq[me]
    for step in range(1, KV):
        total = total + rq[step]
    square_row = total[PROP : PROP + 1]
    square_column = jnp.sum(jnp.where(eye, square_row, 0.0), axis=1, keepdims=True)
    factor = lax.rsqrt(square_column / D + EPS)
    own_q = total[0:PROP] * factor
    zero_tail = jnp.zeros((PAD - PROP, BLOCK), F32)
    qg[me] = jnp.concatenate([own_q, zero_tail], axis=0).astype(BF16)
    for step in PARTNERS:
        qg_copy(step).start()

    for step in PARTNERS:
        kv_copy(step).wait_recv()
    for which in range(2):
        summed = pkv[me, which]
        for step in range(1, KV):
            summed = summed + rkv[step, which]
        kvg[me, which] = jnp.concatenate([summed * factor, zero_tail], axis=0).astype(BF16)
    for step in PARTNERS:
        kvg_copy(step).start()

    transpose_values(2)
    transpose_values(3)
    for b in range(SEQS):
        loads[("k", b)].wait()

    lane = lax.broadcasted_iota(jnp.int32, (HEAD, BLOCK), 1)
    second_head = ((lane >= PROP) & (lane < 2 * PROP)) | (lane >= 3 * PROP)
    for step in PARTNERS:
        qg_copy(step).wait_recv()
    for z_step in (2, 1, 3, 0):
        b = z ^ z_step
        begin = len_ref[b] + acc_ref[b] - me * POS
        position = lax.broadcasted_iota(jnp.int32, (POS, 2 * BLOCK), 0)
        visible = position < begin
        for half in range(2):
            for side in range(2):
                chunk = qg[b * 4 + half * 2 + side, 0:PAD].astype(F32)[0:PROP]
                qe[side * BLOCK : (side + 1) * BLOCK, side * BLOCK : (side + 1) * BLOCK] = _expanded(chunk)
                qe[side * BLOCK : (side + 1) * BLOCK, (1 - side) * BLOCK : (2 - side) * BLOCK] = jnp.zeros(
                    (BLOCK, BLOCK), BF16
                )
            keys = kbuf[b, :, half * 2 * BLOCK : (half + 1) * 2 * BLOCK]
            scores = _dot_nt(keys, qe[...]) * SCALE2
            scores = jnp.where(visible, scores, LOW)
            largest = jnp.max(scores, axis=0, keepdims=True)
            weight = jnp.exp2(scores - largest)
            weight_sum = jnp.sum(weight, axis=0, keepdims=True)
            weight = weight.astype(BF16)
            for side in range(2):
                block = half * 2 + side
                lanes = slice(side * BLOCK, (side + 1) * BLOCK)
                out = _dot(vt[b, block * BLOCK : (block + 1) * BLOCK, :], weight[:, lanes])
                owner = b * 4 + block
                dv[owner] = jnp.where(second_head, out[HEAD:], out[:HEAD]).astype(BF16)
                ds[owner, 0:1] = largest[:, lanes]
                ds[owner, 1:2] = weight_sum[:, lanes]
                ds[owner, 2:8] = jnp.zeros((6, BLOCK), F32)

                def send(block=block):
                    step = (z_step << 2) | (x ^ block)
                    dv_copy(step).start()
                    ds_copy(step).start()

                if z_step == 0:
                    pl.when(x != block)(send)
                else:
                    send()

    par_pad[...] = jnp.full((8, BLOCK), -1, jnp.int32)
    par_pad[0:SEQS, 0:PROP] = par_ref[...]
    parent_row = par_pad[pl.ds(z, 1), :]
    row_index = lax.broadcasted_iota(jnp.int32, (BLOCK, BLOCK), 0)
    lane_index = lax.broadcasted_iota(jnp.int32, (BLOCK, BLOCK), 1)
    reach = ((parent_row == row_index) & (lane_index < PROP)) | (row_index == lane_index)
    reach = jnp.where(reach, 1.0, 0.0).astype(BF16)
    for _ in range(5):
        reach = jnp.minimum(_dot(reach, reach), 1.0).astype(BF16)
    spread = (lax.rem(lane_index, PROP) == row_index) & (lane_index < 4 * PROP) & (row_index < PROP)
    lineage = _dot(reach, jnp.where(spread, 1.0, 0.0).astype(BF16))[0:PAD]
    linked = (lineage > 0.5) & (lax.broadcasted_iota(jnp.int32, (PAD, BLOCK), 0) < PROP)
    own_expanded = _expanded(qg[me].astype(F32)[0:PROP])
    self_scores = _dot_nt(kvg[me, 0], own_expanded) * SCALE2
    self_scores = jnp.where(linked, self_scores, LOW)
    self_max = jnp.max(self_scores, axis=0, keepdims=True)
    self_weight = jnp.where(linked, jnp.exp2(self_scores - self_max), 0.0)
    self_total = jnp.sum(self_weight, axis=0, keepdims=True)
    values_t = jnp.transpose(kvg[me, 1].astype(F32)).astype(BF16)
    self_out = _dot(values_t, self_weight.astype(BF16))
    self_sum = jnp.where(second_head, self_out[HEAD:], self_out[:HEAD])

    for step in PARTNERS:
        ds_copy(step).wait_recv()
    maxima = [ds[me, 0:1]] + [rds[step, 0:1] for step in range(1, KV)]
    totals = [ds[me, 1:2]] + [rds[step, 1:2] for step in range(1, KV)]
    top = functools.reduce(jnp.maximum, maxima, self_max)
    self_factor = jnp.exp2(self_max - top)
    denominator = self_total * self_factor
    factors = []
    for largest, weight_sum in zip(maxima, totals):
        factors.append(jnp.exp2(largest - top))
        denominator = denominator + weight_sum * factors[-1]
    for step in PARTNERS:
        dv_copy(step).wait_recv()
    merged = self_sum * self_factor + dv[me].astype(F32) * factors[0]
    for step in range(1, KV):
        merged = merged + rdv[step].astype(F32) * factors[step]
    attended = merged / denominator
    lane_row = lax.broadcasted_iota(jnp.int32, (1, BLOCK), 1)
    lam = jnp.where(lane_row < PROP, lam_ref[x * 2], lam_ref[x * 2 + 1])
    difference = attended - lam * pltpu.roll(attended, BLOCK - 2 * PROP, 1)
    power = jnp.mean(difference * difference, axis=0, keepdims=True)
    normed = difference * lax.rsqrt(power + EPS)
    stacked = jnp.concatenate([normed, pltpu.roll(normed, BLOCK - PROP, 1)], axis=0)
    turned = jnp.transpose(stacked)[0:PROP]
    turned = turned * og_ref[pl.ds(x, 1), :]
    ng[x, pl.ds(pl.multiple_of(z * PAD, PAD), PAD), :] = jnp.concatenate([turned, zero_tail], axis=0).astype(BF16)
    for step in PARTNERS:
        ng_copy(step).start()

    loads["wo"].wait()
    for step in PARTNERS:
        ng_copy(step).wait_recv()
    rows = jnp.concatenate([ng[block] for block in range(4)], axis=1)
    projected = _dot(rows, wo[...])
    projected = jnp.concatenate([projected[b * PAD : b * PAD + PROP] for b in range(SEQS)], axis=0)
    part[...] = projected.astype(BF16)
    for step in range(1, TP):
        mx_copy(step).start()
    for step in range(1, TP):
        mx_copy(step).wait_recv()
    mixed = part[...].astype(F32)
    for step in range(1, TP):
        mixed = mixed + rpart[step].astype(F32)
    mixed_ref[...] = mixed.astype(BF16)

    for step in PARTNERS:
        kvg_copy(step).wait_recv()
    kvn_ref[...] = kvg[...]
    for step in PARTNERS:
        for copy in (q_copy, kv_copy, qg_copy, kvg_copy, dv_copy, ds_copy, ng_copy):
            copy(step).wait_send()
    for step in range(1, TP):
        mx_copy(step).wait_send()


def _main(tokens, gain, w_query, w_key, w_value, w_output, cache_keys, cache_values, lam, out_gain, parents, lengths, accepted):
    hbm = pl.BlockSpec(memory_space=pl.ANY)
    vmem = pl.BlockSpec(memory_space=pltpu.VMEM)
    smem = pl.BlockSpec(memory_space=pltpu.SMEM)
    dma = pltpu.SemaphoreType.DMA
    return pl.pallas_call(
        _main_kernel,
        out_shape=(
            jax.ShapeDtypeStruct((ROWS, 256), BF16),
            jax.ShapeDtypeStruct((KV, 2, PAD, BLOCK), BF16),
        ),
        in_specs=[hbm, vmem, hbm, hbm, hbm, hbm, hbm, hbm, smem, vmem, vmem, smem, smem],
        out_specs=(vmem, vmem),
        scratch_shapes=[
            pltpu.VMEM((ROWS, 256), BF16),
            pltpu.VMEM((3, 256, 512), BF16),
            pltpu.VMEM((512, 256), BF16),
            pltpu.VMEM((SEQS, POS, 512), BF16),
            pltpu.VMEM((SEQS, POS, 512), BF16),
            pltpu.VMEM((SEQS, 512, POS), BF16),
            pltpu.VMEM((KV, PAD, BLOCK), F32),
            pltpu.VMEM((KV, PAD, BLOCK), F32),
            pltpu.VMEM((KV, 2, PROP, BLOCK), F32),
            pltpu.VMEM((KV, 2, PROP, BLOCK), F32),
            pltpu.VMEM((KV, PAD, BLOCK), BF16),
            pltpu.VMEM((KV, 2, PAD, BLOCK), BF16),
            pltpu.VMEM((KV, HEAD, BLOCK), BF16),
            pltpu.VMEM((KV, HEAD, BLOCK), BF16),
            pltpu.VMEM((KV, 8, BLOCK), F32),
            pltpu.VMEM((KV, 8, BLOCK), F32),
            pltpu.VMEM((4, SEQS * PAD, BLOCK), BF16),
            pltpu.VMEM((ROWS, 256), BF16),
            pltpu.VMEM((TP, ROWS, 256), BF16),
            pltpu.VMEM((8, BLOCK), jnp.int32),
            pltpu.VMEM((2 * BLOCK, 2 * BLOCK), BF16),
            dma((13,)),
        ]
        + [dma((KV,))] * 14
        + [dma((TP,))] * 2,
        compiler_params=pltpu.CompilerParams(
            collective_id=0, has_side_effects=True, vmem_limit_bytes=48 * 1024 * 1024
        ),
        name="attention",
    )(tokens, gain, w_query, w_key, w_value, w_output, cache_keys, cache_values, lam, out_gain, parents, lengths, accepted)


def _cache_kernel(ck_hbm, cv_hbm, kvn_ref, len_ref, acc_ref, nk_hbm, nv_hbm, kbuf, vbuf, in_sem, out_sem):
    me = lax.axis_index("kv")
    pairs = ((ck_hbm, nk_hbm, kbuf), (cv_hbm, nv_hbm, vbuf))

    def fetch(which, b):
        src, _, buf = pairs[which]
        return pltpu.make_async_copy(src.at[b], buf.at[b], in_sem.at[which, b])

    def put(which, b):
        _, dst, buf = pairs[which]
        return pltpu.make_async_copy(buf.at[b], dst.at[b], out_sem.at[which, b])

    for b in range(SEQS):
        for which in range(2):
            fetch(which, b).start()
    for b in range(SEQS):
        begin = len_ref[b] + acc_ref[b] - me * POS
        window = jnp.clip((begin + 8 * PAD) // 16 * 16 - 8 * PAD, 0, POS - 48)
        window = pl.multiple_of(window, 16)
        offset = lax.broadcasted_iota(jnp.int32, (48, PAD), 0) + window - begin
        slot = lax.broadcasted_iota(jnp.int32, (48, PAD), 1)
        placing = jnp.where((offset == slot) & (slot < PROP), 1.0, 0.0).astype(BF16)
        row = lax.broadcasted_iota(jnp.int32, (48, 512), 0) + window - begin
        written = (row >= 0) & (row < PROP)
        for which in range(2):
            fresh = jnp.concatenate([kvn_ref[b * 4 + block, which] for block in range(4)], axis=1)
            moved = _dot(placing, fresh)
            fetch(which, b).wait()
            buf = pairs[which][2]
            old = buf[b, pl.ds(window, 48), :].astype(F32)
            buf[b, pl.ds(window, 48), :] = jnp.where(written, moved, old).astype(BF16)
            put(which, b).start()
    for b in range(SEQS):
        for which in range(2):
            put(which, b).wait()


def _caches(cache_keys, cache_values, fresh, lengths, accepted):
    hbm = pl.BlockSpec(memory_space=pl.ANY)
    smem = pl.BlockSpec(memory_space=pltpu.SMEM)
    return pl.pallas_call(
        _cache_kernel,
        out_shape=(
            jax.ShapeDtypeStruct(cache_keys.shape, BF16),
            jax.ShapeDtypeStruct(cache_values.shape, BF16),
        ),
        in_specs=[hbm, hbm, pl.BlockSpec(memory_space=pltpu.VMEM), smem, smem],
        out_specs=(hbm, hbm),
        scratch_shapes=[
            pltpu.VMEM((SEQS, POS, 512), BF16),
            pltpu.VMEM((SEQS, POS, 512), BF16),
            pltpu.SemaphoreType.DMA((2, SEQS)),
            pltpu.SemaphoreType.DMA((2, SEQS)),
        ],
        name="caches",
    )(cache_keys, cache_values, fresh, lengths, accepted)


def _local(
    tokens,
    norm_gain,
    w_query,
    w_key,
    w_value,
    w_output,
    cache_keys,
    cache_values,
    map_lambda,
    out_gain,
    parents,
    lengths,
    accepted,
):
    mixed, fresh = _main(
        tokens,
        norm_gain.reshape(1, 256),
        w_query,
        w_key,
        w_value,
        w_output,
        cache_keys,
        cache_values,
        map_lambda,
        out_gain.reshape(4, BLOCK),
        parents,
        lengths,
        accepted,
    )
    new_keys, new_values = _caches(cache_keys, cache_values, fresh, lengths, accepted)
    return mixed, new_keys, new_values


def solution(mesh):
    return jax.shard_map(
        _local,
        mesh=mesh,
        in_specs=(
            P(None, "kv"),
            P("kv"),
            P("kv", "tp"),
            P("kv", "tp"),
            P("kv", "tp"),
            P("tp", "kv"),
            P(None, "kv", "tp"),
            P(None, "kv", "tp"),
            P("tp"),
            P("tp"),
            P(),
            P(),
            P(),
        ),
        out_specs=(P(None, "kv"), P(None, "kv", "tp"), P(None, "kv", "tp")),
        check_vma=False,
    )
```

time: 162 us -> 63.3 us (0.39)
  Pallas kernels: 0 us -> 49 us
  local copies, waits for them, and re-layouts: 60 us -> 13.1 us
  starting transfers between devices: 36.6 us -> 0 us
  matrix products: 18.4 us -> 0 us
  blocking collectives: 17.2 us -> 0 us
  waiting for transfers between devices: 15.2 us -> 0 us
  other arithmetic: 11.5 us -> 0 us
    pallas_call x0 -> x2, Pallas kernels: none -> 49 us  [the longest x1 44.5 us: _main(): pl.pallas_call(_main_kernel, out_shape=(jax.ShapeDtypeStruct((ROWS, 256),...]
    mul x22 -> x0, local copies, waits for them, and re-layouts: 37.9 us -> none  [the longest x18 37.5 us: scaled_values(): return shaped * jnp.transpose(factor, (0, 1, 3, 2))[..., None]]
    all_to_all x6 -> x0, starting transfers between devices: 36.6 us -> none  [the longest x5 28.2 us: copy_for_each(): return lax.all_to_all(copies, axis, split_axis=0, concat_axis=0, tiled=True)]
    dot_general x34 -> x0, matrix products: 18.4 us -> none  [the longest x24 4.94 us: extend(): jnp.einsum('bji,bik->bjk', parent_links, reached)]
    psum x2 -> x0, blocking collectives: 17.2 us -> none  [over_axes(): return functools.reduce(lax.psum, axes, array)]
    all_to_all x6 -> x0, waiting for transfers between devices: 15.2 us -> none  [the longest x5 15.2 us: copy_for_each(): return lax.all_to_all(copies, axis, split_axis=0, concat_axis=0, tiled=True)]
    convert_element_type x8 -> x0, other arithmetic: 5.11 us -> none  [the longest x3 4.84 us: combine_blocks(): merged = merged.reshape(values_first.shape).astype(jnp.bfloat16)]
    broadcast_in_dim x6 -> x0, local copies, waits for them, and re-layouts: 3.71 us -> none  [the longest x5 3.71 us: copy_for_each(): copies = jnp.broadcast_to(array, (lax.axis_size(axis), *array.shape))]
  transfers between devices with their start and end apart: 6 -> 0, of which waited for: 4 -> 0; matrix products, arithmetic and copies ran while one was open for 40% -> 0% of each run, Pallas kernels for 0% -> 0%
where the time goes in v1:
time: 63.3 us; the launch traced here: 62.8 us
  Pallas kernels  49 us (77%)
  local copies, waits for them, and re-layouts  13.1 us (21%)
  between operations  0.68 us (1%)
    pallas_call x1, Pallas kernels, _main(): pl.pallas_call(_main_kernel, out_shape=(jax.ShapeDtypeStruct((ROWS, 256),...  44.5 us
    unnamed x29, local copies, waits for them, and re-layouts  13.1 us
    pallas_call x1, Pallas kernels, _caches(): pl.pallas_call(_cache_kernel, out_shape=(jax.ShapeDtypeStruct(cache_keys....  4.49 us

profile of v1, /device:TPU:1, one launch (start us, length us, event | category | flops | bytes accessed | tf_op | source)
XLA Modules:
  0.0 62.8 jit_solution(12130678108833285248)
XLA Ops:
  0.6 0.0 copy-start
  0.6 1.6 %copy-done = bf16[4,512,512]{2,1,0:T(8,128)(2,1)S(1)} copy-done((bf16[4,512,512]{2,1,0:T(8,128)(2,1)S(1)}, bf16[4,512,512]{2,1,0:T(8,128)(2,1)}, u32[]{:S(2)}) %copy-start) | copy-done | bytes 2097176
  2.2 0.0 copy-start.1
  2.2 1.6 %copy-done.1 = bf16[4,512,512]{2,1,0:T(8,128)(2,1)S(1)} copy-done((bf16[4,512,512]{2,1,0:T(8,128)(2,1)S(1)}, bf16[4,512,512]{2,1,0:T(8,128)(2,1)}, u32[]{:S(2)}) %copy-start.1) | copy-done | bytes 2097176
  3.8 0.9 %copy-done.2 = bf16[256,512]{1,0:T(8,128)(2,1)S(1)} copy-done((bf16[256,512]{1,0:T(8,128)(2,1)S(1)}, bf16[256,512]{1,0:T(8,128)(2,1)}, u32[]{:S(2)}) %copy-start.2) | copy-done | bytes 262168
  4.8 0.0 copy-start.3
  4.8 0.9 %copy-done.3 = bf16[256,512]{1,0:T(8,128)(2,1)S(1)} copy-done((bf16[256,512]{1,0:T(8,128)(2,1)S(1)}, bf16[256,512]{1,0:T(8,128)(2,1)}, u32[]{:S(2)}) %copy-start.3) | copy-done | bytes 262168
  5.7 0.0 copy-start.4
  5.7 0.9 %copy-done.4 = bf16[256,512]{1,0:T(8,128)(2,1)S(1)} copy-done((bf16[256,512]{1,0:T(8,128)(2,1)S(1)}, bf16[256,512]{1,0:T(8,128)(2,1)}, u32[]{:S(2)}) %copy-start.4) | copy-done | bytes 262168
  6.7 0.0 copy-start.5
  6.7 0.9 %copy-done.5 = bf16[512,256]{1,0:T(8,128)(2,1)S(1)} copy-done((bf16[512,256]{1,0:T(8,128)(2,1)S(1)}, bf16[512,256]{1,0:T(8,128)(2,1)}, u32[]{:S(2)}) %copy-start.5) | copy-done | bytes 262168
  7.6 0.0 copy-start.7
  7.6 0.8 %copy-done.7 = bf16[96,256]{1,0:T(8,128)(2,1)S(1)} copy-done((bf16[96,256]{1,0:T(8,128)(2,1)S(1)}, bf16[96,256]{1,0:T(8,128)(2,1)}, u32[]{:S(2)}) %copy-start.7) | copy-done | bytes 49176
  8.4 0.7 %copy-done.8 = f32[512]{0:T(512)S(1)} copy-done((f32[512]{0:T(512)S(1)}, f32[512]{0:T(512)}, u32[]{:S(2)}) %copy-start.8) | copy-done | bytes 2072
  9.1 0.7 %copy-done.9 = s32[4,24]{1,0:T(4,128)S(1)} copy-done((s32[4,24]{1,0:T(4,128)S(1)}, s32[4,24]{1,0:T(4,128)}, u32[]{:S(2)}) %copy-start.9) | copy-done | bytes 408
  9.8 0.7 %copy-done.10 = s32[4]{0:T(128)S(1)} copy-done((s32[4]{0:T(128)S(1)}, s32[4]{0:T(128)}, u32[]{:S(2)}) %copy-start.10) | copy-done | bytes 40
  10.4 0.7 %copy-done.11 = s32[4]{0:T(128)S(1)} copy-done((s32[4]{0:T(128)S(1)}, s32[4]{0:T(128)}, u32[]{:S(2)}) %copy-start.11) | copy-done | bytes 40
  11.1 0.7 %copy-done.12 = f32[256]{0:T(256)S(1)} copy-done((f32[256]{0:T(256)S(1)}, f32[256]{0:T(256)}, u32[]{:S(2)}) %copy-start.12) | copy-done | bytes 1048
  11.8 0.7 %copy-done.13 = f32[8]{0:T(128)S(1)} copy-done((f32[8]{0:T(128)S(1)}, f32[8]{0:T(128)}, u32[]{:S(2)}) %copy-start.13) | copy-done | bytes 56
  12.4 44.5 %attention.1 = (bf16[96,256]{1,0:T(8,128)(2,1)S(1)}, bf16[16,2,32,128]{3,2,1,0:T(8,128)(2,1)S(1)}) custom-call(bf16[96,256]{1,0:T(8,128)(2,1)S(1)} %copy-done.7, f32[1,256]{1,0:T(1,128)S(1)} %bitcast.3, bf16[256,512]{1,0:T(8,128)(2,1)S(1)} %copy-done.2, bf16[256,512]{1,0:T(8,128)(2,1)S(1)} %copy-done.3, bf16[256,512]{1,0:T(8,128)(2,1)S(1)} %copy-done.4, ...), custom_call_target="tpu_custom_call" | custom-call | tf_op jit(solution)/shard_map/attention/pallas_call | solution.py:382
  57.0 0.0 copy-start.6
  57.0 0.7 %copy-done.6 = bf16[16,2,32,128]{3,2,1,0:T(8,128)(2,1)} copy-done((bf16[16,2,32,128]{3,2,1,0:T(8,128)(2,1)}, bf16[16,2,32,128]{3,2,1,0:T(8,128)(2,1)S(1)}, u32[]{:S(2)}) %copy-start.6) | copy-done | bytes 262168
  57.7 4.5 %caches.1 = (bf16[4,512,512]{2,1,0:T(8,128)(2,1)}, bf16[4,512,512]{2,1,0:T(8,128)(2,1)}) custom-call(bf16[4,512,512]{2,1,0:T(8,128)(2,1)} %ck_hbm.3, bf16[4,512,512]{2,1,0:T(8,128)(2,1)} %cv_hbm.3, bf16[16,2,32,128]{3,2,1,0:T(8,128)(2,1)} %copy-done.6, s32[4]{0:T(128)} %len_ref.3, s32[4]{0:T(128)} %acc_ref.3), custom_call_target="tpu_custom_call" | custom-call | tf_op jit(solution)/shard_map/caches/pallas_call | solution.py:463
  62.2 0.6 copy.17
  (7 shorter events, 0.0 us)
Async XLA Ops:
  0.6 1.6 %copy-start = (bf16[4,512,512]{2,1,0:T(8,128)(2,1)S(1)}, bf16[4,512,512]{2,1,0:T(8,128)(2,1)}, u32[]{:S(2)}) copy-start(bf16[4,512,512]{2,1,0:T(8,128)(2,1)} %ck_hbm.3) | copy-start | bytes 6291460
  2.2 1.6 %copy-start.1 = (bf16[4,512,512]{2,1,0:T(8,128)(2,1)S(1)}, bf16[4,512,512]{2,1,0:T(8,128)(2,1)}, u32[]{:S(2)}) copy-start(bf16[4,512,512]{2,1,0:T(8,128)(2,1)} %cv_hbm.3) | copy-start | bytes 6291460
  3.8 0.9 %copy-start.2 = (bf16[256,512]{1,0:T(8,128)(2,1)S(1)}, bf16[256,512]{1,0:T(8,128)(2,1)}, u32[]{:S(2)}) copy-start(bf16[256,512]{1,0:T(8,128)(2,1)} %wq_hbm.1) | copy-start | bytes 786436
  4.8 0.9 %copy-start.3 = (bf16[256,512]{1,0:T(8,128)(2,1)S(1)}, bf16[256,512]{1,0:T(8,128)(2,1)}, u32[]{:S(2)}) copy-start(bf16[256,512]{1,0:T(8,128)(2,1)} %wk_hbm.1) | copy-start | bytes 786436
  5.7 0.9 %copy-start.4 = (bf16[256,512]{1,0:T(8,128)(2,1)S(1)}, bf16[256,512]{1,0:T(8,128)(2,1)}, u32[]{:S(2)}) copy-start(bf16[256,512]{1,0:T(8,128)(2,1)} %wv_hbm.1) | copy-start | bytes 786436
  6.7 0.9 %copy-start.5 = (bf16[512,256]{1,0:T(8,128)(2,1)S(1)}, bf16[512,256]{1,0:T(8,128)(2,1)}, u32[]{:S(2)}) copy-start(bf16[512,256]{1,0:T(8,128)(2,1)} %wo_hbm.1) | copy-start | bytes 786436
  7.6 0.8 %copy-start.7 = (bf16[96,256]{1,0:T(8,128)(2,1)S(1)}, bf16[96,256]{1,0:T(8,128)(2,1)}, u32[]{:S(2)}) copy-start(bf16[96,256]{1,0:T(8,128)(2,1)} %tok_hbm.1) | copy-start | bytes 147460
  8.4 0.7 %copy-start.8 = (f32[512]{0:T(512)S(1)}, f32[512]{0:T(512)}, u32[]{:S(2)}) copy-start(f32[512]{0:T(512)} %param.22) | copy-start | bytes 6148
  9.1 0.7 %copy-start.9 = (s32[4,24]{1,0:T(4,128)S(1)}, s32[4,24]{1,0:T(4,128)}, u32[]{:S(2)}) copy-start(s32[4,24]{1,0:T(4,128)} %par_ref.1) | copy-start | bytes 1156
  9.8 0.7 %copy-start.10 = (s32[4]{0:T(128)S(1)}, s32[4]{0:T(128)}, u32[]{:S(2)}) copy-start(s32[4]{0:T(128)} %len_ref.3) | copy-start | bytes 52
  10.4 0.7 %copy-start.11 = (s32[4]{0:T(128)S(1)}, s32[4]{0:T(128)}, u32[]{:S(2)}) copy-start(s32[4]{0:T(128)} %acc_ref.3) | copy-start | bytes 52
  11.1 0.7 %copy-start.12 = (f32[256]{0:T(256)S(1)}, f32[256]{0:T(256)}, u32[]{:S(2)}) copy-start(f32[256]{0:T(256)} %param.14) | copy-start | bytes 3076
  11.8 0.7 %copy-start.13 = (f32[8]{0:T(128)S(1)}, f32[8]{0:T(128)}, u32[]{:S(2)}) copy-start(f32[8]{0:T(128)} %lam_ref.1) | copy-start | bytes 100
  57.0 0.7 %copy-start.6 = (bf16[16,2,32,128]{3,2,1,0:T(8,128)(2,1)}, bf16[16,2,32,128]{3,2,1,0:T(8,128)(2,1)S(1)}, u32[]{:S(2)}) copy-start(bf16[16,2,32,128]{3,2,1,0:T(8,128)(2,1)S(1)} %get-tuple-element.8.kvn_ref) | copy-start | bytes 786436

commit v2 on v1

v2 whole, which is shorter than its diff:
```python
import functools

import jax
import jax.numpy as jnp
from jax import lax
from jax.experimental import pallas as pl
from jax.experimental.pallas import tpu as pltpu
from jax.sharding import PartitionSpec as P

D = 4096
HEAD = 64
QK = 32
SEQS = 4
PROP = 24
KV = 16
TP = 8
BLOCK = 128
PAD = 32
POS = 512
ROWS = 96
EPS = 1e-05
LOW = -1e30
LOG2E = 1.4426950408889634
WRITE_VMEM = 16 * 1024 * 1024
MAIN_VMEM = 40 * 1024 * 1024
SCALE2 = QK ** (-0.5) * LOG2E
F32 = jnp.float32
BF16 = jnp.bfloat16
NT = (((1,), (1,)), ((), ()))


def _distance(step):
    ring = (0, 1, 2, 1)
    return ring[step >> 2] + ring[step & 3]


Z_ORDER = (0, 2, 1, 3)
PARTNERS = sorted(range(1, KV), key=lambda step: -_distance(step))


def _dot(a, b):
    return jnp.dot(a, b, preferred_element_type=F32)


def _dot_nt(a, b):
    return lax.dot_general(a, b, NT, preferred_element_type=F32)


def _split_rows(row):
    high = row.astype(BF16).astype(F32)
    middle = (row - high).astype(BF16).astype(F32)
    low = row - high - middle
    index = lax.broadcasted_iota(jnp.int32, (PAD - PROP, BLOCK), 0)
    return jnp.where(index == 0, high, jnp.where(index == 1, middle, jnp.where(index == 2, low, 0.0)))


def _expanded(chunk):
    lane = lax.broadcasted_iota(jnp.int32, (PROP, BLOCK), 1)
    parts = []
    for which in range(2):
        for head in range(2):
            low = head * HEAD + which * QK
            inside = (lane >= low) & (lane < low + QK)
            parts.append(jnp.where(inside, chunk, 0.0))
    parts.append(jnp.zeros((BLOCK - 4 * PROP, BLOCK), F32))
    return jnp.concatenate(parts, axis=0).astype(BF16)


def _main_kernel(
    tok_hbm,
    gain_hbm,
    wq_hbm,
    wk_hbm,
    wv_hbm,
    wo_hbm,
    ck_hbm,
    cv_hbm,
    lam_hbm,
    og_hbm,
    par_hbm,
    len_hbm,
    acc_hbm,
    mixed_ref,
    kbuf,
    vbuf,
    tok,
    gain_ref,
    og_ref,
    par_ref,
    lam_ref,
    len_ref,
    acc_ref,
    wqkv,
    wo,
    vt,
    pq,
    rq,
    pkv,
    rkv,
    qg,
    kvg,
    dv,
    rdv,
    ds,
    rds,
    ng,
    part,
    rpart,
    par_pad,
    qe,
    load_sem,
    q_send,
    q_recv,
    kv_send,
    kv_recv,
    qg_send,
    qg_recv,
    kvg_send,
    kvg_recv,
    dv_send,
    dv_recv,
    ds_send,
    ds_recv,
    ng_send,
    ng_recv,
    mx_send,
    mx_recv,
):
    me = lax.axis_index("kv")
    tp = lax.axis_index("tp")
    z = me // 4
    x = lax.rem(me, 4)

    barrier = pltpu.get_barrier_semaphore()
    for step in PARTNERS:
        pl.semaphore_signal(barrier, inc=1, device_id={"kv": me ^ step}, device_id_type=pl.DeviceIdType.MESH)
    for step in range(1, TP):
        pl.semaphore_signal(barrier, inc=1, device_id={"tp": tp ^ step}, device_id_type=pl.DeviceIdType.MESH)

    loads = {}

    def load(name, src, dst, index):
        copy = pltpu.make_async_copy(src, dst, load_sem.at[index])
        copy.start()
        loads[name] = copy

    load("tok", tok_hbm, tok, 0)
    load("gain", gain_hbm, gain_ref, 13)
    load("wq", wq_hbm, wqkv.at[0], 1)
    load("wk", wk_hbm, wqkv.at[1], 2)
    load("wv", wv_hbm, wqkv.at[2], 3)
    for b in range(SEQS):
        load(("v", b), cv_hbm.at[b], vbuf.at[b], 4 + b)
    for b in range(SEQS):
        load(("k", b), ck_hbm.at[b], kbuf.at[b], 8 + b)
    load("wo", wo_hbm, wo, 12)
    load("og", og_hbm, og_ref, 14)
    load("par", par_hbm, par_ref, 15)
    load("lam", lam_hbm, lam_ref, 16)
    load("len", len_hbm, len_ref, 17)
    load("acc", acc_hbm, acc_ref, 18)

    def to_kv(step, src, dst, send, recv):
        return pltpu.make_async_remote_copy(
            src_ref=src,
            dst_ref=dst,
            send_sem=send.at[step],
            recv_sem=recv.at[step],
            device_id={"kv": me ^ step},
            device_id_type=pl.DeviceIdType.MESH,
        )

    def q_copy(step):
        return to_kv(step, pq.at[me ^ step], rq.at[step], q_send, q_recv)

    def kv_copy(step):
        return to_kv(step, pkv.at[me ^ step], rkv.at[step], kv_send, kv_recv)

    def qg_copy(step):
        return to_kv(step, qg.at[me], qg.at[me], qg_send, qg_recv)

    def kvg_copy(step):
        return to_kv(step, kvg.at[me], kvg.at[me], kvg_send, kvg_recv)

    def dv_copy(step):
        return to_kv(step, dv.at[me ^ step], rdv.at[step], dv_send, dv_recv)

    def ds_copy(step):
        return to_kv(step, ds.at[me ^ step], rds.at[step], ds_send, ds_recv)

    def ng_slot():
        return ng.at[x, pl.ds(pl.multiple_of(z * PAD, PAD), PAD), :]

    def ng_copy(step):
        return to_kv(step, ng_slot(), ng_slot(), ng_send, ng_recv)

    def mx_copy(far, step):
        return pltpu.make_async_remote_copy(
            src_ref=part.at[z // 2 ^ far],
            dst_ref=rpart.at[far, step],
            send_sem=mx_send.at[far, step],
            recv_sem=mx_recv.at[far, step],
            device_id={"tp": tp ^ step},
            device_id_type=pl.DeviceIdType.MESH,
        )

    loads["tok"].wait()
    loads["gain"].wait()
    wide = tok[...].astype(F32)
    gained = (wide * gain_ref[...]).astype(BF16)
    square = jnp.sum(wide * wide, axis=1, keepdims=True)
    eye = lax.broadcasted_iota(jnp.int32, (PROP, BLOCK), 0) == lax.broadcasted_iota(jnp.int32, (PROP, BLOCK), 1)
    loads["wq"].wait()
    partial_q = _dot(gained, wqkv[0])
    for b in range(SEQS):
        column = square[b * PROP : (b + 1) * PROP]
        row = jnp.sum(jnp.where(eye, column, 0.0), axis=0, keepdims=True)
        tail = _split_rows(row)
        for block in range(4):
            chunk = partial_q[b * PROP : (b + 1) * PROP, block * BLOCK : (block + 1) * BLOCK]
            pq[b * 4 + block] = jnp.concatenate([chunk, tail], axis=0).astype(BF16)
    pl.semaphore_wait(barrier, KV - 1 + TP - 1)
    for step in PARTNERS:
        q_copy(step).start()
    projected = []
    for which in range(2):
        loads["wk" if which == 0 else "wv"].wait()
        projected.append(_dot(gained, wqkv[1 + which]))
    for b in range(SEQS):
        for block in range(4):
            pkv[b * 4 + block] = jnp.concatenate(
                [
                    part_kv[b * PROP : (b + 1) * PROP, block * BLOCK : (block + 1) * BLOCK]
                    for part_kv in projected
                ],
                axis=0,
            ).astype(BF16)
    def transpose_values(b):
        loads[("v", b)].wait()
        for block in range(4):
            vt[b, block * BLOCK : (block + 1) * BLOCK, :] = jnp.transpose(
                vbuf[b, :, block * BLOCK : (block + 1) * BLOCK]
            )

    for order in range(SEQS):
        for half in range(2):
            for side in range(2):
                qe[order, half, side * BLOCK : (side + 1) * BLOCK, (1 - side) * BLOCK : (2 - side) * BLOCK] = (
                    jnp.zeros((BLOCK, BLOCK), BF16)
                )
    transpose_values(0)
    transpose_values(1)

    for step in PARTNERS:
        q_copy(step).wait_recv()
    total = pq[me].astype(F32)
    for step in range(1, KV):
        total = total + rq[step].astype(F32)
    square_row = jnp.sum(total[PROP:PAD], axis=0, keepdims=True)
    square_column = jnp.sum(jnp.where(eye, square_row, 0.0), axis=1, keepdims=True)
    factor = lax.rsqrt(square_column / D + EPS)
    own_q = total[0:PROP] * factor
    zero_tail = jnp.zeros((PAD - PROP, BLOCK), F32)
    qg[me] = jnp.concatenate([own_q, zero_tail], axis=0).astype(BF16)
    for step in PARTNERS:
        qg_copy(step).start()

    for step in PARTNERS:
        kv_copy(step).start()
    transpose_values(2)
    transpose_values(3)
    for b in range(SEQS):
        loads[("k", b)].wait()
    for name in ("og", "par", "lam", "len", "acc"):
        loads[name].wait()

    lane = lax.broadcasted_iota(jnp.int32, (HEAD, BLOCK), 1)
    second_head = ((lane >= PROP) & (lane < 2 * PROP)) | (lane >= 3 * PROP)
    for order, z_step in enumerate(Z_ORDER):
        for step in PARTNERS:
            if step >> 2 == z_step:
                qg_copy(step).wait_recv()
        b = z ^ z_step
        begin = len_ref[b] + acc_ref[b] - me * POS
        visible = lax.broadcasted_iota(jnp.int32, (POS, BLOCK), 0) < begin
        visible = jnp.concatenate([visible, visible], axis=1)
        for half in range(2):
            for side in range(2):
                chunk = qg[b * 4 + half * 2 + side].astype(F32)[0:PROP]
                lanes = slice(side * BLOCK, (side + 1) * BLOCK)
                qe[order, half, lanes, lanes] = _expanded(chunk)
        for half in range(2):
            keys = kbuf[b, :, half * 2 * BLOCK : (half + 1) * 2 * BLOCK]
            scores = _dot_nt(keys, qe[order, half]) * SCALE2
            scores = jnp.where(visible, scores, LOW)
            largest = jnp.max(scores, axis=0, keepdims=True)
            weight = jnp.exp2(scores - largest)
            weight_sum = jnp.sum(weight, axis=0, keepdims=True)
            weight = weight.astype(BF16)
            for side in range(2):
                block = half * 2 + side
                lanes = slice(side * BLOCK, (side + 1) * BLOCK)
                out = _dot(vt[b, block * BLOCK : (block + 1) * BLOCK, :], weight[:, lanes])
                owner = b * 4 + block
                dv[owner] = jnp.where(second_head, out[HEAD:], out[:HEAD]).astype(BF16)
                ds[owner] = jnp.concatenate(
                    [jnp.broadcast_to(largest[:, lanes], (4, BLOCK)), jnp.broadcast_to(weight_sum[:, lanes], (4, BLOCK))],
                    axis=0,
                )
        for x_step in (2, 1, 3, 0):
            step = z_step << 2 | x_step
            if step:
                dv_copy(step).start()
                ds_copy(step).start()

    for step in PARTNERS:
        kv_copy(step).wait_recv()
    summed = pkv[me].astype(F32)
    for step in range(1, KV):
        summed = summed + rkv[step].astype(F32)
    own_k = jnp.concatenate([summed[0:PROP] * factor, zero_tail], axis=0).astype(BF16)
    own_v = jnp.concatenate([summed[PROP:] * factor, zero_tail], axis=0)
    kvg[me] = jnp.concatenate([summed[0:PROP] * factor, summed[PROP:] * factor], axis=0).astype(BF16)
    for step in PARTNERS:
        kvg_copy(step).start()
    par_pad[...] = jnp.full((8, BLOCK), -1, jnp.int32)
    par_pad[0:SEQS, 0:PROP] = par_ref[...]
    parent_row = par_pad[pl.ds(z, 1), :]
    row_index = lax.broadcasted_iota(jnp.int32, (BLOCK, BLOCK), 0)
    lane_index = lax.broadcasted_iota(jnp.int32, (BLOCK, BLOCK), 1)
    reach = ((parent_row == row_index) & (lane_index < PROP)) | (row_index == lane_index)
    reach = jnp.where(reach, 1.0, 0.0).astype(BF16)
    for _ in range(5):
        reach = jnp.minimum(_dot(reach, reach), 1.0).astype(BF16)
    spread = (lax.rem(lane_index, PROP) == row_index) & (lane_index < 4 * PROP) & (row_index < PROP)
    lineage = _dot(reach, jnp.where(spread, 1.0, 0.0).astype(BF16))[0:PAD]
    linked = (lineage > 0.5) & (lax.broadcasted_iota(jnp.int32, (PAD, BLOCK), 0) < PROP)
    own_expanded = _expanded(qg[me].astype(F32)[0:PROP])
    self_scores = _dot_nt(own_k, own_expanded) * SCALE2
    self_scores = jnp.where(linked, self_scores, LOW)
    self_max = jnp.max(self_scores, axis=0, keepdims=True)
    self_weight = jnp.where(linked, jnp.exp2(self_scores - self_max), 0.0)
    self_total = jnp.sum(self_weight, axis=0, keepdims=True)
    values_t = jnp.transpose(own_v).astype(BF16)
    self_out = _dot(values_t, self_weight.astype(BF16))
    self_sum = jnp.where(second_head, self_out[HEAD:], self_out[:HEAD])

    for step in PARTNERS:
        ds_copy(step).wait_recv()
    maxima = [ds[me, 0:1]] + [rds[step, 0:1] for step in range(1, KV)]
    totals = [ds[me, 4:5]] + [rds[step, 4:5] for step in range(1, KV)]
    top = functools.reduce(jnp.maximum, maxima, self_max)
    self_factor = jnp.exp2(self_max - top)
    denominator = self_total * self_factor
    factors = []
    for largest, weight_sum in zip(maxima, totals):
        factors.append(jnp.exp2(largest - top))
        denominator = denominator + weight_sum * factors[-1]
    for step in PARTNERS:
        dv_copy(step).wait_recv()
    merged = self_sum * self_factor + dv[me].astype(F32) * factors[0]
    for step in range(1, KV):
        merged = merged + rdv[step].astype(F32) * factors[step]
    attended = merged / denominator
    lane_row = lax.broadcasted_iota(jnp.int32, (1, BLOCK), 1)
    lam = jnp.where(lane_row < PROP, lam_ref[x * 2], lam_ref[x * 2 + 1])
    difference = attended - lam * pltpu.roll(attended, BLOCK - 2 * PROP, 1)
    power = jnp.mean(difference * difference, axis=0, keepdims=True)
    normed = difference * lax.rsqrt(power + EPS)
    stacked = jnp.concatenate([normed, pltpu.roll(normed, BLOCK - PROP, 1)], axis=0)
    turned = jnp.transpose(stacked)[0:PROP]
    turned = turned * og_ref[pl.ds(x, 1), :]
    ng[x, pl.ds(pl.multiple_of(z * PAD, PAD), PAD), :] = jnp.concatenate([turned, zero_tail], axis=0).astype(BF16)
    for step in PARTNERS:
        ng_copy(step).start()

    loads["wo"].wait()
    for far in range(2):
        for step in PARTNERS:
            if step >> 3 == far:
                ng_copy(step).wait_recv()
        pair = z // 2 ^ far
        first = pl.multiple_of(pair * 2 * PAD, 2 * PAD)
        rows = jnp.concatenate([ng[block, pl.ds(first, 2 * PAD), :] for block in range(4)], axis=1)
        projected = _dot(rows, wo[...])
        projected = jnp.concatenate([projected[0:PROP], projected[PAD : PAD + PROP]], axis=0)
        part[pair] = projected.astype(BF16)
        for step in range(1, TP):
            mx_copy(far, step).start()

    for step in PARTNERS:
        kvg_copy(step).wait_recv()
    for b in range(SEQS):
        begin = len_ref[b] + acc_ref[b] - me * POS
        position = lax.broadcasted_iota(jnp.int32, (POS, BLOCK), 0) - begin
        written = (position >= 0) & (position < PROP)
        slot = lax.broadcasted_iota(jnp.int32, (POS, BLOCK), 1)
        for which, buf in enumerate((kbuf, vbuf)):
            offset = which * PROP
            placing = jnp.where(written & (position + offset == slot), 1.0, 0.0).astype(BF16)[:, 0 : 2 * PROP]
            for block in range(4):
                lanes = slice(block * BLOCK, (block + 1) * BLOCK)
                moved = _dot(placing, kvg[b * 4 + block])
                buf[b, :, lanes] = jnp.where(written, moved, buf[b, :, lanes].astype(F32)).astype(BF16)

    for far in range(2):
        for step in range(1, TP):
            mx_copy(far, step).wait_recv()
        pair = z // 2 ^ far
        mixed = part[pair].astype(F32)
        for step in range(1, TP):
            mixed = mixed + rpart[far, step].astype(F32)
        mixed_ref[pair] = mixed.astype(BF16)

    for step in PARTNERS:
        for copy in (q_copy, kv_copy, qg_copy, kvg_copy, dv_copy, ds_copy, ng_copy):
            copy(step).wait_send()
    for far in range(2):
        for step in range(1, TP):
            mx_copy(far, step).wait_send()


def _main(*arrays):
    hbm = pl.BlockSpec(memory_space=pltpu.HBM)
    vmem = pl.BlockSpec(memory_space=pltpu.VMEM)
    dma = pltpu.SemaphoreType.DMA
    return pl.pallas_call(
        _main_kernel,
        out_shape=(
            jax.ShapeDtypeStruct((2, 2 * PROP, 256), BF16),
            jax.ShapeDtypeStruct((SEQS, POS, 512), BF16),
            jax.ShapeDtypeStruct((SEQS, POS, 512), BF16),
        ),
        in_specs=[hbm] * 13,
        out_specs=(vmem,) * 3,
        scratch_shapes=[
            pltpu.VMEM((ROWS, 256), BF16),
            pltpu.VMEM((1, 256), F32),
            pltpu.VMEM((4, BLOCK), F32),
            pltpu.VMEM((SEQS, PROP), jnp.int32),
            pltpu.SMEM((TP,), F32),
            pltpu.SMEM((SEQS,), jnp.int32),
            pltpu.SMEM((SEQS,), jnp.int32),
            pltpu.VMEM((3, 256, 512), BF16),
            pltpu.VMEM((512, 256), BF16),
            pltpu.VMEM((SEQS, 512, POS), BF16),
            pltpu.VMEM((KV, PAD, BLOCK), BF16),
            pltpu.VMEM((KV, PAD, BLOCK), BF16),
            pltpu.VMEM((KV, 2 * PROP, BLOCK), BF16),
            pltpu.VMEM((KV, 2 * PROP, BLOCK), BF16),
            pltpu.VMEM((KV, PAD, BLOCK), BF16),
            pltpu.VMEM((KV, 2 * PROP, BLOCK), BF16),
            pltpu.VMEM((KV, HEAD, BLOCK), BF16),
            pltpu.VMEM((KV, HEAD, BLOCK), BF16),
            pltpu.VMEM((KV, 8, BLOCK), F32),
            pltpu.VMEM((KV, 8, BLOCK), F32),
            pltpu.VMEM((4, SEQS * PAD, BLOCK), BF16),
            pltpu.VMEM((2, 2 * PROP, 256), BF16),
            pltpu.VMEM((2, TP, 2 * PROP, 256), BF16),
            pltpu.VMEM((8, BLOCK), jnp.int32),
            pltpu.VMEM((SEQS, 2, 2 * BLOCK, 2 * BLOCK), BF16),
            dma((19,)),
        ]
        + [dma((KV,))] * 14
        + [dma((2, TP))] * 2,
        compiler_params=pltpu.CompilerParams(
            collective_id=0, has_side_effects=True, vmem_limit_bytes=MAIN_VMEM
        ),
        name="attention",
    )(*(pltpu.with_memory_space_constraint(array, pltpu.HBM) for array in arrays))


def _write_kernel(mixed_ref, keys_ref, values_ref, mixed_hbm, keys_hbm, values_hbm, sem):
    copies = [pltpu.make_async_copy(mixed_ref, mixed_hbm, sem.at[0])]
    for b in range(SEQS):
        copies.append(pltpu.make_async_copy(keys_ref.at[b], keys_hbm.at[b], sem.at[1 + b]))
        copies.append(pltpu.make_async_copy(values_ref.at[b], values_hbm.at[b], sem.at[1 + SEQS + b]))
    for copy in copies:
        copy.start()
    for copy in copies:
        copy.wait()


def _write(*arrays):
    hbm = pl.BlockSpec(memory_space=pltpu.HBM)
    vmem = pl.BlockSpec(memory_space=pltpu.VMEM)
    return pl.pallas_call(
        _write_kernel,
        out_shape=tuple(jax.ShapeDtypeStruct(array.shape, array.dtype) for array in arrays),
        in_specs=[vmem] * 3,
        out_specs=(hbm,) * 3,
        scratch_shapes=[pltpu.SemaphoreType.DMA((1 + 2 * SEQS,))],
        compiler_params=pltpu.CompilerParams(vmem_limit_bytes=WRITE_VMEM),
        name="write",
    )(*arrays)


def _local(
    tokens,
    norm_gain,
    w_query,
    w_key,
    w_value,
    w_output,
    cache_keys,
    cache_values,
    map_lambda,
    out_gain,
    parents,
    lengths,
    accepted,
):
    mixed, keys, values = _main(
        tokens,
        norm_gain.reshape(1, 256),
        w_query,
        w_key,
        w_value,
        w_output,
        cache_keys,
        cache_values,
        map_lambda,
        out_gain.reshape(4, BLOCK),
        parents,
        lengths,
        accepted,
    )
    mixed, new_keys, new_values = _write(mixed, keys, values)
    return mixed.reshape(ROWS, 256), new_keys, new_values


def solution(mesh):
    return jax.shard_map(
        _local,
        mesh=mesh,
        in_specs=(
            P(None, "kv"),
            P("kv"),
            P("kv", "tp"),
            P("kv", "tp"),
            P("kv", "tp"),
            P("tp", "kv"),
            P(None, "kv", "tp"),
            P(None, "kv", "tp"),
            P("tp"),
            P("tp"),
            P(),
            P(),
            P(),
        ),
        out_specs=(P(None, "kv"), P(None, "kv", "tp"), P(None, "kv", "tp")),
        check_vma=False,
    )
```

time: 63.3 us -> 42.2 us (0.67)
  local copies, waits for them, and re-layouts: 13.1 us -> 0 us
  Pallas kernels: 49 us -> 41.5 us
    unnamed x29 -> x0, local copies, waits for them, and re-layouts: 13.1 us -> none
    pallas_call x2, Pallas kernels: 49 us -> 41.5 us  [the longest x1 39.4 us: _main(): pl.pallas_call(_main_kernel, out_shape=(jax.ShapeDtypeStruct((2, 2 * PROP...]
where the time goes in v2:
time: 42.2 us; the launch traced here: 42.1 us
  Pallas kernels  41.5 us (98%)
  between operations  0.64 us (2%)
    pallas_call x1, Pallas kernels, _main(): pl.pallas_call(_main_kernel, out_shape=(jax.ShapeDtypeStruct((2, 2 * PROP...  39.4 us
    pallas_call x1, Pallas kernels, _write(): pl.pallas_call(_write_kernel, out_shape=tuple((jax.ShapeDtypeStruct(array...  2.1 us

profile of v2, /device:TPU:1, one launch (start us, length us, event | category | flops | bytes accessed | tf_op | source)
XLA Modules:
  0.0 42.1 jit_solution(12810449694721193121)
XLA Ops:
  0.6 39.4 %attention.1 = (bf16[2,48,256]{2,1,0:T(8,128)(2,1)S(1)}, bf16[4,512,512]{2,1,0:T(8,128)(2,1)S(1)}, bf16[4,512,512]{2,1,0:T(8,128)(2,1)S(1)}) custom-call(bf16[96,256]{1,0:T(8,128)(2,1)} %tok_hbm.1, f32[1,256]{1,0:T(1,128)} %bitcast.4, bf16[256,512]{1,0:T(8,128)(2,1)} %wq_hbm.1, bf16[256,512]{1,0:T(8,128)(2,1)} %wk_hbm.1, bf16[256,512]{1,0:T(8,128)(2,1)} %wv_hbm.1, ...), custom_call_target="tpu_custom_call" | custom-call | tf_op jit(solution)/shard_map/attention/pallas_call | solution.py:427
  40.0 2.1 %write.1 = (bf16[2,48,256]{2,1,0:T(8,128)(2,1)}, bf16[4,512,512]{2,1,0:T(8,128)(2,1)}, bf16[4,512,512]{2,1,0:T(8,128)(2,1)}) custom-call(bf16[2,48,256]{2,1,0:T(8,128)(2,1)S(1)} %get-tuple-element.9.mixed_ref, bf16[4,512,512]{2,1,0:T(8,128)(2,1)S(1)} %get-tuple-element.10.keys_ref, bf16[4,512,512]{2,1,0:T(8,128)(2,1)S(1)} %get-tuple-element.11.values_ref), custom_call_target="tpu_custom_call" | custom-call | tf_op jit(solution)/shard_map/write/pallas_call | solution.py:487

commit v3 on v2

v3 whole, which is shorter than its diff:
```python
import functools

import jax
import jax.numpy as jnp
from jax import lax
from jax.experimental import pallas as pl
from jax.experimental.pallas import tpu as pltpu
from jax.sharding import PartitionSpec as P

D = 4096
HEAD = 64
QK = 32
SEQS = 4
PROP = 24
KV = 16
TP = 8
BLOCK = 128
PAD = 32
POS = 512
ROWS = 96
EPS = 1e-05
LOW = -1e30
LOG2E = 1.4426950408889634
WRITE_VMEM = 16 * 1024 * 1024
MAIN_VMEM = 40 * 1024 * 1024
SCALE2 = QK ** (-0.5) * LOG2E
F32 = jnp.float32
BF16 = jnp.bfloat16
NT = (((1,), (1,)), ((), ()))


def _distance(step):
    ring = (0, 1, 2, 1)
    return ring[step >> 2] + ring[step & 3]


Q_SEND = 0
KV_SEND = 1
QG_SEND = 2
KVG_SEND = 3
DV_SEND = 4
DS_SEND = 5
NG_SEND = 6
MX_SEND = 7
Q_RECV = 8
KV_RECV = 9
KVG_RECV = 10
DV_RECV = 11
DS_RECV = 12
QG_RECV = 13
NG_RECV = 17
MX_RECV = 21
SEMAPHORES = 25
Z_ORDER = (0, 2, 1, 3)
Z_OUT = (0, 1, 3, 2)
TP_ORDER = (4, 5, 2, 3, 6, 7, 1)
PARTNERS = sorted(range(1, KV), key=lambda step: -_distance(step))


def _dot(a, b):
    return jnp.dot(a, b, preferred_element_type=F32)


def _dot_nt(a, b):
    return lax.dot_general(a, b, NT, preferred_element_type=F32)


def _split_rows(row):
    high = row.astype(BF16).astype(F32)
    middle = (row - high).astype(BF16).astype(F32)
    low = row - high - middle
    index = lax.broadcasted_iota(jnp.int32, (PAD - PROP, BLOCK), 0)
    return jnp.where(index == 0, high, jnp.where(index == 1, middle, jnp.where(index == 2, low, 0.0)))


def _packed(block):
    rest = block[48:]
    moved = jnp.concatenate([pltpu.roll(rest, 96 - 32 * part, 1) for part in range(3)], axis=0)
    return jnp.where(lax.broadcasted_iota(jnp.int32, (48, BLOCK), 1) < 96, block[:48], moved)


def _unpacked(packed):
    lane = lax.broadcasted_iota(jnp.int32, (16, BLOCK), 1)
    parts = [pltpu.roll(packed[16 * part : 16 * part + 16], 32 * part + 32, 1) for part in range(3)]
    rest = jnp.where(lane < 32, parts[0], jnp.where(lane < 64, parts[1], parts[2]))
    return jnp.concatenate([packed, rest], axis=0)


def _expanded(chunk):
    lane = lax.broadcasted_iota(jnp.int32, (PROP, BLOCK), 1)
    parts = []
    for which in range(2):
        for head in range(2):
            low = head * HEAD + which * QK
            inside = (lane >= low) & (lane < low + QK)
            parts.append(jnp.where(inside, chunk, 0.0))
    parts.append(jnp.zeros((BLOCK - 4 * PROP, BLOCK), F32))
    return jnp.concatenate(parts, axis=0).astype(BF16)


def _main_kernel(
    tok_hbm,
    gain_hbm,
    wq_hbm,
    wk_hbm,
    wv_hbm,
    wo_hbm,
    ck_hbm,
    cv_hbm,
    lam_hbm,
    og_hbm,
    par_hbm,
    len_hbm,
    acc_hbm,
    mixed_ref,
    keys_out,
    values_out,
    kbuf,
    vbuf,
    tok,
    gain_ref,
    og_ref,
    par_ref,
    lam_ref,
    len_ref,
    acc_ref,
    wqkv,
    wo,
    vt,
    pq,
    rq,
    pkv,
    rkv,
    qg,
    kvg,
    dv,
    rdv,
    ds,
    rds,
    ng,
    part,
    rpart,
    par_pad,
    qe,
    load_sem,
    sems,
    out_sem,
):
    me = lax.axis_index("kv")
    tp = lax.axis_index("tp")
    z = me // 4
    x = lax.rem(me, 4)

    barrier = pltpu.get_barrier_semaphore()
    for step in PARTNERS:
        pl.semaphore_signal(barrier, inc=1, device_id={"kv": me ^ step}, device_id_type=pl.DeviceIdType.MESH)
    for step in range(1, TP):
        pl.semaphore_signal(barrier, inc=1, device_id={"tp": tp ^ step}, device_id_type=pl.DeviceIdType.MESH)

    loads = [
        (tok_hbm, tok),
        (gain_hbm, gain_ref),
        (wq_hbm, wqkv.at[0]),
        (wk_hbm, wqkv.at[1]),
        (wv_hbm, wqkv.at[2]),
        (cv_hbm, vbuf),
        (ck_hbm, kbuf),
        (wo_hbm, wo),
        (og_hbm, og_ref),
        (par_hbm, par_ref),
        (lam_hbm, lam_ref),
        (len_hbm, len_ref),
        (acc_hbm, acc_ref),
    ]
    loads = [pltpu.make_async_copy(src, dst, load_sem.at[index]) for index, (src, dst) in enumerate(loads)]
    for copy in loads:
        copy.start()

    def arrived(ref, sem):
        pltpu.make_async_copy(ref, ref, sem).wait()

    def to_kv(step, src, dst, send, recv):
        return pltpu.make_async_remote_copy(
            src_ref=src,
            dst_ref=dst,
            send_sem=send,
            recv_sem=recv,
            device_id={"kv": me ^ step},
            device_id_type=pl.DeviceIdType.MESH,
        )

    def q_copy(step):
        return to_kv(step, pq.at[me ^ step], rq.at[step], sems.at[Q_SEND], sems.at[Q_RECV])

    def kv_copy(step):
        return to_kv(step, pkv.at[me ^ step], rkv.at[step], sems.at[KV_SEND], sems.at[KV_RECV])

    def qg_copy(step):
        return to_kv(step, qg.at[me], qg.at[me], sems.at[QG_SEND], sems.at[QG_RECV + (step >> 2)])

    def kvg_copy(step):
        return to_kv(step, kvg.at[me], kvg.at[me], sems.at[KVG_SEND], sems.at[KVG_RECV])

    def dv_copy(step):
        return to_kv(step, dv.at[me ^ step], rdv.at[step], sems.at[DV_SEND], sems.at[DV_RECV])

    def ds_copy(step):
        return to_kv(step, ds.at[me ^ step], rds.at[step], sems.at[DS_SEND], sems.at[DS_RECV])

    def ng_copy(step):
        return to_kv(step, ng.at[me], ng.at[me], sems.at[NG_SEND], sems.at[NG_RECV + (step >> 2)])

    def mx_copy(z_step, step):
        return pltpu.make_async_remote_copy(
            src_ref=part.at[z ^ z_step],
            dst_ref=rpart.at[z_step, step],
            send_sem=sems.at[MX_SEND],
            recv_sem=sems.at[MX_RECV + z_step],
            device_id={"tp": tp ^ step},
            device_id_type=pl.DeviceIdType.MESH,
        )

    def out_copy(which, b):
        buf, out = ((kbuf, keys_out), (vbuf, values_out))[which]
        return pltpu.make_async_copy(buf.at[b], out.at[b], out_sem.at[which])

    loads[0].wait()
    loads[1].wait()
    wide = tok[...].astype(F32)
    gained = (wide * gain_ref[...]).astype(BF16)
    square = jnp.sum(wide * wide, axis=1, keepdims=True)
    eye = lax.broadcasted_iota(jnp.int32, (PROP, BLOCK), 0) == lax.broadcasted_iota(jnp.int32, (PROP, BLOCK), 1)
    loads[2].wait()
    partial_q = _dot(gained, wqkv[0])
    for b in range(SEQS):
        column = square[b * PROP : (b + 1) * PROP]
        row = jnp.sum(jnp.where(eye, column, 0.0), axis=0, keepdims=True)
        tail = _split_rows(row)
        for block in range(4):
            chunk = partial_q[b * PROP : (b + 1) * PROP, block * BLOCK : (block + 1) * BLOCK]
            pq[b * 4 + block] = jnp.concatenate([chunk, tail], axis=0).astype(BF16)
    pl.semaphore_wait(barrier, KV - 1 + TP - 1)
    for step in PARTNERS:
        q_copy(step).start()
    projected = []
    for which in range(2):
        loads[3 + which].wait()
        projected.append(_dot(gained, wqkv[1 + which]))
    for b in range(SEQS):
        for block in range(4):
            pkv[b * 4 + block] = jnp.concatenate(
                [
                    part_kv[b * PROP : (b + 1) * PROP, block * BLOCK : (block + 1) * BLOCK]
                    for part_kv in projected
                ],
                axis=0,
            ).astype(BF16)
    loads[5].wait()

    def transpose_values(b):
        for block in range(4):
            vt[b, block * BLOCK : (block + 1) * BLOCK, :] = jnp.transpose(
                vbuf[b, :, block * BLOCK : (block + 1) * BLOCK]
            )

    for order in range(SEQS):
        for half in range(2):
            for side in range(2):
                qe[order, half, side * BLOCK : (side + 1) * BLOCK, (1 - side) * BLOCK : (2 - side) * BLOCK] = (
                    jnp.zeros((BLOCK, BLOCK), BF16)
                )
    transpose_values(0)
    transpose_values(1)

    arrived(rq.at[1:], sems.at[Q_RECV])
    total = pq[me].astype(F32)
    for step in range(1, KV):
        total = total + rq[step].astype(F32)
    square_row = jnp.sum(total[PROP:PAD], axis=0, keepdims=True)
    square_column = jnp.sum(jnp.where(eye, square_row, 0.0), axis=1, keepdims=True)
    factor = lax.rsqrt(square_column / D + EPS)
    own_q = total[0:PROP] * factor
    zero_tail = jnp.zeros((PAD - PROP, BLOCK), F32)
    qg[me] = own_q.astype(BF16)
    for z_step in Z_ORDER:
        for step in PARTNERS:
            if step >> 2 == z_step:
                qg_copy(step).start()

    for step in PARTNERS:
        kv_copy(step).start()
    transpose_values(2)
    transpose_values(3)
    for copy in [loads[6]] + loads[8:]:
        copy.wait()

    lane = lax.broadcasted_iota(jnp.int32, (HEAD, BLOCK), 1)
    second_head = ((lane >= PROP) & (lane < 2 * PROP)) | (lane >= 3 * PROP)
    for order, z_step in enumerate(Z_ORDER):
        arrived(qg.at[pl.ds((z ^ z_step) * 4, 4 if z_step else 3)], sems.at[QG_RECV + z_step])
        b = z ^ z_step
        begin = len_ref[b] + acc_ref[b] - me * POS
        visible = lax.broadcasted_iota(jnp.int32, (POS, BLOCK), 0) < begin
        visible = jnp.concatenate([visible, visible], axis=1)
        for half in range(2):
            for side in range(2):
                chunk = qg[b * 4 + half * 2 + side].astype(F32)
                lanes = slice(side * BLOCK, (side + 1) * BLOCK)
                qe[order, half, lanes, lanes] = _expanded(chunk)
        for half in range(2):
            keys = kbuf[b, :, half * 2 * BLOCK : (half + 1) * 2 * BLOCK]
            scores = _dot_nt(keys, qe[order, half]) * SCALE2
            scores = jnp.where(visible, scores, LOW)
            largest = jnp.max(scores, axis=0, keepdims=True)
            weight = jnp.exp2(scores - largest)
            weight_sum = jnp.sum(weight, axis=0, keepdims=True)
            weight = weight.astype(BF16)
            for side in range(2):
                block = half * 2 + side
                lanes = slice(side * BLOCK, (side + 1) * BLOCK)
                out = _dot(vt[b, block * BLOCK : (block + 1) * BLOCK, :], weight[:, lanes])
                owner = b * 4 + block
                dv[owner] = _packed(jnp.where(second_head, out[HEAD:], out[:HEAD])).astype(BF16)
                ds[owner] = jnp.concatenate([largest[:, lanes], weight_sum[:, lanes]], axis=0)
        for x_step in (2, 1, 3, 0):
            step = z_step << 2 | x_step
            if step:
                dv_copy(step).start()
                ds_copy(step).start()

    arrived(rkv.at[1:], sems.at[KV_RECV])
    summed = pkv[me].astype(F32)
    for step in range(1, KV):
        summed = summed + rkv[step].astype(F32)
    own_k = jnp.concatenate([summed[0:PROP] * factor, zero_tail], axis=0).astype(BF16)
    own_v = jnp.concatenate([summed[PROP:] * factor, zero_tail], axis=0)
    kvg[me] = jnp.concatenate([summed[0:PROP] * factor, summed[PROP:] * factor], axis=0).astype(BF16)
    par_pad[...] = jnp.full((8, BLOCK), -1, jnp.int32)
    par_pad[0:SEQS, 0:PROP] = par_ref[...]
    parent_row = par_pad[pl.ds(z, 1), :]
    row_index = lax.broadcasted_iota(jnp.int32, (BLOCK, BLOCK), 0)
    lane_index = lax.broadcasted_iota(jnp.int32, (BLOCK, BLOCK), 1)
    reach = ((parent_row == row_index) & (lane_index < PROP)) | (row_index == lane_index)
    reach = jnp.where(reach, 1.0, 0.0).astype(BF16)
    for _ in range(5):
        reach = jnp.minimum(_dot(reach, reach), 1.0).astype(BF16)
    spread = (lax.rem(lane_index, PROP) == row_index) & (lane_index < 4 * PROP) & (row_index < PROP)
    lineage = _dot(reach, jnp.where(spread, 1.0, 0.0).astype(BF16))[0:PAD]
    linked = (lineage > 0.5) & (lax.broadcasted_iota(jnp.int32, (PAD, BLOCK), 0) < PROP)
    own_expanded = _expanded(qg[me].astype(F32))
    self_scores = _dot_nt(own_k, own_expanded) * SCALE2
    self_scores = jnp.where(linked, self_scores, LOW)
    self_max = jnp.max(self_scores, axis=0, keepdims=True)
    self_weight = jnp.where(linked, jnp.exp2(self_scores - self_max), 0.0)
    self_total = jnp.sum(self_weight, axis=0, keepdims=True)
    values_t = jnp.transpose(own_v).astype(BF16)
    self_out = _dot(values_t, self_weight.astype(BF16))
    self_sum = jnp.where(second_head, self_out[HEAD:], self_out[:HEAD])

    arrived(rds.at[1:], sems.at[DS_RECV])
    maxima = jnp.concatenate([ds[me, 0:1]] + [rds[step, 0:1] for step in range(1, KV)], axis=0)
    totals = jnp.concatenate([ds[me, 1:2]] + [rds[step, 1:2] for step in range(1, KV)], axis=0)
    top = jnp.maximum(jnp.max(maxima, axis=0, keepdims=True), self_max)
    self_factor = jnp.exp2(self_max - top)
    factors = jnp.exp2(maxima - top)
    denominator = self_total * self_factor + jnp.sum(totals * factors, axis=0, keepdims=True)
    used = lax.broadcasted_iota(jnp.int32, (KV, BLOCK), 1) < 96
    factors = [jnp.where(used, factors, pltpu.roll(factors, 96 - 32 * third, 1)) for third in range(3)]
    arrived(rdv.at[1:], sems.at[DV_RECV])
    merged = [dv[me, 16 * third : 16 * third + 16].astype(F32) * factors[third][0:1] for third in range(3)]
    for step in range(1, KV):
        for third in range(3):
            block = rdv[step, 16 * third : 16 * third + 16].astype(F32)
            merged[third] = merged[third] + block * factors[third][step : step + 1]
    merged = _unpacked(jnp.concatenate(merged, axis=0)) + self_sum * self_factor
    attended = merged / denominator
    lane_row = lax.broadcasted_iota(jnp.int32, (1, BLOCK), 1)
    lam = jnp.where(lane_row < PROP, lam_ref[x * 2], lam_ref[x * 2 + 1])
    difference = attended - lam * pltpu.roll(attended, BLOCK - 2 * PROP, 1)
    power = jnp.mean(difference * difference, axis=0, keepdims=True)
    normed = difference * lax.rsqrt(power + EPS)
    stacked = jnp.concatenate([normed, pltpu.roll(normed, BLOCK - PROP, 1)], axis=0)
    turned = jnp.transpose(stacked)[0:PROP]
    turned = turned * og_ref[pl.ds(x, 1), :]
    ng[me] = turned.astype(BF16)
    for step in PARTNERS:
        ng_copy(step).start()
    for step in PARTNERS:
        kvg_copy(step).start()

    loads[7].wait()
    for z_step in Z_OUT:
        arrived(ng.at[pl.ds((z ^ z_step) * 4, 4 if z_step else 3)], sems.at[NG_RECV + z_step])
        b = z ^ z_step
        rows = jnp.concatenate([ng[b * 4 + block] for block in range(4)], axis=1)
        part[b] = _dot(rows, wo[...]).astype(BF16)
        for step in TP_ORDER:
            mx_copy(z_step, step).start()

    arrived(kvg.at[1:], sems.at[KVG_RECV])
    for b in range(SEQS):
        begin = len_ref[b] + acc_ref[b] - me * POS
        position = lax.broadcasted_iota(jnp.int32, (POS, BLOCK), 0) - begin
        written = (position >= 0) & (position < PROP)
        slot = lax.broadcasted_iota(jnp.int32, (POS, BLOCK), 1)
        for which, buf in enumerate((kbuf, vbuf)):
            offset = which * PROP
            placing = jnp.where(written & (position + offset == slot), 1.0, 0.0).astype(BF16)[:, 0 : 2 * PROP]
            for block in range(4):
                lanes = slice(block * BLOCK, (block + 1) * BLOCK)
                moved = _dot(placing, kvg[b * 4 + block])
                buf[b, :, lanes] = jnp.where(written, moved, buf[b, :, lanes].astype(F32)).astype(BF16)
            out_copy(which, b).start()

    for z_step in Z_OUT:
        arrived(rpart.at[z_step, 1:], sems.at[MX_RECV + z_step])
        b = z ^ z_step
        mixed = part[b].astype(F32)
        for step in range(1, TP):
            mixed = mixed + rpart[z_step, step].astype(F32)
        mixed_ref[b] = mixed.astype(BF16)

    arrived(kbuf, out_sem.at[0])
    arrived(vbuf, out_sem.at[1])
    for ref, index in (
        (pq, Q_SEND),
        (pkv, KV_SEND),
        (qg, QG_SEND),
        (kvg, KVG_SEND),
        (dv, DV_SEND),
        (ds, DS_SEND),
        (ng, NG_SEND),
    ):
        arrived(ref.at[1:], sems.at[index])
    arrived(rpart.at[:, 1:], sems.at[MX_SEND])


def _main(*arrays):
    hbm = pl.BlockSpec(memory_space=pltpu.HBM)
    vmem = pl.BlockSpec(memory_space=pltpu.VMEM)
    dma = pltpu.SemaphoreType.DMA
    return pl.pallas_call(
        _main_kernel,
        out_shape=(
            jax.ShapeDtypeStruct((SEQS, PROP, 256), BF16),
            jax.ShapeDtypeStruct((SEQS, POS, 512), BF16),
            jax.ShapeDtypeStruct((SEQS, POS, 512), BF16),
        ),
        in_specs=[hbm] * 13,
        out_specs=(vmem, pl.BlockSpec(memory_space=pl.ANY), pl.BlockSpec(memory_space=pl.ANY)),
        scratch_shapes=[
            pltpu.VMEM((SEQS, POS, 512), BF16),
            pltpu.VMEM((SEQS, POS, 512), BF16),
            pltpu.VMEM((ROWS, 256), BF16),
            pltpu.VMEM((1, 256), F32),
            pltpu.VMEM((4, BLOCK), F32),
            pltpu.VMEM((SEQS, PROP), jnp.int32),
            pltpu.SMEM((TP,), F32),
            pltpu.SMEM((SEQS,), jnp.int32),
            pltpu.SMEM((SEQS,), jnp.int32),
            pltpu.VMEM((3, 256, 512), BF16),
            pltpu.VMEM((512, 256), BF16),
            pltpu.VMEM((SEQS, 512, POS), BF16),
            pltpu.VMEM((KV, PAD, BLOCK), BF16),
            pltpu.VMEM((KV, PAD, BLOCK), BF16),
            pltpu.VMEM((KV, 2 * PROP, BLOCK), BF16),
            pltpu.VMEM((KV, 2 * PROP, BLOCK), BF16),
            pltpu.VMEM((KV, PROP, BLOCK), BF16),
            pltpu.VMEM((KV, 2 * PROP, BLOCK), BF16),
            pltpu.VMEM((KV, 48, BLOCK), BF16),
            pltpu.VMEM((KV, 48, BLOCK), BF16),
            pltpu.VMEM((KV, 2, BLOCK), F32),
            pltpu.VMEM((KV, 2, BLOCK), F32),
            pltpu.VMEM((KV, PROP, BLOCK), BF16),
            pltpu.VMEM((SEQS, PROP, 256), BF16),
            pltpu.VMEM((SEQS, TP, PROP, 256), BF16),
            pltpu.VMEM((8, BLOCK), jnp.int32),
            pltpu.VMEM((SEQS, 2, 2 * BLOCK, 2 * BLOCK), BF16),
            dma((13,)),
            dma((SEMAPHORES,)),
            dma((2,)),
        ],
        compiler_params=pltpu.CompilerParams(
            collective_id=0, has_side_effects=True, vmem_limit_bytes=MAIN_VMEM
        ),
        name="attention",
    )(*(pltpu.with_memory_space_constraint(array, pltpu.HBM) for array in arrays))


def _write_kernel(mixed_ref, keys_ref, values_ref, mixed_hbm, keys_hbm, values_hbm, sem):
    copies = [
        pltpu.make_async_copy(keys_ref, keys_hbm, sem.at[0]),
        pltpu.make_async_copy(values_ref, values_hbm, sem.at[1]),
        pltpu.make_async_copy(mixed_ref, mixed_hbm, sem.at[2]),
    ]
    for copy in copies:
        copy.start()
    for copy in copies:
        copy.wait()


def _write(*arrays):
    hbm = pl.BlockSpec(memory_space=pltpu.HBM)
    return pl.pallas_call(
        _write_kernel,
        out_shape=tuple(jax.ShapeDtypeStruct(array.shape, array.dtype) for array in arrays),
        in_specs=[pl.BlockSpec(memory_space=pl.ANY)] * 3,
        out_specs=(hbm,) * 3,
        scratch_shapes=[pltpu.SemaphoreType.DMA((3,))],
        compiler_params=pltpu.CompilerParams(vmem_limit_bytes=WRITE_VMEM),
        name="write",
    )(*arrays)


def _local(
    tokens,
    norm_gain,
    w_query,
    w_key,
    w_value,
    w_output,
    cache_keys,
    cache_values,
    map_lambda,
    out_gain,
    parents,
    lengths,
    accepted,
):
    mixed, keys, values = _main(
        tokens,
        norm_gain.reshape(1, 256),
        w_query,
        w_key,
        w_value,
        w_output,
        cache_keys,
        cache_values,
        map_lambda,
        out_gain.reshape(4, BLOCK),
        parents,
        lengths,
        accepted,
    )
    mixed, new_keys, new_values = _write(mixed, keys, values)
    return mixed.reshape(ROWS, 256), new_keys, new_values


def solution(mesh):
    return jax.shard_map(
        _local,
        mesh=mesh,
        in_specs=(
            P(None, "kv"),
            P("kv"),
            P("kv", "tp"),
            P("kv", "tp"),
            P("kv", "tp"),
            P("tp", "kv"),
            P(None, "kv", "tp"),
            P(None, "kv", "tp"),
            P("tp"),
            P("tp"),
            P(),
            P(),
            P(),
        ),
        out_specs=(P(None, "kv"), P(None, "kv", "tp"), P(None, "kv", "tp")),
        check_vma=False,
    )
```

time: 42.2 us -> 38.6 us (0.915)
  Pallas kernels: 41.5 us -> 37.9 us
    pallas_call x1, Pallas kernels: 39.4 us -> 35.9 us  [_main(): pl.pallas_call(_main_kernel, out_shape=(jax.ShapeDtypeStruct((SEQS, PROP,...]
where the time goes in v3:
time: 38.6 us; the launch traced here: 38.5 us
  Pallas kernels  37.9 us (98%)
  between operations  0.64 us (2%)
    pallas_call x1, Pallas kernels, _main(): pl.pallas_call(_main_kernel, out_shape=(jax.ShapeDtypeStruct((SEQS, PROP,...  35.9 us
    pallas_call x1, Pallas kernels, _write(): pl.pallas_call(_write_kernel, out_shape=tuple((jax.ShapeDtypeStruct(array...  2.04 us

profile of v3, /device:TPU:1, one launch (start us, length us, event | category | flops | bytes accessed | tf_op | source)
XLA Modules:
  0.0 38.5 jit_solution(6103161010751634305)
XLA Ops:
  0.6 35.9 %attention.1 = (bf16[4,24,256]{2,1,0:T(8,128)(2,1)S(1)}, bf16[4,512,512]{2,1,0:T(8,128)(2,1)S(1)}, bf16[4,512,512]{2,1,0:T(8,128)(2,1)S(1)}) custom-call(bf16[96,256]{1,0:T(8,128)(2,1)} %tok_hbm.1, f32[1,256]{1,0:T(1,128)} %bitcast.4, bf16[256,512]{1,0:T(8,128)(2,1)} %wq_hbm.1, bf16[256,512]{1,0:T(8,128)(2,1)} %wk_hbm.1, bf16[256,512]{1,0:T(8,128)(2,1)} %wv_hbm.1, ...), custom_call_target="tpu_custom_call" | custom-call | tf_op jit(solution)/shard_map/attention/pallas_call | solution.py:442
  36.5 2.0 %write.1 = (bf16[4,24,256]{2,1,0:T(8,128)(2,1)}, bf16[4,512,512]{2,1,0:T(8,128)(2,1)}, bf16[4,512,512]{2,1,0:T(8,128)(2,1)}) custom-call(bf16[4,24,256]{2,1,0:T(8,128)(2,1)S(1)} %get-tuple-element.9.mixed_ref, bf16[4,512,512]{2,1,0:T(8,128)(2,1)S(1)} %get-tuple-element.10.keys_ref, bf16[4,512,512]{2,1,0:T(8,128)(2,1)S(1)} %get-tuple-element.11.values_ref), custom_call_target="tpu_custom_call" | custom-call | tf_op jit(solution)/shard_map/write/pallas_call | solution.py:504

commit v4 on v3

v4 whole, which is shorter than its diff:
```python
import functools

import jax
import jax.numpy as jnp
from jax import lax
from jax.experimental import pallas as pl
from jax.experimental.pallas import tpu as pltpu
from jax.sharding import PartitionSpec as P

D = 4096
HEAD = 64
QK = 32
SEQS = 4
PROP = 24
KV = 16
TP = 8
BLOCK = 128
PAD = 32
POS = 512
ROWS = 96
EPS = 1e-05
LOW = -1e30
LOG2E = 1.4426950408889634
WRITE_VMEM = 16 * 1024 * 1024
MAIN_VMEM = 40 * 1024 * 1024
SCALE2 = QK ** (-0.5) * LOG2E
F32 = jnp.float32
BF16 = jnp.bfloat16
NT = (((1,), (1,)), ((), ()))


def _distance(step):
    ring = (0, 1, 2, 1)
    return ring[step >> 2] + ring[step & 3]


LOADS = 13
Q_SEND = 0
KV_SEND = 1
QG_SEND = 2
KVG_SEND = 4
DV_SEND = 6
DS_SEND = 7
NG_SEND = 8
MX_SEND = 9
GIVE_SEND = 10
Q_RECV = 13
KV_RECV = 15
DV_RECV = 17
DS_RECV = 19
QG_RECV = 21
KVG_RECV = 25
NG_RECV = 26
MX_RECV = 30
GIVE_RECV = 34
SEMAPHORES = 37
OUT = Q_RECV
Z_ORDER = (0, 1, 2, 3)
Z_OUT = (0, 1, 3, 2)
Z_SEND = (0, 2, 1, 3)
Z_GROUPS = ((0,), (1,), (2, 3))
Y_STEPS = (2, 1, 3)
PARTNERS = sorted(range(1, KV), key=lambda step: -_distance(step))


def _dot(a, b):
    return jnp.dot(a, b, preferred_element_type=F32)


def _dot_nt(a, b):
    return lax.dot_general(a, b, NT, preferred_element_type=F32)


def _split_rows(row):
    high = row.astype(BF16).astype(F32)
    middle = (row - high).astype(BF16).astype(F32)
    low = row - high - middle
    index = lax.broadcasted_iota(jnp.int32, (PAD - PROP, BLOCK), 0)
    return jnp.where(index == 0, high, jnp.where(index == 1, middle, jnp.where(index == 2, low, 0.0)))


def _packed(block):
    rest = block[48:]
    moved = jnp.concatenate([pltpu.roll(rest, 96 - 32 * part, 1) for part in range(3)], axis=0)
    return jnp.where(lax.broadcasted_iota(jnp.int32, (48, BLOCK), 1) < 96, block[:48], moved)


def _unpacked(packed):
    lane = lax.broadcasted_iota(jnp.int32, (16, BLOCK), 1)
    parts = [pltpu.roll(packed[16 * part : 16 * part + 16], 32 * part + 32, 1) for part in range(3)]
    rest = jnp.where(lane < 32, parts[0], jnp.where(lane < 64, parts[1], parts[2]))
    return jnp.concatenate([packed, rest], axis=0)


def _expanded(chunk):
    lane = lax.broadcasted_iota(jnp.int32, (PROP, BLOCK), 1)
    parts = []
    for which in range(2):
        for head in range(2):
            low = head * HEAD + which * QK
            inside = (lane >= low) & (lane < low + QK)
            parts.append(jnp.where(inside, chunk, 0.0))
    parts.append(jnp.zeros((BLOCK - 4 * PROP, BLOCK), F32))
    return jnp.concatenate(parts, axis=0).astype(BF16)


def _main_kernel(
    tok_hbm,
    gain_hbm,
    wq_hbm,
    wk_hbm,
    wv_hbm,
    wo_hbm,
    ck_hbm,
    cv_hbm,
    lam_hbm,
    og_hbm,
    par_hbm,
    len_hbm,
    acc_hbm,
    mixed_ref,
    keys_out,
    values_out,
    kbuf,
    vbuf,
    tok,
    gain_ref,
    og,
    par_ref,
    lam,
    len_ref,
    acc_ref,
    wqkv,
    wo,
    vt,
    pq,
    rq,
    pkv,
    rkv,
    oq,
    okv,
    qg,
    kvg,
    dv,
    rdv,
    ds,
    rds,
    ng,
    rpart,
    par_pad,
    qe,
    sc,
    sm,
    sems,
    ready,
    self_stats,
    self_sum,
):
    me = lax.axis_index("kv")
    tp = lax.axis_index("tp")
    z = me // 4
    x = lax.rem(me, 4)
    core = lax.rem(tp, 2)
    first = tp - core
    is_owner = core == 1
    is_other = core == 0

    def spot(kv_step, y_step, to):
        return {"kv": me ^ kv_step, "tp": (first ^ (2 * y_step)) + to}

    barrier = pltpu.get_barrier_semaphore()

    def greet(kv_step, y_step, to):
        pl.semaphore_signal(
            barrier, inc=1, device_id=spot(kv_step, y_step, to), device_id_type=pl.DeviceIdType.MESH
        )

    @pl.when(is_owner)
    def _():
        for step in PARTNERS:
            greet(step, 0, 1)
        for step in PARTNERS + [0]:
            greet(step, 0, 0)
        for step in Y_STEPS:
            greet(0, step, 1)
            greet(0, step, 0)


    loads = [
        (tok_hbm, tok),
        (gain_hbm, gain_ref),
        (wq_hbm, wqkv.at[0]),
        (wk_hbm, wqkv.at[1]),
        (wv_hbm, wqkv.at[2]),
        (cv_hbm, vbuf),
        (ck_hbm, kbuf),
        (wo_hbm, wo.at[core]),
        (og_hbm, og.at[core]),
        (lam_hbm, lam.at[core]),
        (par_hbm, par_ref),
        (len_hbm, len_ref),
        (acc_hbm, acc_ref),
    ]
    loads = [pltpu.make_async_copy(src, dst, sems.at[index]) for index, (src, dst) in enumerate(loads)]
    for copy in loads:
        copy.start()

    def arrived(ref, index):
        pltpu.make_async_copy(ref, ref, sems.at[index]).wait()

    def remote(src, dst, send, recv, where):
        return pltpu.make_async_remote_copy(
            src_ref=src,
            dst_ref=dst,
            send_sem=sems.at[send],
            recv_sem=sems.at[recv],
            device_id=where,
            device_id_type=pl.DeviceIdType.MESH,
        )

    def send_q(step):
        remote(pq.at[me ^ step], rq.at[core, step], Q_SEND, Q_RECV + core, spot(step, 0, 1)).start()

    def send_kv(step):
        remote(pkv.at[me ^ step], rkv.at[core, step], KV_SEND, KV_RECV + core, spot(step, 0, 1)).start()

    def send_d(step):
        remote(ds.at[me ^ step], rds.at[core, step], DS_SEND, DS_RECV + core, spot(step, 0, 1)).start()
        remote(dv.at[me ^ step], rdv.at[core, step], DV_SEND, DV_RECV + core, spot(step, 0, 1)).start()

    def send_qg(step, to):
        src = qg.at[me] if to else oq
        remote(src, qg.at[me], QG_SEND + to, QG_RECV + (step >> 2), spot(step, 0, to)).start()

    def send_kvg(step, to):
        src = kvg.at[me] if to else okv
        remote(src, kvg.at[me], KVG_SEND + to, KVG_RECV, spot(step, 0, to)).start()

    def send_ng(step):
        remote(ng.at[me], ng.at[me], NG_SEND, NG_RECV + (step >> 2), spot(step, 0, 1)).start()

    def send_mx(z_step, y_step, to):
        src = rpart.at[z_step, 0]
        dst = rpart.at[z_step, y_step]
        remote(src, dst, MX_SEND, MX_RECV + z_step, spot(0, y_step, to)).start()

    def out_copy(which, b):
        buf, out = ((kbuf, keys_out), (vbuf, values_out))[which]
        return pltpu.make_async_copy(buf.at[b], out.at[b], sems.at[OUT + which])

    loads[0].wait()
    loads[1].wait()
    wide = tok[...].astype(F32)
    gained = (wide * gain_ref[...]).astype(BF16)
    square = jnp.sum(wide * wide, axis=1, keepdims=True)
    eye = lax.broadcasted_iota(jnp.int32, (PROP, BLOCK), 0) == lax.broadcasted_iota(jnp.int32, (PROP, BLOCK), 1)
    loads[2].wait()
    partial_q = _dot(gained, wqkv[0])
    for b in range(SEQS):
        column = square[b * PROP : (b + 1) * PROP]
        row = jnp.sum(jnp.where(eye, column, 0.0), axis=0, keepdims=True)
        tail = _split_rows(row)
        for block in range(4):
            chunk = partial_q[b * PROP : (b + 1) * PROP, block * BLOCK : (block + 1) * BLOCK]
            pq[b * 4 + block] = jnp.concatenate([chunk, tail], axis=0).astype(BF16)

    @pl.when(is_owner)
    def _():
        pl.semaphore_wait(barrier, KV - 1 + 3)

    @pl.when(is_other)
    def _():
        pl.semaphore_wait(barrier, KV + 3)

    for step in PARTNERS:
        send_q(step)

    @pl.when(is_other)
    def _():
        send_q(0)

        def tell(kv_step, y_step):
            pl.semaphore_signal(
                ready, inc=1, device_id=spot(kv_step, y_step, 1), device_id_type=pl.DeviceIdType.MESH
            )

        for step in PARTNERS + [0]:
            tell(step, 0)
        for step in Y_STEPS:
            tell(0, step)

    projected = []
    for which in range(2):
        loads[3 + which].wait()
        projected.append(_dot(gained, wqkv[1 + which]))
    for b in range(SEQS):
        for block in range(4):
            pkv[b * 4 + block] = jnp.concatenate(
                [
                    part_kv[b * PROP : (b + 1) * PROP, block * BLOCK : (block + 1) * BLOCK]
                    for part_kv in projected
                ],
                axis=0,
            ).astype(BF16)
    loads[5].wait()

    def transpose_values(b):
        for block in range(4):
            vt[b, block * BLOCK : (block + 1) * BLOCK, :] = jnp.transpose(
                vbuf[b, :, block * BLOCK : (block + 1) * BLOCK]
            )

    for order in range(SEQS):
        for half in range(2):
            for side in range(2):
                qe[order, half, side * BLOCK : (side + 1) * BLOCK, (1 - side) * BLOCK : (2 - side) * BLOCK] = (
                    jnp.zeros((BLOCK, BLOCK), BF16)
                )
    for b in range(SEQS):
        transpose_values(b)
    for step in PARTNERS:
        send_kv(step)

    @pl.when(is_other)
    def _():
        send_kv(0)

    for index in (6, 7, 8, 9, 10, 11, 12):
        loads[index].wait()

    zero_tail = jnp.zeros((PAD - PROP, BLOCK), F32)
    lane = lax.broadcasted_iota(jnp.int32, (HEAD, BLOCK), 1)
    second_head = ((lane >= PROP) & (lane < 2 * PROP)) | (lane >= 3 * PROP)

    @pl.when(is_owner)
    def _():
        arrived(rq.at[1, 1:], Q_RECV + 1)
        arrived(rq.at[0], Q_RECV)
        factors = []
        for group in range(2):
            total = (pq[me] if group else rq[0, 0]).astype(F32)
            for step in range(1, KV):
                total = total + rq[group, step].astype(F32)
            square_row = jnp.sum(total[PROP:PAD], axis=0, keepdims=True)
            square_column = jnp.sum(jnp.where(eye, square_row, 0.0), axis=1, keepdims=True)
            factors.append(lax.rsqrt(square_column / D + EPS))
            own_q = (total[0:PROP] * factors[group]).astype(BF16)
            if group:
                qg[me] = own_q
            else:
                oq[...] = own_q
        pl.semaphore_wait(ready, KV + 3)
        for z_step in Z_SEND:
            for step in PARTNERS + [0]:
                if step >> 2 == z_step:
                    send_qg(step, 0)
                    if step:
                        send_qg(step, 1)
        arrived(rkv.at[1, 1:], KV_RECV + 1)
        arrived(rkv.at[0], KV_RECV)
        for group in range(2):
            summed = (pkv[me] if group else rkv[0, 0]).astype(F32)
            for step in range(1, KV):
                summed = summed + rkv[group, step].astype(F32)
            rows = [summed[0:PROP] * factors[group], summed[PROP:] * factors[group]]
            rows = jnp.concatenate(rows, axis=0).astype(BF16)
            if group:
                kvg[me] = rows
            else:
                okv[...] = rows
        for step in PARTNERS + [0]:
            send_kvg(step, 0)
        for step in PARTNERS:
            send_kvg(step, 1)
        par_pad[...] = jnp.full((8, BLOCK), -1, jnp.int32)
        par_pad[0:SEQS, 0:PROP] = par_ref[...]
        parent_row = par_pad[pl.ds(z, 1), :]
        row_index = lax.broadcasted_iota(jnp.int32, (BLOCK, BLOCK), 0)
        lane_index = lax.broadcasted_iota(jnp.int32, (BLOCK, BLOCK), 1)
        reach = ((parent_row == row_index) & (lane_index < PROP)) | (row_index == lane_index)
        reach = jnp.where(reach, 1.0, 0.0).astype(BF16)
        for _ in range(5):
            reach = jnp.minimum(_dot(reach, reach), 1.0).astype(BF16)
        spread = (lax.rem(lane_index, PROP) == row_index) & (lane_index < 4 * PROP) & (row_index < PROP)
        lineage = _dot(reach, jnp.where(spread, 1.0, 0.0).astype(BF16))[0:PAD]
        linked = (lineage > 0.5) & (lax.broadcasted_iota(jnp.int32, (PAD, BLOCK), 0) < PROP)
        for group in range(2):
            own_expanded = _expanded((qg[me] if group else oq[...]).astype(F32))
            own_kv = (kvg[me] if group else okv[...]).astype(F32)
            own_k = jnp.concatenate([own_kv[0:PROP], zero_tail], axis=0).astype(BF16)
            own_v = jnp.concatenate([own_kv[PROP:], zero_tail], axis=0)
            self_scores = _dot_nt(own_k, own_expanded) * SCALE2
            self_scores = jnp.where(linked, self_scores, LOW)
            largest = jnp.max(self_scores, axis=0, keepdims=True)
            self_weight = jnp.where(linked, jnp.exp2(self_scores - largest), 0.0)
            self_stats[group, 0:1] = largest
            self_stats[group, 1:2] = jnp.sum(self_weight, axis=0, keepdims=True)
            self_out = _dot(jnp.transpose(own_v).astype(BF16), self_weight.astype(BF16))
            self_sum[group] = jnp.where(second_head, self_out[HEAD:], self_out[:HEAD])

    @pl.when(is_other)
    def _():
        remote(wo.at[0], wo.at[0], GIVE_SEND, GIVE_RECV, spot(0, 0, 1)).start()
        remote(og.at[0], og.at[0], GIVE_SEND + 1, GIVE_RECV + 1, spot(0, 0, 1)).start()
        remote(lam.at[0], lam.at[0], GIVE_SEND + 2, GIVE_RECV + 2, spot(0, 0, 1)).start()


    def gathered(z_step):
        if z_step:
            arrived(qg.at[pl.ds((z ^ z_step) * 4, 4)], QG_RECV + z_step)
            return

        @pl.when(is_owner)
        def _():
            arrived(qg.at[0:3], QG_RECV)

        @pl.when(is_other)
        def _():
            arrived(qg.at[0:4], QG_RECV)

    def expand(order):
        b = z ^ Z_ORDER[order]
        for half in range(2):
            for side in range(2):
                chunk = qg[b * 4 + half * 2 + side].astype(F32)
                lanes = slice(side * BLOCK, (side + 1) * BLOCK)
                qe[order, half, lanes, lanes] = _expanded(chunk)

    def score(order):
        b = z ^ Z_ORDER[order]
        begin = len_ref[b] + acc_ref[b] - me * POS
        visible = lax.broadcasted_iota(jnp.int32, (POS, BLOCK), 0) < begin
        visible = jnp.concatenate([visible, visible], axis=1)
        for half in range(2):
            keys = kbuf[b, :, half * 2 * BLOCK : (half + 1) * 2 * BLOCK]
            scores = jnp.where(visible, _dot_nt(keys, qe[order, half]) * SCALE2, LOW)
            sc[order % 2, half] = scores
            sm[order % 2, half] = jnp.max(scores, axis=0, keepdims=True)

    def weigh(order):
        b = z ^ Z_ORDER[order]
        for half in range(2):
            largest = sm[order % 2, half]
            weight = jnp.exp2(sc[order % 2, half] - largest)
            weight_sum = jnp.sum(weight, axis=0, keepdims=True)
            weight = weight.astype(BF16)
            for side in range(2):
                block = half * 2 + side
                lanes = slice(side * BLOCK, (side + 1) * BLOCK)
                out = _dot(vt[b, block * BLOCK : (block + 1) * BLOCK, :], weight[:, lanes])
                owner = b * 4 + block
                dv[owner] = _packed(jnp.where(second_head, out[HEAD:], out[:HEAD])).astype(BF16)
                ds[owner] = jnp.concatenate([largest[:, lanes], weight_sum[:, lanes]], axis=0)

    def send(order):
        for x_step in (2, 1, 3, 0):
            step = Z_ORDER[order] << 2 | x_step
            if step:
                send_d(step)
        if Z_ORDER[order] == 0:

            @pl.when(is_other)
            def _():
                send_d(0)

    for group in Z_GROUPS:
        for order in group:
            gathered(Z_ORDER[order])
        for order in group:
            expand(order)
        score(group[0])
        for order in group:
            if order + 1 in group:
                score(order + 1)
            weigh(order)
            send(order)

    @pl.when(is_owner)
    def _():
        arrived(kvg.at[1:], KVG_RECV)

    @pl.when(is_other)
    def _():
        arrived(kvg, KVG_RECV)

    for b in range(SEQS):
        begin = len_ref[b] + acc_ref[b] - me * POS
        position = lax.broadcasted_iota(jnp.int32, (POS, BLOCK), 0) - begin
        written = (position >= 0) & (position < PROP)
        slot = lax.broadcasted_iota(jnp.int32, (POS, BLOCK), 1)
        for which, buf in enumerate((kbuf, vbuf)):
            offset = which * PROP
            placing = jnp.where(written & (position + offset == slot), 1.0, 0.0).astype(BF16)[:, 0 : 2 * PROP]
            for block in range(4):
                lanes = slice(block * BLOCK, (block + 1) * BLOCK)
                moved = _dot(placing, kvg[b * 4 + block])
                buf[b, :, lanes] = jnp.where(written, moved, buf[b, :, lanes].astype(F32)).astype(BF16)
            out_copy(which, b).start()

    @pl.when(is_owner)
    def _():
        lane_row = lax.broadcasted_iota(jnp.int32, (1, BLOCK), 1)
        arrived(og.at[0], GIVE_RECV + 1)
        arrived(lam.at[0], GIVE_RECV + 2)
        arrived(wo.at[0], GIVE_RECV)
        lam_rows = []
        for group in range(2):
            index = lax.broadcasted_iota(jnp.int32, (1, TP), 1)
            pair = [
                jnp.sum(jnp.where(index == x * 2 + head, lam[group], 0.0), axis=1, keepdims=True)
                for head in range(2)
            ]
            lam_rows.append(jnp.where(lane_row < PROP, pair[0], pair[1]))

        arrived(rds.at[1, 1:], DS_RECV + 1)
        arrived(rds.at[0], DS_RECV)
        denominator = []
        self_factor = []
        factors = []
        used = lax.broadcasted_iota(jnp.int32, (KV, BLOCK), 1) < 96
        for group in range(2):
            slots = [ds.at[me] if group else rds.at[0, 0]] + [rds.at[group, step] for step in range(1, KV)]
            maxima = jnp.concatenate([slot[0:1] for slot in slots], axis=0)
            totals = jnp.concatenate([slot[1:2] for slot in slots], axis=0)
            top = jnp.maximum(jnp.max(maxima, axis=0, keepdims=True), self_stats[group, 0:1])
            self_factor.append(jnp.exp2(self_stats[group, 0:1] - top))
            factor = jnp.exp2(maxima - top)
            denominator.append(
                self_stats[group, 1:2] * self_factor[group] + jnp.sum(totals * factor, axis=0, keepdims=True)
            )
            factors.append(
                [jnp.where(used, factor, pltpu.roll(factor, 96 - 32 * third, 1)) for third in range(3)]
            )
        arrived(rdv.at[1, 1:], DV_RECV + 1)
        arrived(rdv.at[0], DV_RECV)
        for group in range(2):
            slots = [dv.at[me] if group else rdv.at[0, 0]] + [rdv.at[group, step] for step in range(1, KV)]
            merged = []
            for third in range(3):
                rows = slice(16 * third, 16 * third + 16)
                sums = [
                    slot[rows].astype(F32) * factors[group][third][step : step + 1]
                    for step, slot in enumerate(slots)
                ]
                while len(sums) > 1:
                    sums = [a + b for a, b in zip(sums[::2], sums[1::2])]
                merged.append(sums[0])
            merged = _unpacked(jnp.concatenate(merged, axis=0)) + self_sum[group] * self_factor[group]
            attended = merged / denominator[group]
            difference = attended - lam_rows[group] * pltpu.roll(attended, BLOCK - 2 * PROP, 1)
            power = jnp.mean(difference * difference, axis=0, keepdims=True)
            normed = difference * lax.rsqrt(power + EPS)
            stacked = jnp.concatenate([normed, pltpu.roll(normed, BLOCK - PROP, 1)], axis=0)
            turned = jnp.transpose(stacked)[0:PROP]
            turned = turned * og[group, pl.ds(x, 1), :]
            ng[me, group] = turned.astype(BF16)
        for step in PARTNERS:
            send_ng(step)

        for z_step in Z_OUT:
            arrived(ng.at[pl.ds((z ^ z_step) * 4, 4 if z_step else 3)], NG_RECV + z_step)
            b = z ^ z_step
            projected = 0.0
            for group in range(2):
                rows = jnp.concatenate([ng[b * 4 + block, group] for block in range(4)], axis=1)
                projected = projected + _dot(rows, wo[group])
            rpart[z_step, 0] = projected.astype(BF16)
            for step in Y_STEPS:
                send_mx(z_step, step, 0)
            for step in Y_STEPS:
                send_mx(z_step, step, 1)
            send_mx(z_step, 0, 0)

    for z_step in Z_OUT:

        @pl.when(is_owner)
        def _(z_step=z_step):
            arrived(rpart.at[z_step, 1:], MX_RECV + z_step)

        @pl.when(is_other)
        def _(z_step=z_step):
            arrived(rpart.at[z_step], MX_RECV + z_step)

        mixed = rpart[z_step, 0].astype(F32)
        for step in range(1, 4):
            mixed = mixed + rpart[z_step, step].astype(F32)
        mixed_ref[z ^ z_step] = mixed.astype(BF16)

    arrived(kbuf, OUT)
    arrived(vbuf, OUT + 1)
    sent = ((pq, Q_SEND), (pkv, KV_SEND), (dv, DV_SEND), (ds, DS_SEND))

    @pl.when(is_owner)
    def _():
        for ref, index in sent + ((qg, QG_SEND + 1), (kvg, KVG_SEND + 1), (ng, NG_SEND)):
            arrived(ref.at[1:], index)
        arrived(qg, QG_SEND)
        arrived(kvg, KVG_SEND)
        arrived(rpart.at[0:7], MX_SEND)

    @pl.when(is_other)
    def _():
        for ref, index in sent:
            arrived(ref, index)
        arrived(wo.at[0], GIVE_SEND)
        arrived(og.at[0], GIVE_SEND + 1)
        arrived(lam.at[0], GIVE_SEND + 2)


def _main(*arrays):
    hbm = pl.BlockSpec(memory_space=pltpu.HBM)
    vmem = pl.BlockSpec(memory_space=pltpu.VMEM)
    dma = pltpu.SemaphoreType.DMA
    return pl.pallas_call(
        _main_kernel,
        out_shape=(
            jax.ShapeDtypeStruct((SEQS, PROP, 256), BF16),
            jax.ShapeDtypeStruct((SEQS, POS, 512), BF16),
            jax.ShapeDtypeStruct((SEQS, POS, 512), BF16),
        ),
        in_specs=[hbm] * 13,
        out_specs=(vmem, pl.BlockSpec(memory_space=pl.ANY), pl.BlockSpec(memory_space=pl.ANY)),
        scratch_shapes=[
            pltpu.VMEM((SEQS, POS, 512), BF16),
            pltpu.VMEM((SEQS, POS, 512), BF16),
            pltpu.VMEM((ROWS, 256), BF16),
            pltpu.VMEM((1, 256), F32),
            pltpu.VMEM((2, 4, BLOCK), F32),
            pltpu.VMEM((SEQS, PROP), jnp.int32),
            pltpu.VMEM((2, 1, TP), F32),
            pltpu.SMEM((SEQS,), jnp.int32),
            pltpu.SMEM((SEQS,), jnp.int32),
            pltpu.VMEM((3, 256, 512), BF16),
            pltpu.VMEM((2, 512, 256), BF16),
            pltpu.VMEM((SEQS, 512, POS), BF16),
            pltpu.VMEM((KV, PAD, BLOCK), BF16),
            pltpu.VMEM((2, KV, PAD, BLOCK), BF16),
            pltpu.VMEM((KV, 2 * PROP, BLOCK), BF16),
            pltpu.VMEM((2, KV, 2 * PROP, BLOCK), BF16),
            pltpu.VMEM((PROP, BLOCK), BF16),
            pltpu.VMEM((2 * PROP, BLOCK), BF16),
            pltpu.VMEM((KV, PROP, BLOCK), BF16),
            pltpu.VMEM((KV, 2 * PROP, BLOCK), BF16),
            pltpu.VMEM((KV, 48, BLOCK), BF16),
            pltpu.VMEM((2, KV, 48, BLOCK), BF16),
            pltpu.VMEM((KV, 2, BLOCK), F32),
            pltpu.VMEM((2, KV, 2, BLOCK), F32),
            pltpu.VMEM((KV, 2, PROP, BLOCK), BF16),
            pltpu.VMEM((8, 4, PROP, 256), BF16),
            pltpu.VMEM((8, BLOCK), jnp.int32),
            pltpu.VMEM((SEQS, 2, 2 * BLOCK, 2 * BLOCK), BF16),
            pltpu.VMEM((2, 2, POS, 2 * BLOCK), F32),
            pltpu.VMEM((2, 2, 1, 2 * BLOCK), F32),
            dma((SEMAPHORES,)),
            pltpu.SemaphoreType.REGULAR,
            pltpu.VMEM((2, 2, BLOCK), F32),
            pltpu.VMEM((2, HEAD, BLOCK), F32),
        ],
        compiler_params=pltpu.CompilerParams(
            collective_id=0, has_side_effects=True, vmem_limit_bytes=MAIN_VMEM
        ),
        name="attention",
    )(*(pltpu.with_memory_space_constraint(array, pltpu.HBM) for array in arrays))


def _write_kernel(mixed_ref, keys_ref, values_ref, mixed_hbm, keys_hbm, values_hbm, sem):
    copies = [
        pltpu.make_async_copy(keys_ref, keys_hbm, sem.at[0]),
        pltpu.make_async_copy(values_ref, values_hbm, sem.at[1]),
        pltpu.make_async_copy(mixed_ref, mixed_hbm, sem.at[2]),
    ]
    for copy in copies:
        copy.start()
    for copy in copies:
        copy.wait()


def _write(*arrays):
    hbm = pl.BlockSpec(memory_space=pltpu.HBM)
    return pl.pallas_call(
        _write_kernel,
        out_shape=tuple(jax.ShapeDtypeStruct(array.shape, array.dtype) for array in arrays),
        in_specs=[pl.BlockSpec(memory_space=pl.ANY)] * 3,
        out_specs=(hbm,) * 3,
        scratch_shapes=[pltpu.SemaphoreType.DMA((3,))],
        compiler_params=pltpu.CompilerParams(vmem_limit_bytes=WRITE_VMEM),
        name="write",
    )(*arrays)


def _local(
    tokens,
    norm_gain,
    w_query,
    w_key,
    w_value,
    w_output,
    cache_keys,
    cache_values,
    map_lambda,
    out_gain,
    parents,
    lengths,
    accepted,
):
    mixed, keys, values = _main(
        tokens,
        norm_gain.reshape(1, 256),
        w_query,
        w_key,
        w_value,
        w_output,
        cache_keys,
        cache_values,
        map_lambda.reshape(1, TP),
        out_gain.reshape(4, BLOCK),
        parents,
        lengths,
        accepted,
    )
    mixed, new_keys, new_values = _write(mixed, keys, values)
    return mixed.reshape(ROWS, 256), new_keys, new_values


def solution(mesh):
    return jax.shard_map(
        _local,
        mesh=mesh,
        in_specs=(
            P(None, "kv"),
            P("kv"),
            P("kv", "tp"),
            P("kv", "tp"),
            P("kv", "tp"),
            P("tp", "kv"),
            P(None, "kv", "tp"),
            P(None, "kv", "tp"),
            P("tp"),
            P("tp"),
            P(),
            P(),
            P(),
        ),
        out_specs=(P(None, "kv"), P(None, "kv", "tp"), P(None, "kv", "tp")),
        check_vma=False,
    )
```

time: 38.6 us -> 35.8 us (0.927)
  Pallas kernels: 37.9 us -> 35 us
    pallas_call x1, Pallas kernels: 35.9 us -> 33 us  [_main(): pl.pallas_call(_main_kernel, out_shape=(jax.ShapeDtypeStruct((SEQS, PROP,...]
where the time goes in v4:
time: 35.8 us; the launch traced here: 35.6 us
  Pallas kernels  35 us (98%)
  between operations  0.64 us (2%)
    pallas_call x1, Pallas kernels, _main(): pl.pallas_call(_main_kernel, out_shape=(jax.ShapeDtypeStruct((SEQS, PROP,...  33 us
    pallas_call x1, Pallas kernels, _write(): pl.pallas_call(_write_kernel, out_shape=tuple((jax.ShapeDtypeStruct(array...  2.04 us

profile of v4, /device:TPU:1, one launch (start us, length us, event | category | flops | bytes accessed | tf_op | source)
XLA Modules:
  0.0 35.6 jit_solution(18202944646496771541)
XLA Ops:
  0.6 33.0 %attention.1 = (bf16[4,24,256]{2,1,0:T(8,128)(2,1)S(1)}, bf16[4,512,512]{2,1,0:T(8,128)(2,1)S(1)}, bf16[4,512,512]{2,1,0:T(8,128)(2,1)S(1)}) custom-call(bf16[96,256]{1,0:T(8,128)(2,1)} %tok_hbm.1, f32[1,256]{1,0:T(1,128)} %bitcast.5, bf16[256,512]{1,0:T(8,128)(2,1)} %wq_hbm.1, bf16[256,512]{1,0:T(8,128)(2,1)} %wk_hbm.1, bf16[256,512]{1,0:T(8,128)(2,1)} %wv_hbm.1, ...), custom_call_target="tpu_custom_call" | custom-call | tf_op jit(solution)/shard_map/attention/pallas_call | solution.py:614
  33.6 2.0 %write.1 = (bf16[4,24,256]{2,1,0:T(8,128)(2,1)}, bf16[4,512,512]{2,1,0:T(8,128)(2,1)}, bf16[4,512,512]{2,1,0:T(8,128)(2,1)}) custom-call(bf16[4,24,256]{2,1,0:T(8,128)(2,1)S(1)} %get-tuple-element.9.mixed_ref, bf16[4,512,512]{2,1,0:T(8,128)(2,1)S(1)} %get-tuple-element.10.keys_ref, bf16[4,512,512]{2,1,0:T(8,128)(2,1)S(1)} %get-tuple-element.11.values_ref), custom_call_target="tpu_custom_call" | custom-call | tf_op jit(solution)/shard_map/write/pallas_call | solution.py:680

commit v5 on v4

--- a/solution.py
+++ b/solution.py
@@ -118,6 +118,7 @@
     par_hbm,
     len_hbm,
     acc_hbm,
+    _first_keys,
     mixed_ref,
     keys_out,
     values_out,
@@ -618,7 +619,7 @@
             jax.ShapeDtypeStruct((SEQS, POS, 512), BF16),
             jax.ShapeDtypeStruct((SEQS, POS, 512), BF16),
         ),
-        in_specs=[hbm] * 13,
+        in_specs=[hbm] * 14,
         out_specs=(vmem, pl.BlockSpec(memory_space=pl.ANY), pl.BlockSpec(memory_space=pl.ANY)),
         scratch_shapes=[
             pltpu.VMEM((SEQS, POS, 512), BF16),
@@ -663,25 +664,69 @@
     )(*(pltpu.with_memory_space_constraint(array, pltpu.HBM) for array in arrays))
 
 
-def _write_kernel(mixed_ref, keys_ref, values_ref, mixed_hbm, keys_hbm, values_hbm, sem):
-    copies = [
-        pltpu.make_async_copy(keys_ref, keys_hbm, sem.at[0]),
-        pltpu.make_async_copy(values_ref, values_hbm, sem.at[1]),
-        pltpu.make_async_copy(mixed_ref, mixed_hbm, sem.at[2]),
-    ]
-    for copy in copies:
-        copy.start()
-    for copy in copies:
-        copy.wait()
+def _copies_first():
+    return (lax.axis_index("kv") < 4) & (lax.axis_index("tp") // 2 * 4 + lax.axis_index("kv") < 5)
+
+
+def _copy_kernel(keys_in, values_in, keys_out, values_out, kbuf, vbuf, sem):
+    @pl.when(_copies_first())
+    def _():
+        pairs = ((keys_in, kbuf, keys_out), (values_in, vbuf, values_out))
+        fetches = [pltpu.make_async_copy(src, buf, sem.at[which]) for which, (src, buf, _) in enumerate(pairs)]
+        puts = [pltpu.make_async_copy(buf, dst, sem.at[which]) for which, (_, buf, dst) in enumerate(pairs)]
+        for copy in fetches:
+            copy.start()
+        for fetch, put in zip(fetches, puts):
+            fetch.wait()
+            put.start()
+        for copy in puts:
+            copy.wait()
+
+
+def _copy(*arrays):
+    hbm = pl.BlockSpec(memory_space=pltpu.HBM)
+    return pl.pallas_call(
+        _copy_kernel,
+        out_shape=tuple(jax.ShapeDtypeStruct(array.shape, array.dtype) for array in arrays),
+        in_specs=[hbm] * 2,
+        out_specs=(hbm,) * 2,
+        scratch_shapes=[
+            pltpu.VMEM((SEQS, POS, 512), BF16),
+            pltpu.VMEM((SEQS, POS, 512), BF16),
+            pltpu.SemaphoreType.DMA((2,)),
+        ],
+        compiler_params=pltpu.CompilerParams(vmem_limit_bytes=MAIN_VMEM),
+        name="copy_caches",
+    )(*(pltpu.with_memory_space_constraint(array, pltpu.HBM) for array in arrays))
+
+
+def _write_kernel(mixed_ref, keys_ref, values_ref, _keys, _values, mixed_hbm, keys_hbm, values_hbm, sem):
+    mixed_copy = pltpu.make_async_copy(mixed_ref, mixed_hbm, sem.at[2])
+    mixed_copy.start()
+
+    @pl.when(jnp.logical_not(_copies_first()))
+    def _():
+        copies = [
+            pltpu.make_async_copy(keys_ref, keys_hbm, sem.at[0]),
+            pltpu.make_async_copy(values_ref, values_hbm, sem.at[1]),
+        ]
+        for copy in copies:
+            copy.start()
+        for copy in copies:
+            copy.wait()
+
+    mixed_copy.wait()
 
 
 def _write(*arrays):
     hbm = pl.BlockSpec(memory_space=pltpu.HBM)
+    anywhere = pl.BlockSpec(memory_space=pl.ANY)
     return pl.pallas_call(
         _write_kernel,
-        out_shape=tuple(jax.ShapeDtypeStruct(array.shape, array.dtype) for array in arrays),
-        in_specs=[pl.BlockSpec(memory_space=pl.ANY)] * 3,
+        out_shape=tuple(jax.ShapeDtypeStruct(array.shape, array.dtype) for array in arrays[:3]),
+        in_specs=[anywhere] * 3 + [hbm] * 2,
         out_specs=(hbm,) * 3,
+        input_output_aliases={3: 1, 4: 2},
         scratch_shapes=[pltpu.SemaphoreType.DMA((3,))],
         compiler_params=pltpu.CompilerParams(vmem_limit_bytes=WRITE_VMEM),
         name="write",
@@ -703,6 +748,7 @@
     lengths,
     accepted,
 ):
+    first_keys, first_values = _copy(cache_keys, cache_values)
     mixed, keys, values = _main(
         tokens,
         norm_gain.reshape(1, 256),
@@ -717,8 +763,9 @@
         parents,
         lengths,
         accepted,
+        first_keys,
     )
-    mixed, new_keys, new_values = _write(mixed, keys, values)
+    mixed, new_keys, new_values = _write(mixed, keys, values, first_keys, first_values)
     return mixed.reshape(ROWS, 256), new_keys, new_values
 
 

time: 35.8 us -> 34.4 us (0.961)
  Pallas kernels: 35 us -> 33.7 us
    pallas_call x0 -> x1, Pallas kernels: none -> 3.63 us  [_copy(): pl.pallas_call(_copy_kernel, out_shape=tuple((jax.ShapeDtypeStruct(array....]
    pallas_call x1, Pallas kernels: 33 us -> 29.4 us  [_main(): pl.pallas_call(_main_kernel, out_shape=(jax.ShapeDtypeStruct((SEQS, PROP,...]
    pallas_call x1, Pallas kernels: 2.04 us -> 0.65 us  [_write(): pl.pallas_call(_write_kernel, out_shape=tuple((jax.ShapeDtypeStruct(array...]
where the time goes in v5:
time: 34.4 us; the launch traced here: 34.3 us
  Pallas kernels  33.7 us (98%)
  between operations  0.65 us (2%)
    pallas_call x1, Pallas kernels, _main(): pl.pallas_call(_main_kernel, out_shape=(jax.ShapeDtypeStruct((SEQS, PROP,...  29.4 us
    pallas_call x1, Pallas kernels, _copy(): pl.pallas_call(_copy_kernel, out_shape=tuple((jax.ShapeDtypeStruct(array....  3.63 us

profile of v5, /device:TPU:1, one launch (start us, length us, event | category | flops | bytes accessed | tf_op | source)
XLA Modules:
  0.0 34.3 jit_solution(9603845253367909801)
XLA Ops:
  0.6 3.6 %copy_caches.1 = (bf16[4,512,512]{2,1,0:T(8,128)(2,1)}, bf16[4,512,512]{2,1,0:T(8,128)(2,1)}) custom-call(bf16[4,512,512]{2,1,0:T(8,128)(2,1)} %ck_hbm.1, bf16[4,512,512]{2,1,0:T(8,128)(2,1)} %cv_hbm.1), custom_call_target="tpu_custom_call" | custom-call | tf_op jit(solution)/shard_map/copy_caches/pallas_call | solution.py:688
  4.3 29.4 %attention.1 = (bf16[4,24,256]{2,1,0:T(8,128)(2,1)S(1)}, bf16[4,512,512]{2,1,0:T(8,128)(2,1)S(1)}, bf16[4,512,512]{2,1,0:T(8,128)(2,1)S(1)}) custom-call(bf16[96,256]{1,0:T(8,128)(2,1)} %tok_hbm.1, f32[1,256]{1,0:T(1,128)} %bitcast.5, bf16[256,512]{1,0:T(8,128)(2,1)} %wq_hbm.1, bf16[256,512]{1,0:T(8,128)(2,1)} %wk_hbm.1, bf16[256,512]{1,0:T(8,128)(2,1)} %wv_hbm.1, ...), custom_call_target="tpu_custom_call" | custom-call | tf_op jit(solution)/shard_map/attention/pallas_call | solution.py:615
  33.7 0.7 %write.1 = (bf16[4,24,256]{2,1,0:T(8,128)(2,1)}, bf16[4,512,512]{2,1,0:T(8,128)(2,1)}, bf16[4,512,512]{2,1,0:T(8,128)(2,1)}) custom-call(bf16[4,24,256]{2,1,0:T(8,128)(2,1)S(1)} %get-tuple-element.12.mixed_ref, bf16[4,512,512]{2,1,0:T(8,128)(2,1)S(1)} %get-tuple-element.13.keys_ref, ...), custom_call_target="tpu_custom_call", output_to_operand_aliasing={{1}: (3, {}), {2}: (4, {})} | custom-call | tf_op jit(solution)/shard_map/write/pallas_call | solution.py:724

commit v6 on v5

--- a/solution.py
+++ b/solution.py
@@ -154,6 +154,8 @@
     sm,
     sems,
     ready,
+    go,
+    own_factor,
     self_stats,
     self_sum,
 ):
@@ -179,9 +181,9 @@
     @pl.when(is_owner)
     def _():
         for step in PARTNERS:
+            greet(step, 0, 0)
             greet(step, 0, 1)
-        for step in PARTNERS + [0]:
-            greet(step, 0, 0)
+        greet(0, 0, 0)
         for step in Y_STEPS:
             greet(0, step, 1)
             greet(0, step, 0)
@@ -319,13 +321,6 @@
                 )
     for b in range(SEQS):
         transpose_values(b)
-    for step in PARTNERS:
-        send_kv(step)
-
-    @pl.when(is_other)
-    def _():
-        send_kv(0)
-
     for index in (6, 7, 8, 9, 10, 11, 12):
         loads[index].wait()
 
@@ -337,15 +332,15 @@
     def _():
         arrived(rq.at[1, 1:], Q_RECV + 1)
         arrived(rq.at[0], Q_RECV)
-        factors = []
         for group in range(2):
             total = (pq[me] if group else rq[0, 0]).astype(F32)
             for step in range(1, KV):
                 total = total + rq[group, step].astype(F32)
             square_row = jnp.sum(total[PROP:PAD], axis=0, keepdims=True)
             square_column = jnp.sum(jnp.where(eye, square_row, 0.0), axis=1, keepdims=True)
-            factors.append(lax.rsqrt(square_column / D + EPS))
-            own_q = (total[0:PROP] * factors[group]).astype(BF16)
+            factor = lax.rsqrt(square_column / D + EPS)
+            own_factor[group] = jnp.broadcast_to(factor, (PROP, BLOCK))
+            own_q = (total[0:PROP] * factor).astype(BF16)
             if group:
                 qg[me] = own_q
             else:
@@ -357,22 +352,104 @@
                     send_qg(step, 0)
                     if step:
                         send_qg(step, 1)
+        pl.semaphore_signal(go, inc=1, device_id=spot(0, 0, 0), device_id_type=pl.DeviceIdType.MESH)
+        for step in PARTNERS:
+            send_kv(step)
+
+    @pl.when(is_other)
+    def _():
+        pl.semaphore_wait(go, 1)
+        for step in PARTNERS + [0]:
+            send_kv(step)
+        remote(wo.at[0], wo.at[0], GIVE_SEND, GIVE_RECV, spot(0, 0, 1)).start()
+        remote(og.at[0], og.at[0], GIVE_SEND + 1, GIVE_RECV + 1, spot(0, 0, 1)).start()
+        remote(lam.at[0], lam.at[0], GIVE_SEND + 2, GIVE_RECV + 2, spot(0, 0, 1)).start()
+
+
+    def gathered(z_step):
+        if z_step:
+            arrived(qg.at[pl.ds((z ^ z_step) * 4, 4)], QG_RECV + z_step)
+            return
+
+        @pl.when(is_owner)
+        def _():
+            arrived(qg.at[0:3], QG_RECV)
+
+        @pl.when(is_other)
+        def _():
+            arrived(qg.at[0:4], QG_RECV)
+
+    def expand(order):
+        b = z ^ Z_ORDER[order]
+        for half in range(2):
+            for side in range(2):
+                chunk = qg[b * 4 + half * 2 + side].astype(F32)
+                lanes = slice(side * BLOCK, (side + 1) * BLOCK)
+                qe[order, half, lanes, lanes] = _expanded(chunk)
+
+    def score(order):
+        b = z ^ Z_ORDER[order]
+        begin = len_ref[b] + acc_ref[b] - me * POS
+        visible = lax.broadcasted_iota(jnp.int32, (POS, BLOCK), 0) < begin
+        visible = jnp.concatenate([visible, visible], axis=1)
+        for half in range(2):
+            keys = kbuf[b, :, half * 2 * BLOCK : (half + 1) * 2 * BLOCK]
+            scores = jnp.where(visible, _dot_nt(keys, qe[order, half]) * SCALE2, LOW)
+            sc[order % 2, half] = scores
+            sm[order % 2, half] = jnp.max(scores, axis=0, keepdims=True)
+
+    def weigh(order):
+        b = z ^ Z_ORDER[order]
+        for half in range(2):
+            largest = sm[order % 2, half]
+            weight = jnp.exp2(sc[order % 2, half] - largest)
+            weight_sum = jnp.sum(weight, axis=0, keepdims=True)
+            weight = weight.astype(BF16)
+            for side in range(2):
+                block = half * 2 + side
+                lanes = slice(side * BLOCK, (side + 1) * BLOCK)
+                out = _dot(vt[b, block * BLOCK : (block + 1) * BLOCK, :], weight[:, lanes])
+                owner = b * 4 + block
+                dv[owner] = _packed(jnp.where(second_head, out[HEAD:], out[:HEAD])).astype(BF16)
+                ds[owner] = jnp.concatenate([largest[:, lanes], weight_sum[:, lanes]], axis=0)
+
+    def send(order):
+        for x_step in (2, 1, 3, 0):
+            step = Z_ORDER[order] << 2 | x_step
+            if step:
+                send_d(step)
+        if Z_ORDER[order] == 0:
+
+            @pl.when(is_other)
+            def _():
+                send_d(0)
+
+    for group in Z_GROUPS:
+        for order in group:
+            gathered(Z_ORDER[order])
+        for order in group:
+            expand(order)
+        score(group[0])
+        for order in group:
+            if order + 1 in group:
+                score(order + 1)
+            weigh(order)
+            send(order)
+
+    @pl.when(is_owner)
+    def _():
         arrived(rkv.at[1, 1:], KV_RECV + 1)
         arrived(rkv.at[0], KV_RECV)
         for group in range(2):
             summed = (pkv[me] if group else rkv[0, 0]).astype(F32)
             for step in range(1, KV):
                 summed = summed + rkv[group, step].astype(F32)
-            rows = [summed[0:PROP] * factors[group], summed[PROP:] * factors[group]]
+            rows = [summed[0:PROP] * own_factor[group], summed[PROP:] * own_factor[group]]
             rows = jnp.concatenate(rows, axis=0).astype(BF16)
             if group:
                 kvg[me] = rows
             else:
                 okv[...] = rows
-        for step in PARTNERS + [0]:
-            send_kvg(step, 0)
-        for step in PARTNERS:
-            send_kvg(step, 1)
         par_pad[...] = jnp.full((8, BLOCK), -1, jnp.int32)
         par_pad[0:SEQS, 0:PROP] = par_ref[...]
         parent_row = par_pad[pl.ds(z, 1), :]
@@ -398,108 +475,6 @@
             self_stats[group, 1:2] = jnp.sum(self_weight, axis=0, keepdims=True)
             self_out = _dot(jnp.transpose(own_v).astype(BF16), self_weight.astype(BF16))
             self_sum[group] = jnp.where(second_head, self_out[HEAD:], self_out[:HEAD])
-
-    @pl.when(is_other)
-    def _():
-        remote(wo.at[0], wo.at[0], GIVE_SEND, GIVE_RECV, spot(0, 0, 1)).start()
-        remote(og.at[0], og.at[0], GIVE_SEND + 1, GIVE_RECV + 1, spot(0, 0, 1)).start()
-        remote(lam.at[0], lam.at[0], GIVE_SEND + 2, GIVE_RECV + 2, spot(0, 0, 1)).start()
-
-
-    def gathered(z_step):
-        if z_step:
-            arrived(qg.at[pl.ds((z ^ z_step) * 4, 4)], QG_RECV + z_step)
-            return
-
-        @pl.when(is_owner)
-        def _():
-            arrived(qg.at[0:3], QG_RECV)
-
-        @pl.when(is_other)
-        def _():
-            arrived(qg.at[0:4], QG_RECV)
-
-    def expand(order):
-        b = z ^ Z_ORDER[order]
-        for half in range(2):
-            for side in range(2):
-                chunk = qg[b * 4 + half * 2 + side].astype(F32)
-                lanes = slice(side * BLOCK, (side + 1) * BLOCK)
-                qe[order, half, lanes, lanes] = _expanded(chunk)
-
-    def score(order):
-        b = z ^ Z_ORDER[order]
-        begin = len_ref[b] + acc_ref[b] - me * POS
-        visible = lax.broadcasted_iota(jnp.int32, (POS, BLOCK), 0) < begin
-        visible = jnp.concatenate([visible, visible], axis=1)
-        for half in range(2):
-            keys = kbuf[b, :, half * 2 * BLOCK : (half + 1) * 2 * BLOCK]
-            scores = jnp.where(visible, _dot_nt(keys, qe[order, half]) * SCALE2, LOW)
-            sc[order % 2, half] = scores
-            sm[order % 2, half] = jnp.max(scores, axis=0, keepdims=True)
-
-    def weigh(order):
-        b = z ^ Z_ORDER[order]
-        for half in range(2):
-            largest = sm[order % 2, half]
-            weight = jnp.exp2(sc[order % 2, half] - largest)
-            weight_sum = jnp.sum(weight, axis=0, keepdims=True)
-            weight = weight.astype(BF16)
-            for side in range(2):
-                block = half * 2 + side
-                lanes = slice(side * BLOCK, (side + 1) * BLOCK)
-                out = _dot(vt[b, block * BLOCK : (block + 1) * BLOCK, :], weight[:, lanes])
-                owner = b * 4 + block
-                dv[owner] = _packed(jnp.where(second_head, out[HEAD:], out[:HEAD])).astype(BF16)
-                ds[owner] = jnp.concatenate([largest[:, lanes], weight_sum[:, lanes]], axis=0)
-
-    def send(order):
-        for x_step in (2, 1, 3, 0):
-            step = Z_ORDER[order] << 2 | x_step
-            if step:
-                send_d(step)
-        if Z_ORDER[order] == 0:
-
-            @pl.when(is_other)
-            def _():
-                send_d(0)
-
-    for group in Z_GROUPS:
-        for order in group:
-            gathered(Z_ORDER[order])
-        for order in group:
-            expand(order)
-        score(group[0])
-        for order in group:
-            if order + 1 in group:
-                score(order + 1)
-            weigh(order)
-            send(order)
-
-    @pl.when(is_owner)
-    def _():
-        arrived(kvg.at[1:], KVG_RECV)
-
-    @pl.when(is_other)
-    def _():
-        arrived(kvg, KVG_RECV)
-
-    for b in range(SEQS):
-        begin = len_ref[b] + acc_ref[b] - me * POS
-        position = lax.broadcasted_iota(jnp.int32, (POS, BLOCK), 0) - begin
-        written = (position >= 0) & (position < PROP)
-        slot = lax.broadcasted_iota(jnp.int32, (POS, BLOCK), 1)
-        for which, buf in enumerate((kbuf, vbuf)):
-            offset = which * PROP
-            placing = jnp.where(written & (position + offset == slot), 1.0, 0.0).astype(BF16)[:, 0 : 2 * PROP]
-            for block in range(4):
-                lanes = slice(block * BLOCK, (block + 1) * BLOCK)
-                moved = _dot(placing, kvg[b * 4 + block])
-                buf[b, :, lanes] = jnp.where(written, moved, buf[b, :, lanes].astype(F32)).astype(BF16)
-            out_copy(which, b).start()
-
-    @pl.when(is_owner)
-    def _():
         lane_row = lax.broadcasted_iota(jnp.int32, (1, BLOCK), 1)
         arrived(og.at[0], GIVE_RECV + 1)
         arrived(lam.at[0], GIVE_RECV + 2)
@@ -557,6 +532,16 @@
             ng[me, group] = turned.astype(BF16)
         for step in PARTNERS:
             send_ng(step)
+        for z_step in (2, 1, 3, 0):
+
+            @pl.when((z ^ z_step) >= 2)
+            def _(z_step=z_step):
+                for step in PARTNERS + [0]:
+                    if step >> 2 == z_step:
+                        send_kvg(step, 0)
+                        if step:
+                            send_kvg(step, 1)
+
 
         for z_step in Z_OUT:
             arrived(ng.at[pl.ds((z ^ z_step) * 4, 4 if z_step else 3)], NG_RECV + z_step)
@@ -567,10 +552,41 @@
                 projected = projected + _dot(rows, wo[group])
             rpart[z_step, 0] = projected.astype(BF16)
             for step in Y_STEPS:
+                send_mx(z_step, step, 1)
+            for step in Y_STEPS:
                 send_mx(z_step, step, 0)
-            for step in Y_STEPS:
-                send_mx(z_step, step, 1)
             send_mx(z_step, 0, 0)
+
+    @pl.when(is_owner & (z >= 2))
+    def _():
+        arrived(kvg.at[1:], KVG_RECV)
+
+    @pl.when(is_other & (z >= 2))
+    def _():
+        arrived(kvg, KVG_RECV)
+
+    @pl.when(z >= 2)
+    def _():
+        for b in range(SEQS):
+            begin = len_ref[b] + acc_ref[b] - me * POS
+            position = lax.broadcasted_iota(jnp.int32, (POS, BLOCK), 0) - begin
+            written = (position >= 0) & (position < PROP)
+            slot = lax.broadcasted_iota(jnp.int32, (POS, BLOCK), 1)
+            for which, buf in enumerate((kbuf, vbuf)):
+                offset = which * PROP
+                placing = jnp.where(written & (position + offset == slot), 1.0, 0.0)
+                placing = placing.astype(BF16)[:, 0 : 2 * PROP]
+                for block in range(4):
+                    lanes = slice(block * BLOCK, (block + 1) * BLOCK)
+                    moved = _dot(placing, kvg[b * 4 + block])
+                    buf[b, :, lanes] = jnp.where(written, moved, buf[b, :, lanes].astype(F32)).astype(BF16)
+                out_copy(which, b).start()
+
+    @pl.when(z < 2)
+    def _():
+        for b in range(SEQS):
+            for which in range(2):
+                out_copy(which, b).start()
 
     for z_step in Z_OUT:
 
@@ -593,11 +609,19 @@
 
     @pl.when(is_owner)
     def _():
-        for ref, index in sent + ((qg, QG_SEND + 1), (kvg, KVG_SEND + 1), (ng, NG_SEND)):
+        for ref, index in sent + ((qg, QG_SEND + 1), (ng, NG_SEND)):
             arrived(ref.at[1:], index)
         arrived(qg, QG_SEND)
-        arrived(kvg, KVG_SEND)
+        arrived(kvg.at[0:8], KVG_SEND)
         arrived(rpart.at[0:7], MX_SEND)
+
+    @pl.when(is_owner & (z < 2))
+    def _():
+        arrived(kvg.at[0:8], KVG_SEND + 1)
+
+    @pl.when(is_owner & (z >= 2))
+    def _():
+        arrived(kvg.at[0:7], KVG_SEND + 1)
 
     @pl.when(is_other)
     def _():
@@ -654,6 +678,8 @@
             pltpu.VMEM((2, 2, 1, 2 * BLOCK), F32),
             dma((SEMAPHORES,)),
             pltpu.SemaphoreType.REGULAR,
+            pltpu.SemaphoreType.REGULAR,
+            pltpu.VMEM((2, PROP, BLOCK), F32),
             pltpu.VMEM((2, 2, BLOCK), F32),
             pltpu.VMEM((2, HEAD, BLOCK), F32),
         ],
@@ -664,23 +690,35 @@
     )(*(pltpu.with_memory_space_constraint(array, pltpu.HBM) for array in arrays))
 
 
-def _copies_first():
-    return (lax.axis_index("kv") < 4) & (lax.axis_index("tp") // 2 * 4 + lax.axis_index("kv") < 5)
+def _copies_first(which):
+    kv = lax.axis_index("kv")
+    y = lax.axis_index("tp") // 2
+    return (kv < 4) & (kv + y * 4 < 6) if which else (kv + y) < 1
 
 
 def _copy_kernel(keys_in, values_in, keys_out, values_out, kbuf, vbuf, sem):
-    @pl.when(_copies_first())
-    def _():
-        pairs = ((keys_in, kbuf, keys_out), (values_in, vbuf, values_out))
-        fetches = [pltpu.make_async_copy(src, buf, sem.at[which]) for which, (src, buf, _) in enumerate(pairs)]
-        puts = [pltpu.make_async_copy(buf, dst, sem.at[which]) for which, (_, buf, dst) in enumerate(pairs)]
-        for copy in fetches:
-            copy.start()
-        for fetch, put in zip(fetches, puts):
-            fetch.wait()
-            put.start()
-        for copy in puts:
-            copy.wait()
+    pairs = ((keys_in, kbuf, keys_out), (values_in, vbuf, values_out))
+    fetches = [pltpu.make_async_copy(src, buf, sem.at[which]) for which, (src, buf, _) in enumerate(pairs)]
+    puts = [pltpu.make_async_copy(buf, dst, sem.at[which]) for which, (_, buf, dst) in enumerate(pairs)]
+
+    @pl.when(_copies_first(1))
+    def _():
+        fetches[1].start()
+
+        @pl.when(_copies_first(0))
+        def _():
+            fetches[0].start()
+
+        fetches[1].wait()
+        puts[1].start()
+
+        @pl.when(_copies_first(0))
+        def _():
+            fetches[0].wait()
+            puts[0].start()
+            puts[0].wait()
+
+        puts[1].wait()
 
 
 def _copy(*arrays):
@@ -704,16 +742,21 @@
     mixed_copy = pltpu.make_async_copy(mixed_ref, mixed_hbm, sem.at[2])
     mixed_copy.start()
 
-    @pl.when(jnp.logical_not(_copies_first()))
-    def _():
-        copies = [
-            pltpu.make_async_copy(keys_ref, keys_hbm, sem.at[0]),
-            pltpu.make_async_copy(values_ref, values_hbm, sem.at[1]),
-        ]
-        for copy in copies:
-            copy.start()
-        for copy in copies:
-            copy.wait()
+    copies = [
+        pltpu.make_async_copy(keys_ref, keys_hbm, sem.at[0]),
+        pltpu.make_async_copy(values_ref, values_hbm, sem.at[1]),
+    ]
+
+    @pl.when(jnp.logical_not(_copies_first(0)))
+    def _():
+        copies[0].start()
+
+        @pl.when(jnp.logical_not(_copies_first(1)))
+        def _():
+            copies[1].start()
+            copies[1].wait()
+
+        copies[0].wait()
 
     mixed_copy.wait()
 

time: 34.4 us -> 33.9 us (0.985)
  Pallas kernels: 33.7 us -> 33.1 us
    pallas_call x1, Pallas kernels: 29.4 us -> 28.8 us  [_main(): pl.pallas_call(_main_kernel, out_shape=(jax.ShapeDtypeStruct((SEQS, PROP,...]
where the time goes in v6:
time: 33.9 us; the launch traced here: 33.7 us
  Pallas kernels  33.1 us (98%)
  between operations  0.65 us (2%)
    pallas_call x1, Pallas kernels, _main(): pl.pallas_call(_main_kernel, out_shape=(jax.ShapeDtypeStruct((SEQS, PROP,...  28.8 us
    pallas_call x1, Pallas kernels, _copy(): pl.pallas_call(_copy_kernel, out_shape=tuple((jax.ShapeDtypeStruct(array....  3.63 us

profile of v6, /device:TPU:1, one launch (start us, length us, event | category | flops | bytes accessed | tf_op | source)
XLA Modules:
  0.0 33.7 jit_solution(5150685046425233983)
XLA Ops:
  0.6 3.6 %copy_caches.1 = (bf16[4,512,512]{2,1,0:T(8,128)(2,1)}, bf16[4,512,512]{2,1,0:T(8,128)(2,1)}) custom-call(bf16[4,512,512]{2,1,0:T(8,128)(2,1)} %ck_hbm.1, bf16[4,512,512]{2,1,0:T(8,128)(2,1)} %cv_hbm.1), custom_call_target="tpu_custom_call" | custom-call | tf_op jit(solution)/shard_map/copy_caches/pallas_call | solution.py:726
  4.3 28.8 %attention.1 = (bf16[4,24,256]{2,1,0:T(8,128)(2,1)S(1)}, bf16[4,512,512]{2,1,0:T(8,128)(2,1)S(1)}, bf16[4,512,512]{2,1,0:T(8,128)(2,1)S(1)}) custom-call(bf16[96,256]{1,0:T(8,128)(2,1)} %tok_hbm.1, f32[1,256]{1,0:T(1,128)} %bitcast.5, bf16[256,512]{1,0:T(8,128)(2,1)} %wq_hbm.1, bf16[256,512]{1,0:T(8,128)(2,1)} %wk_hbm.1, bf16[256,512]{1,0:T(8,128)(2,1)} %wv_hbm.1, ...), custom_call_target="tpu_custom_call" | custom-call | tf_op jit(solution)/shard_map/attention/pallas_call | solution.py:639
  33.1 0.7 %write.1 = (bf16[4,24,256]{2,1,0:T(8,128)(2,1)}, bf16[4,512,512]{2,1,0:T(8,128)(2,1)}, bf16[4,512,512]{2,1,0:T(8,128)(2,1)}) custom-call(bf16[4,24,256]{2,1,0:T(8,128)(2,1)S(1)} %get-tuple-element.12.mixed_ref, bf16[4,512,512]{2,1,0:T(8,128)(2,1)S(1)} %get-tuple-element.13.keys_ref, ...), custom_call_target="tpu_custom_call", output_to_operand_aliasing={{1}: (3, {}), {2}: (4, {})} | custom-call | tf_op jit(solution)/shard_map/write/pallas_call | solution.py:767

commit v7 on v6

--- a/solution.py
+++ b/solution.py
@@ -45,19 +45,19 @@
 MX_SEND = 9
 GIVE_SEND = 10
 Q_RECV = 13
-KV_RECV = 15
-DV_RECV = 17
-DS_RECV = 19
-QG_RECV = 21
-KVG_RECV = 25
-NG_RECV = 26
-MX_RECV = 30
-GIVE_RECV = 34
-SEMAPHORES = 37
-OUT = Q_RECV
+KV_RECV = 14
+DV_RECV = 15
+DS_RECV = 16
+QG_RECV = 17
+KVG_RECV = 21
+NG_RECV = 22
+MX_RECV = 26
+GIVE_RECV = 30
+SEMAPHORES = 33
+OUT = 8
 Z_ORDER = (0, 1, 2, 3)
 Z_OUT = (0, 1, 3, 2)
-Z_SEND = (0, 2, 1, 3)
+Z_SEND = (0, 1, 2, 3)
 Z_GROUPS = ((0,), (1,), (2, 3))
 Y_STEPS = (2, 1, 3)
 PARTNERS = sorted(range(1, KV), key=lambda step: -_distance(step))
@@ -222,14 +222,14 @@
         )
 
     def send_q(step):
-        remote(pq.at[me ^ step], rq.at[core, step], Q_SEND, Q_RECV + core, spot(step, 0, 1)).start()
+        remote(pq.at[me ^ step], rq.at[core * KV + step], Q_SEND, Q_RECV, spot(step, 0, 1)).start()
 
     def send_kv(step):
-        remote(pkv.at[me ^ step], rkv.at[core, step], KV_SEND, KV_RECV + core, spot(step, 0, 1)).start()
+        remote(pkv.at[me ^ step], rkv.at[core * KV + step], KV_SEND, KV_RECV, spot(step, 0, 1)).start()
 
     def send_d(step):
-        remote(ds.at[me ^ step], rds.at[core, step], DS_SEND, DS_RECV + core, spot(step, 0, 1)).start()
-        remote(dv.at[me ^ step], rdv.at[core, step], DV_SEND, DV_RECV + core, spot(step, 0, 1)).start()
+        remote(ds.at[me ^ step], rds.at[core * KV + step], DS_SEND, DS_RECV, spot(step, 0, 1)).start()
+        remote(dv.at[me ^ step], rdv.at[core * KV + step], DV_SEND, DV_RECV, spot(step, 0, 1)).start()
 
     def send_qg(step, to):
         src = qg.at[me] if to else oq
@@ -249,7 +249,7 @@
 
     def out_copy(which, b):
         buf, out = ((kbuf, keys_out), (vbuf, values_out))[which]
-        return pltpu.make_async_copy(buf.at[b], out.at[b], sems.at[OUT + which])
+        return pltpu.make_async_copy(buf.at[b], out.at[b], sems.at[OUT + 3 * core + which])
 
     loads[0].wait()
     loads[1].wait()
@@ -330,12 +330,11 @@
 
     @pl.when(is_owner)
     def _():
-        arrived(rq.at[1, 1:], Q_RECV + 1)
-        arrived(rq.at[0], Q_RECV)
+        arrived(rq.at[0:31], Q_RECV)
         for group in range(2):
-            total = (pq[me] if group else rq[0, 0]).astype(F32)
+            total = (pq[me] if group else rq[0]).astype(F32)
             for step in range(1, KV):
-                total = total + rq[group, step].astype(F32)
+                total = total + rq[group * KV + step].astype(F32)
             square_row = jnp.sum(total[PROP:PAD], axis=0, keepdims=True)
             square_column = jnp.sum(jnp.where(eye, square_row, 0.0), axis=1, keepdims=True)
             factor = lax.rsqrt(square_column / D + EPS)
@@ -438,12 +437,11 @@
 
     @pl.when(is_owner)
     def _():
-        arrived(rkv.at[1, 1:], KV_RECV + 1)
-        arrived(rkv.at[0], KV_RECV)
+        arrived(rkv.at[0:31], KV_RECV)
         for group in range(2):
-            summed = (pkv[me] if group else rkv[0, 0]).astype(F32)
+            summed = (pkv[me] if group else rkv[0]).astype(F32)
             for step in range(1, KV):
-                summed = summed + rkv[group, step].astype(F32)
+                summed = summed + rkv[group * KV + step].astype(F32)
             rows = [summed[0:PROP] * own_factor[group], summed[PROP:] * own_factor[group]]
             rows = jnp.concatenate(rows, axis=0).astype(BF16)
             if group:
@@ -488,29 +486,27 @@
             ]
             lam_rows.append(jnp.where(lane_row < PROP, pair[0], pair[1]))
 
-        arrived(rds.at[1, 1:], DS_RECV + 1)
-        arrived(rds.at[0], DS_RECV)
-        denominator = []
+        arrived(rds.at[0:31], DS_RECV)
         self_factor = []
         factors = []
         used = lax.broadcasted_iota(jnp.int32, (KV, BLOCK), 1) < 96
         for group in range(2):
-            slots = [ds.at[me] if group else rds.at[0, 0]] + [rds.at[group, step] for step in range(1, KV)]
+            slots = [ds.at[me] if group else rds.at[0]] + [rds.at[group * KV + step] for step in range(1, KV)]
             maxima = jnp.concatenate([slot[0:1] for slot in slots], axis=0)
             totals = jnp.concatenate([slot[1:2] for slot in slots], axis=0)
             top = jnp.maximum(jnp.max(maxima, axis=0, keepdims=True), self_stats[group, 0:1])
-            self_factor.append(jnp.exp2(self_stats[group, 0:1] - top))
+            own = jnp.exp2(self_stats[group, 0:1] - top)
             factor = jnp.exp2(maxima - top)
-            denominator.append(
-                self_stats[group, 1:2] * self_factor[group] + jnp.sum(totals * factor, axis=0, keepdims=True)
-            )
+            denominator = self_stats[group, 1:2] * own + jnp.sum(totals * factor, axis=0, keepdims=True)
+            inverse = 1.0 / denominator
+            factor = factor * inverse
+            self_factor.append(own * inverse)
             factors.append(
                 [jnp.where(used, factor, pltpu.roll(factor, 96 - 32 * third, 1)) for third in range(3)]
             )
-        arrived(rdv.at[1, 1:], DV_RECV + 1)
-        arrived(rdv.at[0], DV_RECV)
+        arrived(rdv.at[0:31], DV_RECV)
         for group in range(2):
-            slots = [dv.at[me] if group else rdv.at[0, 0]] + [rdv.at[group, step] for step in range(1, KV)]
+            slots = [dv.at[me] if group else rdv.at[0]] + [rdv.at[group * KV + step] for step in range(1, KV)]
             merged = []
             for third in range(3):
                 rows = slice(16 * third, 16 * third + 16)
@@ -521,8 +517,7 @@
                 while len(sums) > 1:
                     sums = [a + b for a, b in zip(sums[::2], sums[1::2])]
                 merged.append(sums[0])
-            merged = _unpacked(jnp.concatenate(merged, axis=0)) + self_sum[group] * self_factor[group]
-            attended = merged / denominator[group]
+            attended = _unpacked(jnp.concatenate(merged, axis=0)) + self_sum[group] * self_factor[group]
             difference = attended - lam_rows[group] * pltpu.roll(attended, BLOCK - 2 * PROP, 1)
             power = jnp.mean(difference * difference, axis=0, keepdims=True)
             normed = difference * lax.rsqrt(power + EPS)
@@ -603,8 +598,8 @@
             mixed = mixed + rpart[z_step, step].astype(F32)
         mixed_ref[z ^ z_step] = mixed.astype(BF16)
 
-    arrived(kbuf, OUT)
-    arrived(vbuf, OUT + 1)
+    arrived(kbuf, OUT + 3 * core)
+    arrived(vbuf, OUT + 3 * core + 1)
     sent = ((pq, Q_SEND), (pkv, KV_SEND), (dv, DV_SEND), (ds, DS_SEND))
 
     @pl.when(is_owner)
@@ -659,17 +654,17 @@
             pltpu.VMEM((2, 512, 256), BF16),
             pltpu.VMEM((SEQS, 512, POS), BF16),
             pltpu.VMEM((KV, PAD, BLOCK), BF16),
-            pltpu.VMEM((2, KV, PAD, BLOCK), BF16),
+            pltpu.VMEM((2 * KV, PAD, BLOCK), BF16),
             pltpu.VMEM((KV, 2 * PROP, BLOCK), BF16),
-            pltpu.VMEM((2, KV, 2 * PROP, BLOCK), BF16),
+            pltpu.VMEM((2 * KV, 2 * PROP, BLOCK), BF16),
             pltpu.VMEM((PROP, BLOCK), BF16),
             pltpu.VMEM((2 * PROP, BLOCK), BF16),
             pltpu.VMEM((KV, PROP, BLOCK), BF16),
             pltpu.VMEM((KV, 2 * PROP, BLOCK), BF16),
             pltpu.VMEM((KV, 48, BLOCK), BF16),
-            pltpu.VMEM((2, KV, 48, BLOCK), BF16),
+            pltpu.VMEM((2 * KV, 48, BLOCK), BF16),
             pltpu.VMEM((KV, 2, BLOCK), F32),
-            pltpu.VMEM((2, KV, 2, BLOCK), F32),
+            pltpu.VMEM((2 * KV, 2, BLOCK), F32),
             pltpu.VMEM((KV, 2, PROP, BLOCK), BF16),
             pltpu.VMEM((8, 4, PROP, 256), BF16),
             pltpu.VMEM((8, BLOCK), jnp.int32),

time: 33.9 us -> 33.8 us (level)
  no operation moved by 1% of the time
where the time goes in v7:
time: 33.8 us; the launch traced here: 33.7 us
  Pallas kernels  33 us (98%)
  between operations  0.65 us (2%)
    pallas_call x1, Pallas kernels, _main(): pl.pallas_call(_main_kernel, out_shape=(jax.ShapeDtypeStruct((SEQS, PROP,...  28.8 us
    pallas_call x1, Pallas kernels, _copy(): pl.pallas_call(_copy_kernel, out_shape=tuple((jax.ShapeDtypeStruct(array....  3.63 us

profile of v7, /device:TPU:1, one launch (start us, length us, event | category | flops | bytes accessed | tf_op | source)
XLA Modules:
  0.0 33.7 jit_solution(557869603132336586)
XLA Ops:
  0.6 3.6 %copy_caches.1 = (bf16[4,512,512]{2,1,0:T(8,128)(2,1)}, bf16[4,512,512]{2,1,0:T(8,128)(2,1)}) custom-call(bf16[4,512,512]{2,1,0:T(8,128)(2,1)} %ck_hbm.1, bf16[4,512,512]{2,1,0:T(8,128)(2,1)} %cv_hbm.1), custom_call_target="tpu_custom_call" | custom-call | tf_op jit(solution)/shard_map/copy_caches/pallas_call | solution.py:721
  4.3 28.8 %attention.1 = (bf16[4,24,256]{2,1,0:T(8,128)(2,1)S(1)}, bf16[4,512,512]{2,1,0:T(8,128)(2,1)S(1)}, bf16[4,512,512]{2,1,0:T(8,128)(2,1)S(1)}) custom-call(bf16[96,256]{1,0:T(8,128)(2,1)} %tok_hbm.1, f32[1,256]{1,0:T(1,128)} %bitcast.5, bf16[256,512]{1,0:T(8,128)(2,1)} %wq_hbm.1, bf16[256,512]{1,0:T(8,128)(2,1)} %wk_hbm.1, bf16[256,512]{1,0:T(8,128)(2,1)} %wv_hbm.1, ...), custom_call_target="tpu_custom_call" | custom-call | tf_op jit(solution)/shard_map/attention/pallas_call | solution.py:634
  33.0 0.7 %write.1 = (bf16[4,24,256]{2,1,0:T(8,128)(2,1)}, bf16[4,512,512]{2,1,0:T(8,128)(2,1)}, bf16[4,512,512]{2,1,0:T(8,128)(2,1)}) custom-call(bf16[4,24,256]{2,1,0:T(8,128)(2,1)S(1)} %get-tuple-element.12.mixed_ref, bf16[4,512,512]{2,1,0:T(8,128)(2,1)S(1)} %get-tuple-element.13.keys_ref, ...), custom_call_target="tpu_custom_call", output_to_operand_aliasing={{1}: (3, {}), {2}: (4, {})} | custom-call | tf_op jit(solution)/shard_map/write/pallas_call | solution.py:762

commit v8 on v7

--- a/solution.py
+++ b/solution.py
@@ -57,6 +57,7 @@
 OUT = 8
 Z_ORDER = (0, 1, 2, 3)
 Z_OUT = (0, 1, 3, 2)
+Z_OUT_GROUPS = ((0,), (1,), (3, 2))
 Z_SEND = (0, 1, 2, 3)
 Z_GROUPS = ((0,), (1,), (2, 3))
 Y_STEPS = (2, 1, 3)
@@ -538,19 +539,24 @@
                             send_kvg(step, 1)
 
 
-        for z_step in Z_OUT:
-            arrived(ng.at[pl.ds((z ^ z_step) * 4, 4 if z_step else 3)], NG_RECV + z_step)
-            b = z ^ z_step
-            projected = 0.0
-            for group in range(2):
-                rows = jnp.concatenate([ng[b * 4 + block, group] for block in range(4)], axis=1)
-                projected = projected + _dot(rows, wo[group])
-            rpart[z_step, 0] = projected.astype(BF16)
-            for step in Y_STEPS:
-                send_mx(z_step, step, 1)
-            for step in Y_STEPS:
-                send_mx(z_step, step, 0)
-            send_mx(z_step, 0, 0)
+        for group in Z_OUT_GROUPS:
+            for z_step in group:
+                arrived(ng.at[pl.ds((z ^ z_step) * 4, 4 if z_step else 3)], NG_RECV + z_step)
+            sums = []
+            for z_step in group:
+                rows = [
+                    jnp.concatenate([ng[(z ^ z_step) * 4 + block, half] for block in range(4)], axis=1)
+                    for half in range(2)
+                ]
+                sums.append((_dot(rows[0], wo[0]) + _dot(rows[1], wo[1])).astype(BF16))
+            for z_step, piece in zip(group, sums):
+                rpart[z_step, 0] = piece
+            for to in (1, 0):
+                for z_step in group:
+                    for step in Y_STEPS:
+                        send_mx(z_step, step, to)
+            for z_step in group:
+                send_mx(z_step, 0, 0)
 
     @pl.when(is_owner & (z >= 2))
     def _():
@@ -688,7 +694,7 @@
 def _copies_first(which):
     kv = lax.axis_index("kv")
     y = lax.axis_index("tp") // 2
-    return (kv < 4) & (kv + y * 4 < 6) if which else (kv + y) < 1
+    return (kv < 5) & (kv + y * 4 < 6) if which else (kv + y) < 1
 
 
 def _copy_kernel(keys_in, values_in, keys_out, values_out, kbuf, vbuf, sem):

time: 33.8 us -> 33.5 us (level)
  no operation moved by 1% of the time
where the time goes in v8:
time: 33.5 us; the launch traced here: 33.4 us
  Pallas kernels  32.8 us (98%)
  between operations  0.65 us (2%)
    pallas_call x1, Pallas kernels, _main(): pl.pallas_call(_main_kernel, out_shape=(jax.ShapeDtypeStruct((SEQS, PROP,...  28.5 us
    pallas_call x1, Pallas kernels, _copy(): pl.pallas_call(_copy_kernel, out_shape=tuple((jax.ShapeDtypeStruct(array....  3.63 us

profile of v8, /device:TPU:1, one launch (start us, length us, event | category | flops | bytes accessed | tf_op | source)
XLA Modules:
  0.0 33.4 jit_solution(10627059088525880554)
XLA Ops:
  0.6 3.6 %copy_caches.1 = (bf16[4,512,512]{2,1,0:T(8,128)(2,1)}, bf16[4,512,512]{2,1,0:T(8,128)(2,1)}) custom-call(bf16[4,512,512]{2,1,0:T(8,128)(2,1)} %ck_hbm.1, bf16[4,512,512]{2,1,0:T(8,128)(2,1)} %cv_hbm.1), custom_call_target="tpu_custom_call" | custom-call | tf_op jit(solution)/shard_map/copy_caches/pallas_call | solution.py:727
  4.3 28.5 %attention.1 = (bf16[4,24,256]{2,1,0:T(8,128)(2,1)S(1)}, bf16[4,512,512]{2,1,0:T(8,128)(2,1)S(1)}, bf16[4,512,512]{2,1,0:T(8,128)(2,1)S(1)}) custom-call(bf16[96,256]{1,0:T(8,128)(2,1)} %tok_hbm.1, f32[1,256]{1,0:T(1,128)} %bitcast.5, bf16[256,512]{1,0:T(8,128)(2,1)} %wq_hbm.1, bf16[256,512]{1,0:T(8,128)(2,1)} %wk_hbm.1, bf16[256,512]{1,0:T(8,128)(2,1)} %wv_hbm.1, ...), custom_call_target="tpu_custom_call" | custom-call | tf_op jit(solution)/shard_map/attention/pallas_call | solution.py:640
  32.8 0.7 %write.1 = (bf16[4,24,256]{2,1,0:T(8,128)(2,1)}, bf16[4,512,512]{2,1,0:T(8,128)(2,1)}, bf16[4,512,512]{2,1,0:T(8,128)(2,1)}) custom-call(bf16[4,24,256]{2,1,0:T(8,128)(2,1)S(1)} %get-tuple-element.12.mixed_ref, bf16[4,512,512]{2,1,0:T(8,128)(2,1)S(1)} %get-tuple-element.13.keys_ref, ...), custom_call_target="tpu_custom_call", output_to_operand_aliasing={{1}: (3, {}), {2}: (4, {})} | custom-call | tf_op jit(solution)/shard_map/write/pallas_call | solution.py:768

commit v9 on v8

--- a/solution.py
+++ b/solution.py
@@ -60,7 +60,7 @@
 Z_OUT_GROUPS = ((0,), (1,), (3, 2))
 Z_SEND = (0, 1, 2, 3)
 Z_GROUPS = ((0,), (1,), (2, 3))
-Y_STEPS = (2, 1, 3)
+Y_STEPS = (3, 2, 1)
 PARTNERS = sorted(range(1, KV), key=lambda step: -_distance(step))
 
 

time: 33.5 us -> 33.5 us (level)
  no operation moved by 1% of the time
where the time goes in v9:
time: 33.5 us; the launch traced here: 33.4 us
  Pallas kernels  32.8 us (98%)
  between operations  0.65 us (2%)
    pallas_call x1, Pallas kernels, _main(): pl.pallas_call(_main_kernel, out_shape=(jax.ShapeDtypeStruct((SEQS, PROP,...  28.5 us
    pallas_call x1, Pallas kernels, _copy(): pl.pallas_call(_copy_kernel, out_shape=tuple((jax.ShapeDtypeStruct(array....  3.63 us

profile of v9, /device:TPU:1, one launch (start us, length us, event | category | flops | bytes accessed | tf_op | source)
XLA Modules:
  0.0 33.4 jit_solution(7946795662317619246)
XLA Ops:
  0.6 3.6 %copy_caches.1 = (bf16[4,512,512]{2,1,0:T(8,128)(2,1)}, bf16[4,512,512]{2,1,0:T(8,128)(2,1)}) custom-call(bf16[4,512,512]{2,1,0:T(8,128)(2,1)} %ck_hbm.1, bf16[4,512,512]{2,1,0:T(8,128)(2,1)} %cv_hbm.1), custom_call_target="tpu_custom_call" | custom-call | tf_op jit(solution)/shard_map/copy_caches/pallas_call | solution.py:727
  4.3 28.5 %attention.1 = (bf16[4,24,256]{2,1,0:T(8,128)(2,1)S(1)}, bf16[4,512,512]{2,1,0:T(8,128)(2,1)S(1)}, bf16[4,512,512]{2,1,0:T(8,128)(2,1)S(1)}) custom-call(bf16[96,256]{1,0:T(8,128)(2,1)} %tok_hbm.1, f32[1,256]{1,0:T(1,128)} %bitcast.5, bf16[256,512]{1,0:T(8,128)(2,1)} %wq_hbm.1, bf16[256,512]{1,0:T(8,128)(2,1)} %wk_hbm.1, bf16[256,512]{1,0:T(8,128)(2,1)} %wv_hbm.1, ...), custom_call_target="tpu_custom_call" | custom-call | tf_op jit(solution)/shard_map/attention/pallas_call | solution.py:640
  32.8 0.7 %write.1 = (bf16[4,24,256]{2,1,0:T(8,128)(2,1)}, bf16[4,512,512]{2,1,0:T(8,128)(2,1)}, bf16[4,512,512]{2,1,0:T(8,128)(2,1)}) custom-call(bf16[4,24,256]{2,1,0:T(8,128)(2,1)S(1)} %get-tuple-element.12.mixed_ref, bf16[4,512,512]{2,1,0:T(8,128)(2,1)S(1)} %get-tuple-element.13.keys_ref, ...), custom_call_target="tpu_custom_call", output_to_operand_aliasing={{1}: (3, {}), {2}: (4, {})} | custom-call | tf_op jit(solution)/shard_map/write/pallas_call | solution.py:768

commit v10 on v9

--- a/solution.py
+++ b/solution.py
@@ -50,10 +50,10 @@
 DS_RECV = 16
 QG_RECV = 17
 KVG_RECV = 21
-NG_RECV = 22
-MX_RECV = 26
-GIVE_RECV = 30
-SEMAPHORES = 33
+NG_RECV = QG_RECV
+MX_RECV = 22
+GIVE_RECV = 26
+SEMAPHORES = 29
 OUT = 8
 Z_ORDER = (0, 1, 2, 3)
 Z_OUT = (0, 1, 3, 2)

time: 33.5 us -> 33.5 us (level)
  no operation moved by 1% of the time
where the time goes in v10:
time: 33.5 us; the launch traced here: 33.4 us
  Pallas kernels  32.7 us (98%)
  between operations  0.65 us (2%)
    pallas_call x1, Pallas kernels, _main(): pl.pallas_call(_main_kernel, out_shape=(jax.ShapeDtypeStruct((SEQS, PROP,...  28.5 us
    pallas_call x1, Pallas kernels, _copy(): pl.pallas_call(_copy_kernel, out_shape=tuple((jax.ShapeDtypeStruct(array....  3.63 us

profile of v10, /device:TPU:1, one launch (start us, length us, event | category | flops | bytes accessed | tf_op | source)
XLA Modules:
  0.0 33.4 jit_solution(13718949515536681620)
XLA Ops:
  0.6 3.6 %copy_caches.1 = (bf16[4,512,512]{2,1,0:T(8,128)(2,1)}, bf16[4,512,512]{2,1,0:T(8,128)(2,1)}) custom-call(bf16[4,512,512]{2,1,0:T(8,128)(2,1)} %ck_hbm.1, bf16[4,512,512]{2,1,0:T(8,128)(2,1)} %cv_hbm.1), custom_call_target="tpu_custom_call" | custom-call | tf_op jit(solution)/shard_map/copy_caches/pallas_call | solution.py:727
  4.3 28.5 %attention.1 = (bf16[4,24,256]{2,1,0:T(8,128)(2,1)S(1)}, bf16[4,512,512]{2,1,0:T(8,128)(2,1)S(1)}, bf16[4,512,512]{2,1,0:T(8,128)(2,1)S(1)}) custom-call(bf16[96,256]{1,0:T(8,128)(2,1)} %tok_hbm.1, f32[1,256]{1,0:T(1,128)} %bitcast.5, bf16[256,512]{1,0:T(8,128)(2,1)} %wq_hbm.1, bf16[256,512]{1,0:T(8,128)(2,1)} %wk_hbm.1, bf16[256,512]{1,0:T(8,128)(2,1)} %wv_hbm.1, ...), custom_call_target="tpu_custom_call" | custom-call | tf_op jit(solution)/shard_map/attention/pallas_call | solution.py:640
  32.7 0.7 %write.1 = (bf16[4,24,256]{2,1,0:T(8,128)(2,1)}, bf16[4,512,512]{2,1,0:T(8,128)(2,1)}, bf16[4,512,512]{2,1,0:T(8,128)(2,1)}) custom-call(bf16[4,24,256]{2,1,0:T(8,128)(2,1)S(1)} %get-tuple-element.12.mixed_ref, bf16[4,512,512]{2,1,0:T(8,128)(2,1)S(1)} %get-tuple-element.13.keys_ref, ...), custom_call_target="tpu_custom_call", output_to_operand_aliasing={{1}: (3, {}), {2}: (4, {})} | custom-call | tf_op jit(solution)/shard_map/write/pallas_call | solution.py:768
